TPU v7x, 256 devices: a whole 4x4x8 slice. The times are simulated.
256 devices in a mesh: sp: 64 (over z, x, core), tp: 4 (over y).
Axes of the slice: x: 4, y: 4, z: 8, core: 2. Of those that a mesh axis runs over, the one named last changes fastest.
Arguments:
- residual_in: bfloat16 [16384, 2048], P(('sp', 'tp')), may hold values from -6 to 6
- queries: bfloat16 [16384, 512], P('sp', 'tp'), may hold values from -6 to 6
- key_rows: bfloat16 [16384, 512], P('sp', 'tp'), may hold values from -6 to 6
- value_rows: bfloat16 [16384, 1024], P('sp', 'tp'), may hold values from -6 to 6
- out_gate: bfloat16 [16384, 1024], P('sp', 'tp'), may hold values from -6 to 6
- decay_logit: float32 [16384, 512], P('sp', 'tp'), may hold values from -30 to 30
- head_gain: bfloat16 [128], replicated, may hold values from 0.099609375 to 1.8984375
- w_out: bfloat16 [1024, 2048], replicated, may hold values from -0.1875 to 0.1875
- ffn_gain: bfloat16 [2048], replicated, may hold values from 0.099609375 to 1.8984375
- routing: int32 [16384, 4], P('sp'), may hold values from 0 to 63, all different within a row; in each aligned block of 64 rows (0 to 63, 64 to 127, ...) at most 8 rows name the same one
- route_weight: float32 [16384, 4], P(('sp', 'tp')), may hold values from 0.05 to 0.6
- w_gate: bfloat16 [64, 2048, 2048], P('sp', None, 'tp'), may hold values from -4 to 4
- w_up: bfloat16 [64, 2048, 2048], P('sp', None, 'tp'), may hold values from -4 to 4
- w_down: bfloat16 [64, 2048, 2048], P('sp', 'tp'), may hold values from -0.125 to 0.125
Outputs:
- layer_out: bfloat16 [16384, 2048], P(('sp', 'tp'))
Inputs may be any that keep to these rules, and one draw needn't show every extreme that they name: `routing`: each row names 4 different experts. In each aligned block of 64 rows no expert is named more than 8 times, a bound that some blocks reach.
All inputs are finite; a program needn't handle non-finite values.
Results may differ from a plain program's by a relative error of at most 0.03.
Values may be sent and summed in bfloat16 or wider, within the bound.
No kernel may reach another device: no remote copies, remote signals or barrier semaphores. Data moves between devices by JAX's collectives and lax.ppermute only.
A program may use at most 128 MiB of HBM per device.

v0:
```python
import jax
import jax.numpy as jnp
from jax import lax
from jax.sharding import Mesh
from jax.sharding import PartitionSpec as P

DK = 64
DV = 128
BLOCK = 64
SP = ("sp_0", "sp_1", "sp_2")
SP_TP = ("sp_0", "sp_1", "sp_2", "tp")


DECAY_TEMP = 16.0
CLAMP_LIMIT = 7.0
SIGMOID_SLOPE = 1.702
NORM_EPS = 1e-06


def filled_with(value, identity):
    return jax.tree.map(
        lambda part, zero: jnp.zeros_like(part) + jnp.asarray(zero, part.dtype), value, identity
    )


def collected_together(value, axis):
    leaves = jax.tree.leaves(value)
    order = sorted(range(len(leaves)), key=lambda k: -leaves[k].size)
    width = (1, *leaves[order[0]].shape)[-1]
    lines = [
        jnp.pad(leaves[k].reshape(-1), (0, -leaves[k].size % width)).reshape(-1, width)
        for k in order
    ]
    both, at, found = (lax.all_gather(jnp.concatenate(lines), axis), 0, {})
    for k, line in zip(order, lines):
        piece = both[:, at : at + len(line)].reshape(len(both), -1)
        found[k] = piece[:, : leaves[k].size].reshape(-1, *leaves[k].shape)
        at += len(line)
    numbers = iter(range(len(leaves)))
    return jax.tree.map(lambda _: found[next(numbers)], value)


def prefix_by_axis(value, axes, combine, identity):
    before = start = filled_with(value, identity)
    running = value
    for axis in reversed(axes):
        size, place = (lax.axis_size(axis), lax.axis_index(axis))
        pieces = collected_together(
            jax.tree.map(
                lambda part, kind: part.astype(kind), running, (jnp.bfloat16, jnp.bfloat16)
            ),
            axis,
        )
        inside, running = (start, start)
        for k in range(size):
            passed = k < place
            running = combine(
                running, jax.tree.map(lambda part, own: part[k].astype(own.dtype), pieces, value)
            )
            inside = jax.tree.map(lambda new, old: jnp.where(passed, new, old), running, inside)
        before = combine(inside, before)
    return before


def block_parts(query_blk, key_blk, value_blk, logdecay_blk):
    cumulative = jnp.cumsum(logdecay_blk, axis=2)
    length = cumulative.shape[2]
    causal = (jnp.arange(length)[:, None] >= jnp.arange(length)[None, :])[:, :, None]
    spread = cumulative[:, :, :, None, :] - cumulative[:, :, None, :, :]
    weighted = query_blk[:, :, :, None, :] * jnp.exp(jnp.where(causal, spread, -jnp.inf))
    scores = jnp.einsum("nhtsk,nhsk->nhts", weighted, key_blk)
    inner_part = jnp.einsum("nhts,nhsv->nhtv", scores, value_blk)
    ending = cumulative[:, :, -1:, :]
    contrib = jnp.einsum("nhsk,nhsv->nhkv", key_blk * jnp.exp(ending - cumulative), value_blk)
    return (inner_part, query_blk * jnp.exp(cumulative), contrib, jnp.exp(ending[:, :, 0, :]))


def carry_blocks(query_dec, contrib, passing, begin):

    def advance(recurrent_state, inputs):
        current_query, contrib_now, passing_now = inputs
        state_readout = jnp.einsum("uaz,uze->uae", current_query, recurrent_state)
        return (passing_now[..., None] * recurrent_state + contrib_now, state_readout)

    final_state, readouts = lax.scan(advance, begin, (query_dec, contrib, passing))
    return (readouts, final_state)


def fold_state(contrib, passing):

    def absorb(recurrent_state, inputs):
        contrib_now, passing_now = inputs
        return (passing_now[..., None] * recurrent_state + contrib_now, None)

    final_state, _ = lax.scan(absorb, jnp.zeros_like(contrib[0]), (contrib, passing))
    return final_state


def combine_states(earlier, following):
    return (earlier[0] * following[0], following[0][..., None] * earlier[1] + following[1])


def carried_state(total_decay, local_state):
    identity = (jnp.ones_like(total_decay), jnp.zeros_like(local_state))
    return prefix_by_axis((total_decay, local_state), SP, combine_states, identity)[1]


def to_blocks(array, head_width):
    tokens = array.shape[0]
    head_count = array.shape[1] // head_width
    return (
        array.astype(jnp.float32)
        .reshape(tokens // BLOCK, BLOCK, head_count, head_width)
        .transpose(0, 2, 1, 3)
    )


def finish_heads(blocks_out, head_gain, out_gate):
    count_blk, head_count, length, head_width = blocks_out.shape
    tokens = count_blk * length
    attended = blocks_out.transpose(0, 2, 1, 3).reshape(tokens, head_count, head_width)
    inv_scale = lax.rsqrt(jnp.mean(attended * attended, axis=-1, keepdims=True) + NORM_EPS)
    headed = attended * inv_scale * head_gain.astype(jnp.float32)
    gated = headed.reshape(tokens, head_count * head_width) * jax.nn.silu(
        out_gate.astype(jnp.float32)
    )
    return gated.astype(jnp.bfloat16)


def norm_rows(residual, gain_vec):
    values = residual.astype(jnp.float32)
    inv_scale = lax.rsqrt(jnp.mean(values * values, axis=-1, keepdims=True) + NORM_EPS)
    return (values * inv_scale * gain_vec.astype(jnp.float32)).astype(jnp.bfloat16)


def clamped_unit(gate_pre, up_pre):
    gate_cut = jnp.minimum(gate_pre, CLAMP_LIMIT)
    up_cut = jnp.clip(up_pre, -CLAMP_LIMIT, CLAMP_LIMIT)
    return (up_cut + 1.0) * (gate_cut * jax.nn.sigmoid(SIGMOID_SLOPE * gate_cut))


def slot_ids(routes, capacity, experts):
    batch_size, rows_each, top_count = routes.shape
    flat_ids = routes.reshape(batch_size, rows_each * top_count)
    onehot = (flat_ids[:, :, None] == jnp.arange(experts, dtype=jnp.int32)[None, None, :]).astype(
        jnp.int32
    )
    earlier = jnp.cumsum(onehot, axis=1) - onehot
    rank_in = jnp.sum(earlier * onehot, axis=2)
    return (flat_ids * capacity + rank_in).reshape(batch_size, rows_each, top_count)


def dispatch_rows(slots, row_data, slot_total):
    chosen = jnp.any(slots[..., None] == jnp.arange(slot_total, dtype=jnp.int32), axis=2).astype(
        jnp.bfloat16
    )
    return jnp.einsum("brs,brd->bsd", chosen, row_data, preferred_element_type=jnp.float32).astype(
        jnp.bfloat16
    )


def on_device(
    residual_in,
    queries,
    key_rows,
    value_rows,
    out_gate,
    decay_logit,
    head_gain,
    w_out,
    ffn_gain,
    routing,
    route_weight,
    w_gate,
    w_up,
    w_down,
):
    query_blk = to_blocks(queries, DK) * DK ** (-0.5)
    key_blk = to_blocks(key_rows, DK)
    value_blk = to_blocks(value_rows, DV)
    logdecay_blk = to_blocks(jax.nn.log_sigmoid(decay_logit) / DECAY_TEMP, DK)
    inner_part, query_dec, contrib, passing = block_parts(
        query_blk, key_blk, value_blk, logdecay_blk
    )
    total_decay = jnp.prod(passing, axis=0)
    local_state = fold_state(contrib, passing)
    incoming = carried_state(total_decay, local_state)
    readouts, _ = carry_blocks(query_dec, contrib, passing, incoming)
    mixed_blk = inner_part + readouts
    mixed_out = finish_heads(mixed_blk, head_gain, out_gate)
    tp_count = lax.axis_size("tp")
    quarter = mixed_out.shape[0] // tp_count
    by_token = lax.all_to_all(mixed_out, "tp", split_axis=0, concat_axis=1, tiled=True)
    projected = jnp.dot(by_token, w_out, preferred_element_type=jnp.float32)
    residual = (residual_in.astype(jnp.float32) + projected).astype(jnp.bfloat16)
    normed = norm_rows(residual, ffn_gain)
    experts = lax.axis_size(SP)
    top_count = routing.shape[1]
    capacity = 2 * routing.shape[0] * top_count // (tp_count * experts)
    model_width = normed.shape[1]
    slot_total = experts * capacity
    gate_cols = w_gate[0]
    up_cols = w_up[0]
    down_rows = w_down[0]
    own_routes = lax.dynamic_slice_in_dim(routing, lax.axis_index("tp") * quarter, quarter, 0)
    own_slots = slot_ids(own_routes[None], capacity, experts)[0]
    outgoing = dispatch_rows(own_slots[None], normed[None], slot_total)[0]
    arrived = lax.all_to_all(
        outgoing.reshape(experts, capacity, model_width),
        SP,
        split_axis=0,
        concat_axis=0,
        tiled=True,
    )
    portion = lax.all_gather(arrived[None], "tp", axis=0, tiled=True)
    flat_rows = portion.reshape(-1, model_width)
    gate_pre = jnp.dot(flat_rows, gate_cols, preferred_element_type=jnp.float32)
    up_pre = jnp.dot(flat_rows, up_cols, preferred_element_type=jnp.float32)
    hidden_rows = clamped_unit(gate_pre, up_pre).astype(jnp.bfloat16)
    hidden = hidden_rows.reshape(portion.shape[:-1] + (gate_cols.shape[1],))
    portion = hidden
    partial_out = jnp.dot(
        portion.reshape(-1, hidden.shape[-1]), down_rows, preferred_element_type=jnp.float32
    ).astype(jnp.bfloat16)
    partial_out = lax.optimization_barrier(partial_out)
    summed = lax.psum_scatter(
        partial_out.astype(jnp.float32)
        .reshape(portion.shape[:-1] + (model_width,))
        .astype(jnp.bfloat16),
        "tp",
        scatter_dimension=0,
        tiled=True,
    ).astype(jnp.float32)
    returned = lax.all_to_all(
        summed[0].astype(jnp.bfloat16), SP, split_axis=0, concat_axis=0, tiled=True
    )
    picked = jnp.take(
        returned.reshape(slot_total, model_width), own_slots.reshape(-1), axis=0
    ).reshape(quarter, top_count, model_width)
    routed = jnp.sum(picked.astype(jnp.float32) * route_weight[:, :, None], axis=1)
    return (residual.astype(jnp.float32) + routed).astype(jnp.bfloat16)


def solution(mesh):
    torus = Mesh(mesh.devices.reshape(8, 4, 2, mesh.shape["tp"]), ("sp_0", "sp_1", "sp_2", "tp"))
    placed = (
        P(SP_TP, None),
        P(SP, "tp"),
        P(SP, "tp"),
        P(SP, "tp"),
        P(SP, "tp"),
        P(SP, "tp"),
        P(),
        P(),
        P(),
        P(SP, None),
        P(SP_TP, None),
        P(SP, None, "tp"),
        P(SP, None, "tp"),
        P(SP, "tp", None),
    )
    return jax.shard_map(
        on_device, mesh=torus, in_specs=placed, out_specs=P(SP_TP, None), check_vma=False
    )
```

profile of v0, /device:TPU:2, one launch (start us, length us, event | category | flops | bytes accessed | tf_op | source)
XLA Modules:
  0.0 427.1 jit_solution(1445477589650038241)
XLA Ops:
  6.5 1.1 fusion.44
  8.2 0.9 reshape.647
  9.1 0.9 reshape.648
  11.0 1.8 all-gather.4
  13.5 12.1 %all-gather.5 = bf16[4,129,128]{2,1,0:T(8,128)(2,1)S(1)} all-gather(bf16[1,129,128]{2,1,0:T(8,128)(2,1)S(1)} %maximum_bitcast_fusion.1), channel_id=3, replica_groups=mesh['sp_0'=8,'sp_1'=4,'sp_2'=2,'tp'=4] {'sp_1'}, dimensions={0}, use_global_device_ids=true | all-gather | bytes 165120 | tf_op jit(solution)/shard_map/all_gather | solution.py:34
  26.3 28.6 %all-gather.6 = bf16[8,129,128]{2,1,0:T(8,128)(2,1)S(1)} all-gather(bf16[1,129,128]{2,1,0:T(8,128)(2,1)S(1)} %maximum_bitcast_fusion.2), channel_id=4, replica_groups=mesh['sp_0'=8,'sp_1'=4,'sp_2'=2,'tp'=4] {'sp_0'}, dimensions={0}, use_global_device_ids=true | all-gather | bytes 297216 | tf_op jit(solution)/shard_map/all_gather | solution.py:34
  58.6 0.7 reshape.662
  63.1 0.7 reshape.676
  66.8 1.5 fusion.54
  68.2 3.5 while.23
  68.3 0.8 fusion.111
  69.1 0.8 fusion.111
  70.0 0.8 fusion.111
  70.9 0.8 fusion.111
  71.8 3.9 exponential_multiply_fusion
  75.8 5.1 %fusion.5 = f32[4,2,64,1,64]{4,3,2,1,0:T(1,128)S(1)} fusion(bf16[4,2,64,64,64]{4,3,2,1,0:T(8,128)(2,1)S(1)} %exponential_multiply_fusion, bf16[4,2,64,64,1]{3,2,1,0,4:T(8,128)(2,1)S(1)} %bitcast.231), kind=kOutput, calls=%fused_computation.12 | convolution fusion | flops 4194304 | bytes 4390912 | tf_op jit(solution)/shard_map/nhtsk,nhsk->nhts/dot_general | solution.py:71
  82.0 0.8 fusion.42
  82.7 4.5 %all-to-all-start = ((bf16[4,64,256]{2,1,0:T(8,128)(2,1)}), bf16[4,64,256]{2,1,0:T(8,128)(2,1)S(1)}, u32[]{:S(2)}, u32[]{:S(2)}) async-start(bf16[4,64,256]{2,1,0:T(8,128)(2,1)} %bitcast.46), calls=%async_computation | async-start | bytes 262144 | tf_op jit(solution)/shard_map/all_to_all | solution.py:193
  89.2 4.0 all-to-all-done
  93.2 3.2 multiply_reduce_fusion.1
  96.4 0.8 fusion.13
  97.2 59.2 %all_to_all.29 = bf16[64,8,2048]{2,1,0:T(8,128)(2,1)} all-to-all(bf16[64,8,2048]{2,1,0:T(8,128)(2,1)S(1)} %fusion.13), channel_id=1, replica_groups=mesh['sp_0'=8,'sp_1'=4,'sp_2'=2,'tp'=4] {'sp_0','sp_1','sp_2'}, dimensions={0} | all-to-all | bytes 4194304 | tf_op jit(solution)/shard_map/all_to_all | solution.py:208
  156.5 80.1 %all-gather.9.cloned.1.call-done = bf16[256,8,2048]{2,1,0:T(8,128)(2,1)} async-done(((bf16[64,8,2048]{2,1,0:T(8,128)(2,1)}), bf16[256,8,2048]{2,1,0:T(8,128)(2,1)}) %all-gather.9.cloned.1.call-update) | async-done | bytes 8388624 | tf_op jit(solution)/shard_map/all_gather | solution.py:215
  236.5 10.4 %fusion.7 = f32[2048,512]{1,0:T(8,128)} fusion(bf16[256,8,2048]{2,1,0:T(8,128)(2,1)} %all-gather.9.cloned.1.call-done, bf16[1,2048,512]{2,1,0:T(8,128)(2,1)} %param.29), kind=kOutput, calls=%fused_computation.15 | convolution fusion | flops 4294967296 | bytes 14680064 | tf_op jit(solution)/shard_map/dot_general | solution.py:217
  247.0 15.2 %convolution_convert_fusion = bf16[2048,2048]{1,0:T(8,128)(2,1)} fusion(bf16[1,512,2048]{2,1,0:T(8,128)(2,1)S(1)} %copy-done, f32[2048,512]{1,0:T(8,128)} %fusion.7, bf16[256,8,2048]{2,1,0:T(8,128)(2,1)} %all-gather.9.cloned.1.call-done, bf16[1,2048,512]{2,1,0:T(8,128)(2,1)} %param.30), kind=kOutput, calls=%fused_computation.19 | convolution fusion | flops 8604614656 | bytes 25165824 | tf_op jit(solution)/shard_map/dot_general | solution.py:222
  262.2 84.2 %reduce-scatter.2.cloned.1.call-done = bf16[1,64,8,2048]{3,2,1,0:T(8,128)(2,1)} async-done(((bf16[4,64,8,2048]{3,2,1,0:T(8,128)(2,1)}), bf16[1,64,8,2048]{3,2,1,0:T(8,128)(2,1)}) %reduce-scatter.2.cloned.1.call-update) | async-done | bytes 2097168 | tf_op jit(solution)/shard_map/reduce_scatter | solution.py:226
  346.4 10.7 %all-to-all-start.2 = ((bf16[64,8,2048]{2,1,0:T(8,128)(2,1)}), bf16[64,8,2048]{2,1,0:T(8,128)(2,1)}, u32[]{:S(2)}, u32[]{:S(2)}) async-start(bf16[64,8,2048]{2,1,0:T(8,128)(2,1)} %bitcast.204), calls=%async_computation.3 | async-start | bytes 4194304 | tf_op jit(solution)/shard_map/all_to_all | solution.py:234
  357.6 50.7 %all-to-all-done.2 = bf16[64,8,2048]{2,1,0:T(8,128)(2,1)} async-done(((bf16[64,8,2048]{2,1,0:T(8,128)(2,1)}), bf16[64,8,2048]{2,1,0:T(8,128)(2,1)}, u32[]{:S(2)}, u32[]{:S(2)}) %all-to-all-start.2) | async-done | bytes 2097184 | tf_op jit(solution)/shard_map/all_to_all | solution.py:234
  408.3 5.2 %gather_fusion = bf16[256,2048]{1,0:T(8,128)(2,1)} fusion(bf16[512,2048]{1,0:T(8,128)(2,1)} %bitcast.61, s32[1024]{0:T(1024)S(1)} %pad_clamp_fusion), kind=kCustom, calls=%fused_computation | custom fusion | bytes 2098176 | tf_op jit(solution)/shard_map/jit(_take)/gather | solution.py:237
  413.5 2.3 gather.7
  415.8 3.6 multiply_reduce_fusion
  419.5 0.8 add_convert_fusion
  (116 shorter events, 17.3 us)
Async XLA Ops:
  6.5 240.4 %copy-start = (bf16[1,512,2048]{2,1,0:T(8,128)(2,1)S(1)}, bf16[1,512,2048]{2,1,0:T(8,128)(2,1)}, u32[]{:S(2)}) copy-start(bf16[1,512,2048]{2,1,0:T(8,128)(2,1)} %param.31) | copy-start | bytes 6291460
  6.5 51.1 %copy-start.5 = (bf16[256,128]{1,0:T(8,128)(2,1)S(1)}, bf16[256,128]{1,0:T(8,128)(2,1)}, u32[]{:S(2)}) copy-start(bf16[256,128]{1,0:T(8,128)(2,1)} %param.19) | copy-start | bytes 196612
  71.8 3.9 copy-start.3
  75.7 5.2 %copy-start.1 = (f32[4,2,64,128]{3,2,1,0:T(8,128)S(1)}, f32[4,2,64,128]{3,2,1,0:T(8,128)}, u32[]{:S(2)}) copy-start(f32[4,2,64,128]{3,2,1,0:T(8,128)} %get-tuple-element.60) | copy-start | bytes 786436
  75.7 5.9 %copy-start.9 = (bf16[128]{0:T(256)(128)(2,1)S(1)}, bf16[128]{0:T(256)(128)(2,1)}, u32[]{:S(2)}) copy-start(bf16[128]{0:T(256)(128)(2,1)} %param.24) | copy-start | bytes 772
  75.8 6.2 %copy-start.4 = (bf16[256,256]{1,0:T(8,128)(2,1)S(1)}, bf16[256,256]{1,0:T(8,128)(2,1)}, u32[]{:S(2)}) copy-start(bf16[256,256]{1,0:T(8,128)(2,1)} %param.22) | copy-start | bytes 393220
  75.8 11.4 %copy-start.8 = (s32[256,4]{0,1:T(4,128)S(1)}, s32[256,4]{0,1:T(4,128)}, u32[]{:S(2)}) copy-start(s32[256,4]{0,1:T(4,128)} %param.27) | copy-start | bytes 12292
  75.8 13.3 %copy-start.6 = (bf16[2048]{0:T(1024)(128)(2,1)S(1)}, bf16[2048]{0:T(1024)(128)(2,1)}, u32[]{:S(2)}) copy-start(bf16[2048]{0:T(1024)(128)(2,1)} %param.26) | copy-start | bytes 12292
  80.9 12.3 %copy-start.2 = (bf16[64,2048]{1,0:T(8,128)(2,1)S(1)}, bf16[64,2048]{1,0:T(8,128)(2,1)}, u32[]{:S(2)}) copy-start(bf16[64,2048]{1,0:T(8,128)(2,1)} %param.18) | copy-start | bytes 786436
  82.7 10.4 %all-to-all-start = ((bf16[4,64,256]{2,1,0:T(8,128)(2,1)}), bf16[4,64,256]{2,1,0:T(8,128)(2,1)S(1)}, u32[]{:S(2)}, u32[]{:S(2)}) async-start(bf16[4,64,256]{2,1,0:T(8,128)(2,1)} %bitcast.46), calls=%async_computation | async-start | bytes 262144 | tf_op jit(solution)/shard_map/all_to_all | solution.py:193
  87.2 149.3 %all-gather.9.cloned.1.call-start = ((), (), s32[]{:S(2)}) async-start(), calls=%async_computation.5 | async-start | bytes 10485760 | tf_op jit(solution)/shard_map/all_gather | solution.py:215
  156.4 190.0 %reduce-scatter.2.cloned.1.call-start = ((), (), s32[]{:S(2)}) async-start(), calls=%async_computation.4 | async-start | bytes 10485760 | tf_op jit(solution)/shard_map/reduce_scatter | solution.py:226
  262.2 95.3 %copy-start.7 = (f32[64,4]{0,1:T(4,128)S(1)}, f32[64,4]{0,1:T(4,128)}, u32[]{:S(2)}) copy-start(f32[64,4]{0,1:T(4,128)} %param.28) | copy-start | bytes 3076
  346.4 61.9 %all-to-all-start.2 = ((bf16[64,8,2048]{2,1,0:T(8,128)(2,1)}), bf16[64,8,2048]{2,1,0:T(8,128)(2,1)}, u32[]{:S(2)}, u32[]{:S(2)}) async-start(bf16[64,8,2048]{2,1,0:T(8,128)(2,1)} %bitcast.204), calls=%async_computation.3 | async-start | bytes 4194304 | tf_op jit(solution)/shard_map/all_to_all | solution.py:234
Sparse Core Ops, SparseCore 0:
  156.5 79.9 all-gather.8
  262.3 84.0 reduce-scatter.1
where the time goes:
time: 428 us; the launch traced here: 427 us
  waiting for transfers between devices  219 us (51%)
  blocking collectives  102 us (24%)
  matrix products  38.4 us (9%)
  local copies, waits for them, and re-layouts  21.3 us (5%)
  other arithmetic  17.3 us (4%)
  starting transfers between devices  15.2 us (4%)
  between operations  13.8 us (3%)
    reduce_scatter x1, waiting for transfers between devices, on_device(): lax.psum_scatter(partial_out.astype(jnp.float32).reshape(portion.shape[:-...  84.2 us
    all_gather x1, waiting for transfers between devices, on_device(): portion = lax.all_gather(arrived[None], 'tp', axis=0, tiled=True)  80.1 us
    all_to_all x1, blocking collectives, on_device(): lax.all_to_all(outgoing.reshape(experts, capacity, model_width), SP, spli...  59.2 us
    all_to_all x1, waiting for transfers between devices, on_device(): lax.all_to_all(summed[0].astype(jnp.bfloat16), SP, split_axis=0, concat_a...  50.7 us
    all_gather x3, blocking collectives, collected_together(): both, at, found = (lax.all_gather(jnp.concatenate(lines), axis), 0, {})  42.6 us
    dot_general x1, matrix products, on_device(): jnp.dot(portion.reshape(-1, hidden.shape[-1]), down_rows, preferred_eleme...  15.2 us
    all_to_all x1, starting transfers between devices, on_device(): lax.all_to_all(summed[0].astype(jnp.bfloat16), SP, split_axis=0, concat_a...  10.7 us
    dot_general x1, matrix products, on_device(): gate_pre = jnp.dot(flat_rows, gate_cols, preferred_element_type=jnp.float32)  10.4 us
  transfers between devices with their start and end apart: 4, of which 4 were waited for; matrix products, arithmetic and copies ran while one was open for 1% of the time, Pallas kernels for 0%

commit v1 on v0

v1 whole, which is shorter than its diff:
```python
import jax
import jax.numpy as jnp
from jax import lax
from jax.experimental import pallas as pl
from jax.experimental.pallas import tpu as pltpu
from jax.sharding import Mesh
from jax.sharding import PartitionSpec as P


DK = 64
DV = 128
BLOCK = 64
SP = ("sp_0", "sp_1", "sp_2")
SP_TP = ("sp_0", "sp_1", "sp_2", "tp")
PLANE = ("sp_1", "sp_2")
DECAY_TEMP = 16.0
CLAMP_LIMIT = 7.0
SIGMOID_SLOPE = 1.702
NORM_EPS = 1e-06
F32 = jnp.float32
BF16 = jnp.bfloat16

ROW_PAIRS = [(c * 4 + y, c * 4 + ((y ^ 1) if c == 0 else 3 - y)) for c in range(2) for y in range(4)]
WEIGHT_PAIRS = [(c * 4 + y, c * 4 + ((3 - y) if c == 0 else (y ^ 1))) for c in range(2) for y in range(4)]


def dot(a, b, dims):
    return lax.dot_general(a, b, (dims, ((), ())), preferred_element_type=F32)


def split3(x):
    hi = x.astype(BF16)
    rest = x - hi.astype(F32)
    mid = rest.astype(BF16)
    return hi, mid, (rest - mid.astype(F32)).astype(BF16)


def head_mask(shape):
    return lax.broadcasted_iota(jnp.int32, shape, 1) < DK


def pick_heads(both):
    top, bottom = both[:DV], both[DV:]
    return jnp.where(head_mask(top.shape), top, bottom)


def stack_heads(x):
    zero = jnp.zeros_like(x)
    mask = head_mask(x.shape)
    return jnp.concatenate([jnp.where(mask, x, zero), jnp.where(mask, zero, x)], axis=0)


def store_state(out_ref, state_t, log_total):
    packed = jnp.concatenate(
        [
            state_t,
            *(part.astype(F32) for part in split3(log_total)),
            jnp.zeros((5, 2 * DK), F32),
        ],
        axis=0,
    ).astype(BF16)
    for copy in range(out_ref.shape[0]):
        out_ref[copy] = packed


def load_state(ref, k):
    item = ref[k].astype(F32)
    return item[:DV], item[DV : DV + 1] + item[DV + 1 : DV + 2] + item[DV + 2 : DV + 3]


def local_kernel(k_ref, v_ref, d_ref, state_ref, cum_ref):
    logit = d_ref[...]
    logdecay = (jnp.minimum(logit, 0.0) - jnp.log1p(jnp.exp(-jnp.abs(logit)))) / DECAY_TEMP
    rows = logdecay.shape[0]
    low = (
        lax.broadcasted_iota(jnp.int32, (rows, rows), 0)
        >= lax.broadcasted_iota(jnp.int32, (rows, rows), 1)
    ).astype(F32).astype(BF16)
    cum = sum(dot(low, part, ((1,), (0,))) for part in split3(logdecay))
    cum_ref[...] = cum
    end = cum[rows - 1 : rows]
    kdec = (k_ref[...].astype(F32) * jnp.exp(end - cum)).astype(BF16)
    state_t = pick_heads(dot(v_ref[...], kdec, ((0,), (0,))))
    store_state(state_ref, state_t, end)


def inner_kernel(q_ref, k_ref, v_ref, cum_ref, inner_ref, qdec_ref):
    rows = q_ref.shape[0]
    half = BLOCK // 2
    cum_all = cum_ref[...]
    q_all = q_ref[...].astype(F32) * (DK**-0.5)
    qdec_ref[...] = (q_all * jnp.exp(cum_all)).astype(BF16)
    row = lax.broadcasted_iota(jnp.int32, (BLOCK, 2 * DK), 0)
    t = lax.broadcasted_iota(jnp.int32, (2 * BLOCK, BLOCK), 0) % BLOCK
    s = lax.broadcasted_iota(jnp.int32, (2 * BLOCK, BLOCK), 1)
    near = (t >= s) & ((t < half) == (s < half))
    far = (t >= half) & (s < half)
    state = jnp.zeros((DV, 2 * DK), F32)
    for b in range(rows // BLOCK):
        at = slice(b * BLOCK, (b + 1) * BLOCK)
        cum = cum_all[at]
        if b:
            cum = cum - cum_all[b * BLOCK - 1 : b * BLOCK]
        q, k, v = q_all[at], k_ref[at, :].astype(F32), v_ref[at, :]
        middle = jnp.where(row < half, cum[half // 2 - 1 : half // 2], cum[half + half // 2 - 1 : half + half // 2])
        border = cum[half - 1 : half]
        end = cum[BLOCK - 1 : BLOCK]
        shifted = cum - middle
        q_near = (q * jnp.exp(shifted)).astype(BF16)
        k_near = (k * jnp.exp(-shifted)).astype(BF16)
        q_far = (q * jnp.exp(jnp.minimum(cum - border, 0.0))).astype(BF16)
        k_far = (k * jnp.exp(jnp.minimum(border - cum, 0.0))).astype(BF16)
        s_near = dot(stack_heads(q_near), k_near, ((1,), (1,)))
        s_far = dot(stack_heads(q_far), k_far, ((1,), (1,)))
        scores = jnp.where(near, s_near, jnp.where(far, s_far, 0.0)).astype(BF16)
        part0 = dot(scores[:BLOCK], v[:, :DV], ((1,), (0,)))
        part1 = dot(scores[BLOCK:], v[:, DV:], ((1,), (0,)))
        if b:
            read = dot(stack_heads((q * jnp.exp(cum)).astype(BF16)), state.astype(BF16), ((1,), (1,)))
            part0 = part0 + read[:BLOCK]
            part1 = part1 + read[BLOCK:]
        inner_ref[at, :DV] = part0
        inner_ref[at, DV:] = part1
        if (b + 1) * BLOCK < rows:
            kdec = (k * jnp.exp(end - cum)).astype(BF16)
            added = pick_heads(dot(v, kdec, ((0,), (0,))))
            state = added if b == 0 else state * jnp.exp(end) + added


def plane_kernel(at_ref, all_ref, total_ref, before_ref, logb_ref):
    place = at_ref[0]
    before = total = jnp.zeros((DV, 2 * DK), F32)
    log_before = log_total = jnp.zeros((1, 2 * DK), F32)
    for k in range(all_ref.shape[0]):
        state, log = load_state(all_ref, k)
        decay = jnp.exp(log)
        total = total * decay + state
        log_total = log_total + log
        before = jnp.where(k < place, before * decay + state, before)
        log_before = jnp.where(k < place, log_before + log, log_before)
    store_state(total_ref, total, log_total)
    before_ref[...] = before
    logb_ref[...] = jnp.broadcast_to(log_before, logb_ref.shape)


def finish_kernel(at_ref, all_ref, before_ref, logb_ref, inner_ref, qdec_ref, gate_ref, gain_ref, out_ref):
    place = at_ref[0]
    state = jnp.zeros((DV, 2 * DK), F32)
    for k in range(all_ref.shape[0]):
        added, log = load_state(all_ref, k)
        state = jnp.where(k < place, state * jnp.exp(log) + added, state)
    state = state * jnp.exp(logb_ref[0:1]) + before_ref[...]
    read = dot(stack_heads(qdec_ref[...]), state.astype(BF16), ((1,), (1,)))
    rows = inner_ref.shape[0]
    quarter = rows // out_ref.shape[0]
    gain = gain_ref[...].astype(F32)
    for h in range(2):
        cols = slice(h * DV, (h + 1) * DV)
        attended = inner_ref[:, cols] + read[h * rows : (h + 1) * rows]
        scale = lax.rsqrt(jnp.mean(attended * attended, axis=1, keepdims=True) + NORM_EPS)
        gate = gate_ref[:, cols].astype(F32)
        mixed = (attended * scale * gain * (gate / (1.0 + jnp.exp(-gate)))).astype(BF16)
        for j in range(out_ref.shape[0]):
            out_ref[j, :, cols] = mixed[j * quarter : (j + 1) * quarter]


def call(kernel, outs, *args, flops=2**20):
    specs = [
        pl.BlockSpec(memory_space=pltpu.SMEM if a.dtype == jnp.int32 else pltpu.VMEM) for a in args
    ]
    return pl.pallas_call(
        kernel,
        out_shape=outs,
        in_specs=specs,
        out_specs=[pl.BlockSpec(memory_space=pltpu.VMEM)] * len(outs),
        cost_estimate=pl.CostEstimate(flops=flops, bytes_accessed=2**19, transcendentals=2**16),
    )(*args)


def shaped(shape, dtype):
    return jax.ShapeDtypeStruct(shape, dtype)


def mixer(queries, key_rows, value_rows, out_gate, decay_logit, head_gain):
    rows = queries.shape[0]
    planes, members, tps = lax.axis_size("sp_0"), lax.axis_size(PLANE), lax.axis_size("tp")
    packed = DV + 8
    state, cum = call(
        local_kernel,
        [shaped((members, packed, 2 * DK), BF16), shaped((rows, 2 * DK), F32)],
        key_rows, value_rows, decay_logit,
    )
    inner, qdec = call(
        inner_kernel,
        [shaped((rows, 2 * DV), F32), shaped((rows, 2 * DK), BF16)],
        queries, key_rows, value_rows, cum,
    )
    in_plane = lax.all_to_all(state, PLANE, 0, 0, tiled=True)
    total, before, logb = call(
        plane_kernel,
        [shaped((planes, packed, 2 * DK), BF16), shaped((DV, 2 * DK), F32), shaped((8, 2 * DK), F32)],
        lax.axis_index(PLANE)[None].astype(jnp.int32), in_plane,
    )
    along = lax.all_to_all(total, "sp_0", 0, 0, tiled=True)
    (mixed,) = call(
        finish_kernel,
        [shaped((tps, rows // tps, 2 * DV), BF16)],
        lax.axis_index("sp_0")[None].astype(jnp.int32), along, before, logb, inner, qdec, out_gate,
        head_gain[None],
    )
    return lax.all_to_all(mixed, "tp", 0, 0, tiled=True)


def clamped_unit(gate_pre, up_pre):
    gate_cut = jnp.minimum(gate_pre, CLAMP_LIMIT)
    up_cut = jnp.clip(up_pre, -CLAMP_LIMIT, CLAMP_LIMIT)
    return (up_cut + 1.0) * (gate_cut / (1.0 + jnp.exp(-SIGMOID_SLOPE * gate_cut)))


def ffn_kernel(x_ref, g0, u0, d0, g1, u1, d1, out_ref, g_buf, u_buf, d_buf, sem):
    copies = [
        [
            pltpu.make_async_copy(src, buf.at[half], sem.at[half, j])
            for j, (src, buf) in enumerate(zip(srcs, (g_buf, u_buf, d_buf)))
        ]
        for half, srcs in enumerate(((g0, u0, d0), (g1, u1, d1)))
    ]
    for half in copies:
        for copy in half:
            copy.start()
    total = None
    for half, (gate_copy, up_copy, down_copy) in enumerate(copies):
        gate_copy.wait()
        gate_pre = dot(x_ref[...], g_buf[half], ((1,), (0,)))
        up_copy.wait()
        up_pre = dot(x_ref[...], u_buf[half], ((1,), (0,)))
        hidden = clamped_unit(gate_pre, up_pre).astype(BF16)
        down_copy.wait()
        part = dot(hidden, d_buf[half], ((1,), (0,)))
        total = part if total is None else total + part
    out_ref[...] = total.astype(out_ref.dtype)


def ffn(x, own, other, dtype):
    rows, width = x.shape
    units = own[0].shape[1]
    return pl.pallas_call(
        ffn_kernel,
        out_shape=shaped((rows, width), dtype),
        in_specs=[pl.BlockSpec(memory_space=pltpu.VMEM)] + [pl.BlockSpec(memory_space=pl.ANY)] * 6,
        out_specs=pl.BlockSpec(memory_space=pltpu.VMEM),
        scratch_shapes=[
            pltpu.VMEM((2, width, units), BF16),
            pltpu.VMEM((2, width, units), BF16),
            pltpu.VMEM((2, units, width), BF16),
            pltpu.SemaphoreType.DMA((2, 3)),
        ],
        cost_estimate=pl.CostEstimate(
            flops=12 * rows * width * units, bytes_accessed=12 * width * units, transcendentals=2 * rows * units
        ),
    )(x, *own, *other)


def blend(rank, weight, cap):
    slots = jnp.arange(cap).astype(F32)
    full = jnp.where(rank[:, :, None] == slots, weight[:, :, None], 0.0).reshape(rank.shape[0], -1)
    lead = lax.reduce_precision(full, 8, 7)
    return lead.astype(BF16), (full - lead).astype(BF16)


def on_device(
    residual_in, queries, key_rows, value_rows, out_gate, decay_logit, head_gain, w_out, ffn_gain,
    routing, route_weight, w_gate, w_up, w_down,
):
    core_tp = ("sp_2", "tp")
    own = (w_gate[0], w_up[0], w_down[0])
    other = []
    for w in own:
        other.append(lax.ppermute(w, core_tp, WEIGHT_PAIRS))
    experts, cores = lax.axis_size(SP), lax.axis_size("sp_2")
    columns = experts // cores
    quarter, width = residual_in.shape
    cap = 2 * routing.shape[0] * routing.shape[1] // (lax.axis_size("tp") * experts)
    slots = jnp.arange(cap).astype(F32)
    swap_cores = [(0, 1), (1, 0)]

    routes = lax.dynamic_slice_in_dim(routing, lax.axis_index("tp") * quarter, quarter, 0)
    named = routes[:, :, None] == jnp.arange(experts, dtype=jnp.int32)
    chosen = jnp.any(named, axis=1)
    weight = jnp.sum(jnp.where(named, route_weight[:, :, None], 0.0), axis=1)
    earlier = jnp.tril(jnp.ones((quarter, quarter), BF16), -1)
    rank = jnp.where(chosen, jnp.dot(earlier, chosen.astype(BF16), preferred_element_type=F32), -1.0)
    both = jnp.stack([rank, weight]).reshape(2, quarter, columns, cores)
    core = lax.axis_index("sp_2")
    here = lax.dynamic_index_in_dim(both, core, 3, keepdims=False)
    away = lax.dynamic_index_in_dim(both, 1 - core, 3, keepdims=False)
    theirs_plan = lax.ppermute(away, "sp_2", swap_cores)
    plans = (here, theirs_plan)

    by_token = mixer(queries, key_rows, value_rows, out_gate, decay_logit, head_gain)
    by_token = by_token.transpose(1, 0, 2).reshape(quarter, -1)
    projected = jnp.dot(by_token, w_out, preferred_element_type=F32)
    residual = (residual_in.astype(F32) + projected).astype(BF16)
    values = residual.astype(F32)
    scale = lax.rsqrt(jnp.mean(values * values, axis=-1, keepdims=True) + NORM_EPS)
    normed = (values * scale * ffn_gain.astype(F32)).astype(BF16)
    normed_other = lax.ppermute(normed, "sp_2", swap_cores)

    columns_axes = ("sp_0", "sp_1")
    arrived, swapped = [], []
    for c, source in enumerate((normed, normed_other)):
        send = (plans[c][0].T[:, None, :] == slots[None, :, None]).astype(BF16)
        rows = jnp.dot(send.reshape(columns * cap, quarter), source, preferred_element_type=F32).astype(BF16)
        rows = lax.all_to_all(rows.reshape(columns, cap, width), columns_axes, 0, 0, tiled=True)
        rows = rows.reshape(columns * cap, width)
        arrived.append(rows)
        swapped.append(lax.ppermute(rows, core_tp, ROW_PAIRS))
    sums = []
    for c in range(2):
        mine = ffn(arrived[c], own, other, F32)
        theirs = ffn(swapped[c], own, other, BF16)
        back = lax.ppermute(theirs, core_tp, ROW_PAIRS)
        out = (mine + back.astype(F32)).astype(BF16)
        home = lax.all_to_all(out.reshape(columns, cap, width), columns_axes, 0, 0, tiled=True)
        home = home.reshape(columns * cap, width)
        lead, rest = blend(plans[c][0], plans[c][1], cap)
        sums.append(jnp.dot(jnp.concatenate([lead, rest], axis=1), jnp.concatenate([home, home]), preferred_element_type=F32))
    from_other = lax.ppermute(sums[1], "sp_2", swap_cores)
    return (residual.astype(F32) + (sums[0] + from_other)).astype(BF16)


def solution(mesh):
    torus = Mesh(mesh.devices.reshape(8, 4, 2, mesh.shape["tp"]), ("sp_0", "sp_1", "sp_2", "tp"))
    placed = (
        P(SP_TP, None), P(SP, "tp"), P(SP, "tp"), P(SP, "tp"), P(SP, "tp"), P(SP, "tp"),
        P(), P(), P(),
        P(SP, None), P(SP_TP, None),
        P(SP, None, "tp"), P(SP, None, "tp"), P(SP, "tp", None),
    )

    return jax.shard_map(on_device, mesh=torus, in_specs=placed, out_specs=P(SP_TP, None), check_vma=False)
```

time: 428 us -> 247 us (0.58)
  blocking collectives: 102 us -> 0 us
  waiting for transfers between devices: 219 us -> 127 us
  Pallas kernels: 0 us -> 43.4 us
  starting transfers between devices: 15.2 us -> 55.6 us
  matrix products: 38.4 us -> 8.84 us
  local copies, waits for them, and re-layouts: 21.3 us -> 3.5 us
  between operations: 13.8 us -> 0.28 us
  other arithmetic: 17.3 us -> 7.13 us
    reduce_scatter x1 -> x0, waiting for transfers between devices: 84.2 us -> none  [on_device(): lax.psum_scatter(partial_out.astype(jnp.float32).reshape(portion.shape[:-...]
    all_gather x1 -> x0, waiting for transfers between devices: 80.1 us -> none  [on_device(): portion = lax.all_gather(arrived[None], 'tp', axis=0, tiled=True)]
    ppermute x0 -> x10, waiting for transfers between devices: none -> 60.2 us  [the longest x3 48.6 us: on_device(): other.append(lax.ppermute(w, core_tp, WEIGHT_PAIRS))]
    all_to_all x1 -> x0, blocking collectives: 59.2 us -> none  [on_device(): lax.all_to_all(outgoing.reshape(experts, capacity, model_width), SP, spli...]
    pallas_call x0 -> x8, Pallas kernels: none -> 43.4 us  [the longest x4 34.6 us: ffn(): pl.pallas_call(ffn_kernel, out_shape=shaped((rows, width), dtype), in_spe...]
    all_gather x3 -> x0, blocking collectives: 42.6 us -> none  [collected_together(): both, at, found = (lax.all_gather(jnp.concatenate(lines), axis), 0, {})]
    all_to_all x2 -> x7, starting transfers between devices: 15.2 us -> 48.1 us  [the longest x2 19.7 us: on_device(): lax.all_to_all(out.reshape(columns, cap, width), columns_axes, 0, 0, tile...]
    dot_general x11 -> x6, matrix products: 38.4 us -> 8.84 us  [the longest x1 3.16 us: on_device(): projected = jnp.dot(by_token, w_out, preferred_element_type=F32)]
  transfers between devices with their start and end apart: 4 -> 17, of which waited for: 4 -> 10; matrix products, arithmetic and copies ran while one was open for 1% -> 6% of each run, Pallas kernels for 0% -> 15%
where the time goes in v1:
time: 247 us; the launch traced here: 246 us
  waiting for transfers between devices  127 us (51%)
  starting transfers between devices  55.6 us (23%)
  Pallas kernels  43.4 us (18%)
  matrix products  8.84 us (4%)
  other arithmetic  7.13 us (3%)
  local copies, waits for them, and re-layouts  3.5 us (1%)
    ppermute x3, waiting for transfers between devices, on_device(): other.append(lax.ppermute(w, core_tp, WEIGHT_PAIRS))  48.6 us
    pallas_call x4, Pallas kernels, ffn(): pl.pallas_call(ffn_kernel, out_shape=shaped((rows, width), dtype), in_spe...  34.6 us
    all_to_all x2, waiting for transfers between devices, on_device(): lax.all_to_all(out.reshape(columns, cap, width), columns_axes, 0, 0, tile...  23.9 us
    all_to_all x2, waiting for transfers between devices, on_device(): lax.all_to_all(rows.reshape(columns, cap, width), columns_axes, 0, 0, til...  22.8 us
    all_to_all x2, starting transfers between devices, on_device(): lax.all_to_all(out.reshape(columns, cap, width), columns_axes, 0, 0, tile...  19.7 us
    all_to_all x2, starting transfers between devices, on_device(): lax.all_to_all(rows.reshape(columns, cap, width), columns_axes, 0, 0, til...  10.7 us
    ppermute x2, waiting for transfers between devices, on_device(): back = lax.ppermute(theirs, core_tp, ROW_PAIRS)  10.2 us
    pallas_call x4, Pallas kernels, call(): pl.pallas_call(kernel, out_shape=outs, in_specs=specs, out_specs=[pl.Bloc...  8.81 us
  transfers between devices with their start and end apart: 17, of which 10 were waited for; matrix products, arithmetic and copies ran while one was open for 6% of the time, Pallas kernels for 15%

profile of v1, /device:TPU:2, one launch (start us, length us, event | category | flops | bytes accessed | tf_op | source)
XLA Modules:
  0.0 245.7 jit_solution(4050193320461797452)
XLA Ops:
  0.0 2.3 shard_map.136
  2.3 5.6 %all-to-all-start = ((bf16[8,136,128]{2,1,0:T(8,128)(2,1)}), bf16[8,136,128]{2,1,0:T(8,128)(2,1)S(1)}, u32[]{:S(2)}, u32[]{:S(2)}) async-start(bf16[8,136,128]{2,1,0:T(8,128)(2,1)} %get-tuple-element.12), calls=%async_computation | async-start | bytes 557056 | tf_op jit(solution)/shard_map/all_to_all | solution.py:198
  8.0 6.2 %all-to-all-done.all_ref = bf16[8,136,128]{2,1,0:T(8,128)(2,1)S(1)} async-done(((bf16[8,136,128]{2,1,0:T(8,128)(2,1)}), bf16[8,136,128]{2,1,0:T(8,128)(2,1)S(1)}, u32[]{:S(2)}, u32[]{:S(2)}) %all-to-all-start) | async-done | bytes 278560 | tf_op jit(solution)/shard_map/all_to_all | solution.py:198
  14.9 1.8 shard_map.137
  16.7 7.7 %all-to-all-start.1 = ((bf16[8,136,128]{2,1,0:T(8,128)(2,1)}), bf16[8,136,128]{2,1,0:T(8,128)(2,1)S(1)}, u32[]{:S(2)}, u32[]{:S(2)}) async-start(bf16[8,136,128]{2,1,0:T(8,128)(2,1)} %get-tuple-element.13), calls=%async_computation.1 | async-start | bytes 557056 | tf_op jit(solution)/shard_map/all_to_all | solution.py:204
  25.7 2.5 %shard_map.138 = (f32[256,256]{1,0:T(8,128)}, bf16[256,128]{1,0:T(8,128)(2,1)}) custom-call(bf16[256,128]{1,0:T(8,128)(2,1)} %q_ref.1, bf16[256,128]{1,0:T(8,128)(2,1)} %k_ref.3, bf16[256,256]{1,0:T(8,128)(2,1)} %v_ref.3, f32[256,128]{1,0:T(8,128)} %get-tuple-element.16.cum_ref), custom_call_target="tpu_custom_call" | custom-call | flops 1048576 | bytes 524288 | tf_op jit(solution)/shard_map/pallas_call | solution.py:171
  28.2 8.1 %all-to-all-done.1.all_ref = bf16[8,136,128]{2,1,0:T(8,128)(2,1)S(1)} async-done(((bf16[8,136,128]{2,1,0:T(8,128)(2,1)}), bf16[8,136,128]{2,1,0:T(8,128)(2,1)S(1)}, u32[]{:S(2)}, u32[]{:S(2)}) %all-to-all-start.1) | async-done | bytes 278560 | tf_op jit(solution)/shard_map/all_to_all | solution.py:204
  36.9 2.2 shard_map.139
  39.1 4.5 %all-to-all-start.2 = ((bf16[4,64,256]{2,1,0:T(8,128)(2,1)}), bf16[4,64,256]{2,1,0:T(8,128)(2,1)S(1)}, u32[]{:S(2)}, u32[]{:S(2)}) async-start(bf16[4,64,256]{2,1,0:T(8,128)(2,1)} %shard_map.139), calls=%async_computation.2 | async-start | bytes 262144 | tf_op jit(solution)/shard_map/all_to_all | solution.py:211
  43.8 5.8 %all-to-all-done.2 = bf16[4,64,256]{2,1,0:T(8,128)(2,1)S(1)} async-done(((bf16[4,64,256]{2,1,0:T(8,128)(2,1)}), bf16[4,64,256]{2,1,0:T(8,128)(2,1)S(1)}, u32[]{:S(2)}, u32[]{:S(2)}) %all-to-all-start.2) | async-done | bytes 131104 | tf_op jit(solution)/shard_map/all_to_all | solution.py:211
  49.6 3.2 %multiply_reduce_fusion = (f32[64]{0:T(128)S(1)}, f32[64,2048]{1,0:T(8,128)S(1)}) fusion(bf16[64,1024]{1,0:T(8,128)(2,1)S(1)} %bitcast.90, bf16[1024,2048]{1,0:T(8,128)(2,1)} %param.21, bf16[64,2048]{1,0:T(8,128)(2,1)S(1)} %copy-done.8), kind=kOutput, calls=%fused_computation.23 | convolution fusion | flops 269221824 | bytes 5112064 | tf_op jit(solution)/shard_map/dot_general | solution.py:302
  53.9 1.4 collective-permute-done.6
  55.3 1.6 fusion.1
  56.9 5.0 %all-to-all-start.5 = ((bf16[32,8,2048]{2,1,0:T(8,128)(2,1)}), bf16[32,8,2048]{2,1,0:T(8,128)(2,1)S(1)}, u32[]{:S(2)}, u32[]{:S(2)}) async-start(bf16[32,8,2048]{2,1,0:T(8,128)(2,1)} %fusion.1), calls=%async_computation.5 | async-start | bytes 2097152 | tf_op jit(solution)/shard_map/all_to_all | solution.py:314
  63.2 2.1 collective-permute-start.1
  66.4 1.4 fusion
  67.8 22.8 %all-to-all-done.5 = bf16[32,8,2048]{2,1,0:T(8,128)(2,1)S(1)} async-done(((bf16[32,8,2048]{2,1,0:T(8,128)(2,1)}), bf16[32,8,2048]{2,1,0:T(8,128)(2,1)S(1)}, u32[]{:S(2)}, u32[]{:S(2)}) %all-to-all-start.5) | async-done | bytes 1048608 | tf_op jit(solution)/shard_map/all_to_all | solution.py:314
  90.6 5.6 %all-to-all-start.3 = ((bf16[32,8,2048]{2,1,0:T(8,128)(2,1)}), bf16[32,8,2048]{2,1,0:T(8,128)(2,1)}, u32[]{:S(2)}, u32[]{:S(2)}) async-start(bf16[32,8,2048]{2,1,0:T(8,128)(2,1)} %fusion), calls=%async_computation.3 | async-start | bytes 2097152 | tf_op jit(solution)/shard_map/all_to_all | solution.py:314
  96.9 26.1 %collective-permute-done.1.u1 = bf16[2048,512]{1,0:T(8,128)(2,1)} collective-permute-done((bf16[2048,512]{1,0:T(8,128)(2,1)}, bf16[2048,512]{1,0:T(8,128)(2,1)}, u32[]{:S(2)}, u32[]{:S(2)}) %collective-permute-start.1) | collective-permute-done | bytes 2097184 | tf_op jit(solution)/shard_map/ppermute | solution.py:279
  123.1 22.5 %collective-permute-done.2.d1 = bf16[512,2048]{1,0:T(8,128)(2,1)} collective-permute-done((bf16[512,2048]{1,0:T(8,128)(2,1)}, bf16[512,2048]{1,0:T(8,128)(2,1)}, u32[]{:S(2)}, u32[]{:S(2)}) %collective-permute-start.2) | collective-permute-done | bytes 2097184 | tf_op jit(solution)/shard_map/ppermute | solution.py:279
  145.5 8.4 %shard_map.143 = bf16[256,2048]{1,0:T(8,128)(2,1)} custom-call(bf16[256,2048]{1,0:T(8,128)(2,1)} %collective-permute-done.7.x_ref, bf16[2048,512]{1,0:T(8,128)(2,1)} %bitcast.70, bf16[2048,512]{1,0:T(8,128)(2,1)} %bitcast.76, bf16[512,2048]{1,0:T(8,128)(2,1)} %bitcast.81, bf16[2048,512]{1,0:T(8,128)(2,1)} %collective-permute-done.g1, ...), custom_call_target="tpu_custom_call" | custom-call | flops 3221225472 | bytes 12582912 | tf_op jit(solution)/shard_map/pallas_call | solution.py:247
  154.1 2.0 collective-permute-start.3
  156.1 8.9 %shard_map.142 = f32[256,2048]{1,0:T(8,128)} custom-call(bf16[256,2048]{1,0:T(8,128)(2,1)} %bitcast.86, bf16[2048,512]{1,0:T(8,128)(2,1)} %bitcast.71, bf16[2048,512]{1,0:T(8,128)(2,1)} %bitcast.77, bf16[512,2048]{1,0:T(8,128)(2,1)} %bitcast.82, bf16[2048,512]{1,0:T(8,128)(2,1)} %collective-permute-done.g1, bf16[2048,512]{1,0:T(8,128)(2,1)} %collective-permute-done.1.u1, ...), custom_call_target="tpu_custom_call" | custom-call | flops 3221225472 | bytes 12582912 | tf_op jit(solution)/shard_map/pallas_call | solution.py:247
  165.0 4.1 %collective-permute-done.8 = bf16[256,2048]{1,0:T(8,128)(2,1)S(1)} collective-permute-done((bf16[256,2048]{1,0:T(8,128)(2,1)}, bf16[256,2048]{1,0:T(8,128)(2,1)S(1)}, u32[]{:S(2)}, u32[]{:S(2)}) %collective-permute-start.8) | collective-permute-done | bytes 1048608 | tf_op jit(solution)/shard_map/ppermute | solution.py:322
  169.1 2.9 %fusion.14 = bf16[32,8,2048]{2,1,0:T(8,128)(2,1)} fusion(f32[256,2048]{1,0:T(8,128)} %shard_map.142, bf16[256,2048]{1,0:T(8,128)(2,1)S(1)} %collective-permute-done.8), kind=kLoop, calls=%fused_computation.21 | loop fusion | flops 1572864 | bytes 4194304 | tf_op jit(solution)/shard_map/reshape | solution.py:324
  172.0 9.9 %all-to-all-start.6 = ((bf16[32,8,2048]{2,1,0:T(8,128)(2,1)}), bf16[32,8,2048]{2,1,0:T(8,128)(2,1)S(1)}, u32[]{:S(2)}, u32[]{:S(2)}) async-start(bf16[32,8,2048]{2,1,0:T(8,128)(2,1)} %fusion.14), calls=%async_computation.6 | async-start | bytes 2097152 | tf_op jit(solution)/shard_map/all_to_all | solution.py:324
  182.9 8.4 %shard_map.141 = bf16[256,2048]{1,0:T(8,128)(2,1)} custom-call(bf16[256,2048]{1,0:T(8,128)(2,1)} %copy-done.7, bf16[2048,512]{1,0:T(8,128)(2,1)} %bitcast.72, bf16[2048,512]{1,0:T(8,128)(2,1)} %bitcast.78, bf16[512,2048]{1,0:T(8,128)(2,1)} %bitcast.83, bf16[2048,512]{1,0:T(8,128)(2,1)} %collective-permute-done.g1, ...), custom_call_target="tpu_custom_call" | custom-call | flops 3221225472 | bytes 12582912 | tf_op jit(solution)/shard_map/pallas_call | solution.py:247
  191.4 8.9 %shard_map.140 = f32[256,2048]{1,0:T(8,128)} custom-call(bf16[256,2048]{1,0:T(8,128)(2,1)} %bitcast.13.x_ref, bf16[2048,512]{1,0:T(8,128)(2,1)} %bitcast.73, bf16[2048,512]{1,0:T(8,128)(2,1)} %bitcast.79, bf16[512,2048]{1,0:T(8,128)(2,1)} %bitcast.84, bf16[2048,512]{1,0:T(8,128)(2,1)} %collective-permute-done.g1, ...), custom_call_target="tpu_custom_call" | custom-call | flops 3221225472 | bytes 12582912 | tf_op jit(solution)/shard_map/pallas_call | solution.py:247
  200.3 6.1 %collective-permute-done.4 = bf16[256,2048]{1,0:T(8,128)(2,1)S(1)} collective-permute-done((bf16[256,2048]{1,0:T(8,128)(2,1)}, bf16[256,2048]{1,0:T(8,128)(2,1)S(1)}, u32[]{:S(2)}, u32[]{:S(2)}) %collective-permute-start.4) | collective-permute-done | bytes 1048608 | tf_op jit(solution)/shard_map/ppermute | solution.py:322
  206.4 2.9 %fusion.13 = bf16[32,8,2048]{2,1,0:T(8,128)(2,1)} fusion(f32[256,2048]{1,0:T(8,128)} %shard_map.140, bf16[256,2048]{1,0:T(8,128)(2,1)S(1)} %collective-permute-done.4), kind=kLoop, calls=%fused_computation.20 | loop fusion | flops 1572864 | bytes 4194304 | tf_op jit(solution)/shard_map/reshape | solution.py:324
  209.4 9.8 %all-to-all-start.4 = ((bf16[32,8,2048]{2,1,0:T(8,128)(2,1)}), bf16[32,8,2048]{2,1,0:T(8,128)(2,1)S(1)}, u32[]{:S(2)}, u32[]{:S(2)}) async-start(bf16[32,8,2048]{2,1,0:T(8,128)(2,1)} %fusion.13), calls=%async_computation.4 | async-start | bytes 2097152 | tf_op jit(solution)/shard_map/all_to_all | solution.py:324
  220.6 23.9 %all-to-all-done.4 = bf16[32,8,2048]{2,1,0:T(8,128)(2,1)S(1)} async-done(((bf16[32,8,2048]{2,1,0:T(8,128)(2,1)}), bf16[32,8,2048]{2,1,0:T(8,128)(2,1)S(1)}, u32[]{:S(2)}, u32[]{:S(2)}) %all-to-all-start.4) | async-done | bytes 1048608 | tf_op jit(solution)/shard_map/all_to_all | solution.py:324
  (55 shorter events, 10.9 us)
Async XLA Ops:
  0.0 7.9 %copy-start = (s32[256,4]{0,1:T(4,128)S(1)}, s32[256,4]{0,1:T(4,128)}, u32[]{:S(2)}) copy-start(s32[256,4]{0,1:T(4,128)} %param.23) | copy-start | bytes 12292
  0.0 43.8 %copy-start.9 = (bf16[2048]{0:T(1024)(128)(2,1)S(1)}, bf16[2048]{0:T(1024)(128)(2,1)}, u32[]{:S(2)}) copy-start(bf16[2048]{0:T(1024)(128)(2,1)} %param.22) | copy-start | bytes 12292
  0.0 49.6 %copy-start.8 = (bf16[64,2048]{1,0:T(8,128)(2,1)S(1)}, bf16[64,2048]{1,0:T(8,128)(2,1)}, u32[]{:S(2)}) copy-start(bf16[64,2048]{1,0:T(8,128)(2,1)} %param.14) | copy-start | bytes 786436
  2.3 11.8 %all-to-all-start = ((bf16[8,136,128]{2,1,0:T(8,128)(2,1)}), bf16[8,136,128]{2,1,0:T(8,128)(2,1)S(1)}, u32[]{:S(2)}, u32[]{:S(2)}) async-start(bf16[8,136,128]{2,1,0:T(8,128)(2,1)} %get-tuple-element.12), calls=%async_computation | async-start | bytes 557056 | tf_op jit(solution)/shard_map/all_to_all | solution.py:198
  14.2 0.7 copy-start.6
  16.7 19.5 %all-to-all-start.1 = ((bf16[8,136,128]{2,1,0:T(8,128)(2,1)}), bf16[8,136,128]{2,1,0:T(8,128)(2,1)S(1)}, u32[]{:S(2)}, u32[]{:S(2)}) async-start(bf16[8,136,128]{2,1,0:T(8,128)(2,1)} %get-tuple-element.13), calls=%async_computation.1 | async-start | bytes 557056 | tf_op jit(solution)/shard_map/all_to_all | solution.py:204
  36.2 0.7 copy-start.5
  39.1 10.4 %all-to-all-start.2 = ((bf16[4,64,256]{2,1,0:T(8,128)(2,1)}), bf16[4,64,256]{2,1,0:T(8,128)(2,1)S(1)}, u32[]{:S(2)}, u32[]{:S(2)}) async-start(bf16[4,64,256]{2,1,0:T(8,128)(2,1)} %shard_map.139), calls=%async_computation.2 | async-start | bytes 262144 | tf_op jit(solution)/shard_map/all_to_all | solution.py:211
  43.7 10.2 %collective-permute-start.5 = (f32[2,64,32]{1,2,0:T(8,128)S(1)}, f32[2,64,32]{1,2,0:T(8,128)S(1)}, u32[]{:S(2)}, u32[]{:S(2)}) collective-permute-start(f32[2,64,32]{1,2,0:T(8,128)S(1)} %bitcast.96), channel_id=1, source_target_pairs={{0,4},{4,0},{1,5},{5,1},{2,6},{6,2},{3,7},{7,3},{8,12},{12,8},{9,1... | collective-permute-start | bytes 49160 | tf_op jit(solution)/shard_map/ppermute | solution.py:297
  52.7 0.8 copy-start.3
  53.6 8.3 %copy-start.1 = (bf16[1,2048,512]{2,1,0:T(8,128)(2,1)S(1)}, bf16[1,2048,512]{2,1,0:T(8,128)(2,1)}, u32[]{:S(2)}) copy-start(bf16[1,2048,512]{2,1,0:T(8,128)(2,1)} %param.25) | copy-start | bytes 6291460
  53.7 1.6 collective-permute-start.6
  56.9 33.8 %all-to-all-start.5 = ((bf16[32,8,2048]{2,1,0:T(8,128)(2,1)}), bf16[32,8,2048]{2,1,0:T(8,128)(2,1)S(1)}, u32[]{:S(2)}, u32[]{:S(2)}) async-start(bf16[32,8,2048]{2,1,0:T(8,128)(2,1)} %fusion.1), calls=%async_computation.5 | async-start | bytes 2097152 | tf_op jit(solution)/shard_map/all_to_all | solution.py:314
  61.9 35.0 %collective-permute-start = (bf16[2048,512]{1,0:T(8,128)(2,1)S(1)}, bf16[2048,512]{1,0:T(8,128)(2,1)}, u32[]{:S(2)}, u32[]{:S(2)}) collective-permute-start(bf16[2048,512]{1,0:T(8,128)(2,1)S(1)} %bitcast.74), channel_id=1, source_target_pairs={{0,3},{1,2},{2,1},{3,0},{4,5},{5,4},{6,7},{7,6},{8,11},{9,10},{10,... | collective-permute-start | bytes 6291464 | tf_op jit(solution)/shard_map/ppermute | solution.py:279
  63.2 59.9 %collective-permute-start.1 = (bf16[2048,512]{1,0:T(8,128)(2,1)}, bf16[2048,512]{1,0:T(8,128)(2,1)}, u32[]{:S(2)}, u32[]{:S(2)}) collective-permute-start(bf16[2048,512]{1,0:T(8,128)(2,1)} %bitcast.75), channel_id=1, source_target_pairs={{0,3},{1,2},{2,1},{3,0},{4,5},{5,4},{6,7},{7,6},{8,11},{9,10},{10,... | collective-permute-start | bytes 6291464 | tf_op jit(solution)/shard_map/ppermute | solution.py:279
  65.2 80.3 %collective-permute-start.2 = (bf16[512,2048]{1,0:T(8,128)(2,1)}, bf16[512,2048]{1,0:T(8,128)(2,1)}, u32[]{:S(2)}, u32[]{:S(2)}) collective-permute-start(bf16[512,2048]{1,0:T(8,128)(2,1)} %bitcast.80), channel_id=1, source_target_pairs={{0,3},{1,2},{2,1},{3,0},{4,5},{5,4},{6,7},{7,6},{8,11},{9,10},{10,... | collective-permute-start | bytes 6291464 | tf_op jit(solution)/shard_map/ppermute | solution.py:279
  90.6 63.4 %copy-start.2 = (bf16[32,8,2048]{2,1,0:T(8,128)(2,1)}, bf16[32,8,2048]{2,1,0:T(8,128)(2,1)S(1)}, u32[]{:S(2)}) copy-start(bf16[32,8,2048]{2,1,0:T(8,128)(2,1)S(1)} %all-to-all-done.5) | copy-start | bytes 3145732
  90.6 63.5 %all-to-all-start.3 = ((bf16[32,8,2048]{2,1,0:T(8,128)(2,1)}), bf16[32,8,2048]{2,1,0:T(8,128)(2,1)}, u32[]{:S(2)}, u32[]{:S(2)}) async-start(bf16[32,8,2048]{2,1,0:T(8,128)(2,1)} %fusion), calls=%async_computation.3 | async-start | bytes 2097152 | tf_op jit(solution)/shard_map/all_to_all | solution.py:314
  96.3 49.3 %collective-permute-start.7 = (bf16[256,2048]{1,0:T(8,128)(2,1)S(1)}, bf16[256,2048]{1,0:T(8,128)(2,1)}, u32[]{:S(2)}, u32[]{:S(2)}) collective-permute-start(bf16[256,2048]{1,0:T(8,128)(2,1)S(1)} %bitcast.85), channel_id=1, source_target_pairs={{0,1},{1,0},{2,3},{3,2},{4,7},{5,6},{6,5},{7,4},{8,9},{9,8},{10,11... | collective-permute-start | bytes 3145736 | tf_op jit(solution)/shard_map/ppermute | solution.py:317
  154.0 15.1 %collective-permute-start.8 = (bf16[256,2048]{1,0:T(8,128)(2,1)}, bf16[256,2048]{1,0:T(8,128)(2,1)S(1)}, u32[]{:S(2)}, u32[]{:S(2)}) collective-permute-start(bf16[256,2048]{1,0:T(8,128)(2,1)} %shard_map.143), channel_id=1, source_target_pairs={{0,1},{1,0},{2,3},{3,2},{4,7},{5,6},{6,5},{7,4},{8,9},{9,8},{10,11... | collective-permute-start | bytes 3145736 | tf_op jit(solution)/shard_map/ppermute | solution.py:322
  154.1 27.8 %collective-permute-start.3 = (bf16[256,2048]{1,0:T(8,128)(2,1)}, bf16[256,2048]{1,0:T(8,128)(2,1)S(1)}, u32[]{:S(2)}, u32[]{:S(2)}) collective-permute-start(bf16[256,2048]{1,0:T(8,128)(2,1)} %bitcast.13.x_ref), channel_id=1, source_target_pairs={{0,1},{1,0},{2,3},{3,2},{4,7},{5,6},{6,5},{7,4},{8,9},{9,8},{10,11... | collective-permute-start | bytes 3145736 | tf_op jit(solution)/shard_map/ppermute | solution.py:317
  172.0 37.3 %all-to-all-start.6 = ((bf16[32,8,2048]{2,1,0:T(8,128)(2,1)}), bf16[32,8,2048]{2,1,0:T(8,128)(2,1)S(1)}, u32[]{:S(2)}, u32[]{:S(2)}) async-start(bf16[32,8,2048]{2,1,0:T(8,128)(2,1)} %fusion.14), calls=%async_computation.6 | async-start | bytes 2097152 | tf_op jit(solution)/shard_map/all_to_all | solution.py:324
  181.9 1.0 copy-start.7
  191.3 15.1 %collective-permute-start.4 = (bf16[256,2048]{1,0:T(8,128)(2,1)}, bf16[256,2048]{1,0:T(8,128)(2,1)S(1)}, u32[]{:S(2)}, u32[]{:S(2)}) collective-permute-start(bf16[256,2048]{1,0:T(8,128)(2,1)} %shard_map.141), channel_id=1, source_target_pairs={{0,1},{1,0},{2,3},{3,2},{4,7},{5,6},{6,5},{7,4},{8,9},{9,8},{10,11... | collective-permute-start | bytes 3145736 | tf_op jit(solution)/shard_map/ppermute | solution.py:322
  209.4 35.1 %all-to-all-start.4 = ((bf16[32,8,2048]{2,1,0:T(8,128)(2,1)}), bf16[32,8,2048]{2,1,0:T(8,128)(2,1)S(1)}, u32[]{:S(2)}, u32[]{:S(2)}) async-start(bf16[32,8,2048]{2,1,0:T(8,128)(2,1)} %fusion.13), calls=%async_computation.4 | async-start | bytes 2097152 | tf_op jit(solution)/shard_map/all_to_all | solution.py:324
  219.1 25.4 %copy-start.4 = (f32[64,2048]{1,0:T(8,128)S(1)}, f32[64,2048]{1,0:T(8,128)}, u32[]{:S(2)}) copy-start(f32[64,2048]{1,0:T(8,128)} %copy-done.3) | copy-start | bytes 1572868
  220.6 23.9 %collective-permute-start.9 = (f32[64,2048]{1,0:T(8,128)}, f32[64,2048]{1,0:T(8,128)S(1)}, u32[]{:S(2)}, u32[]{:S(2)}) collective-permute-start(f32[64,2048]{1,0:T(8,128)} %fusion.9), channel_id=1, source_target_pairs={{0,4},{4,0},{1,5},{5,1},{2,6},{6,2},{3,7},{7,3},{8,12},{12,8},{9,1... | collective-permute-start | bytes 1572872 | tf_op jit(solution)/shard_map/ppermute | solution.py:328

commit v2 on v1

--- a/solution.py
+++ b/solution.py
@@ -84,7 +84,7 @@
     store_state(state_ref, state_t, end)
 
 
-def inner_kernel(q_ref, k_ref, v_ref, cum_ref, inner_ref, qdec_ref):
+def inner_kernel(cum_ref, q_ref, k_ref, v_ref, inner_ref, qdec_ref):
     rows = q_ref.shape[0]
     half = BLOCK // 2
     cum_all = cum_ref[...]
@@ -143,7 +143,7 @@
     logb_ref[...] = jnp.broadcast_to(log_before, logb_ref.shape)
 
 
-def finish_kernel(at_ref, all_ref, before_ref, logb_ref, inner_ref, qdec_ref, gate_ref, gain_ref, out_ref):
+def finish_kernel(at_ref, before_ref, logb_ref, inner_ref, qdec_ref, gate_ref, gain_ref, all_ref, out_ref):
     place = at_ref[0]
     state = jnp.zeros((DV, 2 * DK), F32)
     for k in range(all_ref.shape[0]):
@@ -164,21 +164,36 @@
             out_ref[j, :, cols] = mixed[j * quarter : (j + 1) * quarter]
 
 
-def call(kernel, outs, *args, flops=2**20):
+SMALL = 16 * 2**20
+
+
+def held(x):
+    return pltpu.with_memory_space_constraint(x, pltpu.VMEM)
+
+
+def call(kernel, outs, *args, kept=(), loads=(), scratch=(), flops=2**20, limit=None):
     specs = [
         pl.BlockSpec(memory_space=pltpu.SMEM if a.dtype == jnp.int32 else pltpu.VMEM) for a in args
     ]
+    specs += [pl.BlockSpec(memory_space=pltpu.VMEM)] * len(kept)
+    specs += [pl.BlockSpec(memory_space=pl.ANY)] * len(loads)
     return pl.pallas_call(
         kernel,
         out_shape=outs,
         in_specs=specs,
         out_specs=[pl.BlockSpec(memory_space=pltpu.VMEM)] * len(outs),
+        scratch_shapes=scratch,
         cost_estimate=pl.CostEstimate(flops=flops, bytes_accessed=2**19, transcendentals=2**16),
-    )(*args)
+        compiler_params=pltpu.CompilerParams(vmem_limit_bytes=limit),
+    )(*args, *(held(a) for a in kept), *loads)
 
 
 def shaped(shape, dtype):
     return jax.ShapeDtypeStruct(shape, dtype)
+
+
+def resident(shape, dtype):
+    return pltpu.VMEM(shape, dtype)
 
 
 def mixer(queries, key_rows, value_rows, out_gate, decay_logit, head_gain):
@@ -192,21 +207,21 @@
     )
     inner, qdec = call(
         inner_kernel,
-        [shaped((rows, 2 * DV), F32), shaped((rows, 2 * DK), BF16)],
-        queries, key_rows, value_rows, cum,
+        [resident((rows, 2 * DV), F32), resident((rows, 2 * DK), BF16)],
+        cum, queries, key_rows, value_rows,
     )
     in_plane = lax.all_to_all(state, PLANE, 0, 0, tiled=True)
     total, before, logb = call(
         plane_kernel,
         [shaped((planes, packed, 2 * DK), BF16), shaped((DV, 2 * DK), F32), shaped((8, 2 * DK), F32)],
-        lax.axis_index(PLANE)[None].astype(jnp.int32), in_plane,
+        lax.axis_index(PLANE)[None].astype(jnp.int32), kept=(in_plane,), limit=SMALL,
     )
     along = lax.all_to_all(total, "sp_0", 0, 0, tiled=True)
     (mixed,) = call(
         finish_kernel,
         [shaped((tps, rows // tps, 2 * DV), BF16)],
-        lax.axis_index("sp_0")[None].astype(jnp.int32), along, before, logb, inner, qdec, out_gate,
-        head_gain[None],
+        lax.axis_index("sp_0")[None].astype(jnp.int32), before, logb, inner, qdec, out_gate,
+        head_gain[None], kept=(along,), limit=SMALL,
     )
     return lax.all_to_all(mixed, "tp", 0, 0, tiled=True)
 
@@ -217,48 +232,72 @@
     return (up_cut + 1.0) * (gate_cut / (1.0 + jnp.exp(-SIGMOID_SLOPE * gate_cut)))
 
 
-def ffn_kernel(x_ref, g0, u0, d0, g1, u1, d1, out_ref, g_buf, u_buf, d_buf, sem):
-    copies = [
-        [
-            pltpu.make_async_copy(src, buf.at[half], sem.at[half, j])
-            for j, (src, buf) in enumerate(zip(srcs, (g_buf, u_buf, d_buf)))
-        ]
-        for half, srcs in enumerate(((g0, u0, d0), (g1, u1, d1)))
-    ]
-    for half in copies:
-        for copy in half:
+def ffn_kernel(x_ref, *refs):
+    sources, out_ref, bufs, sem = refs[:-8], refs[-8], refs[-7:-1], refs[-1]
+    copies, k = [], 0
+    for buf in bufs:
+        at, parts = 0, []
+        while at < buf.shape[0]:
+            rows = sources[k].shape[0]
+            parts.append(pltpu.make_async_copy(sources[k], buf.at[pl.ds(at, rows)], sem.at[k]))
+            at, k = at + rows, k + 1
+        copies.append(parts)
+    for parts in copies:
+        for copy in parts:
             copy.start()
+
+    def product(x, which):
+        for copy in copies[which]:
+            copy.wait()
+        return dot(x, bufs[which][...], ((1,), (0,)))
+
+    x = x_ref[...]
     total = None
-    for half, (gate_copy, up_copy, down_copy) in enumerate(copies):
-        gate_copy.wait()
-        gate_pre = dot(x_ref[...], g_buf[half], ((1,), (0,)))
-        up_copy.wait()
-        up_pre = dot(x_ref[...], u_buf[half], ((1,), (0,)))
-        hidden = clamped_unit(gate_pre, up_pre).astype(BF16)
-        down_copy.wait()
-        part = dot(hidden, d_buf[half], ((1,), (0,)))
+    for half in (0, 3):
+        gate_pre = product(x, half)
+        up_pre = product(x, half + 1)
+        part = product(clamped_unit(gate_pre, up_pre).astype(BF16), half + 2)
         total = part if total is None else total + part
     out_ref[...] = total.astype(out_ref.dtype)
 
 
-def ffn(x, own, other, dtype):
+def ffn(x, own, other, kind):
     rows, width = x.shape
-    units = own[0].shape[1]
-    return pl.pallas_call(
-        ffn_kernel,
-        out_shape=shaped((rows, width), dtype),
-        in_specs=[pl.BlockSpec(memory_space=pltpu.VMEM)] + [pl.BlockSpec(memory_space=pl.ANY)] * 6,
-        out_specs=pl.BlockSpec(memory_space=pltpu.VMEM),
-        scratch_shapes=[
-            pltpu.VMEM((2, width, units), BF16),
-            pltpu.VMEM((2, width, units), BF16),
-            pltpu.VMEM((2, units, width), BF16),
-            pltpu.SemaphoreType.DMA((2, 3)),
+    sources = (*own, *other)
+    (out,) = call(
+        ffn_kernel, [kind((rows, width), BF16)], x, loads=sources,
+        scratch=[
+            *(pltpu.VMEM(w.shape, w.dtype) for w in (*own, *own)),
+            pltpu.SemaphoreType.DMA((len(sources),)),
         ],
-        cost_estimate=pl.CostEstimate(
-            flops=12 * rows * width * units, bytes_accessed=12 * width * units, transcendentals=2 * rows * units
-        ),
-    )(x, *own, *other)
+        flops=12 * rows * width * own[0].shape[1],
+    )
+    return out
+
+
+def prepare_kernel(res_ref, gain_ref, rank_ref, piece_ref, w_ref, residual_ref, normed_ref, rows_ref, buf, sem):
+    count, _, wide = piece_ref.shape
+    copies = [
+        pltpu.make_async_copy(w_ref.at[pl.ds(j * wide, wide)], buf.at[j], sem.at[j]) for j in range(count)
+    ]
+    for copy in copies:
+        copy.start()
+    total = res_ref[...].astype(F32)
+    for j in range(count):
+        copies[j].wait()
+        total = total + dot(piece_ref[j], buf[j], ((1,), (0,)))
+    residual = total.astype(BF16)
+    residual_ref[...] = residual
+    values = residual.astype(F32)
+    scale = lax.rsqrt(jnp.mean(values * values, axis=1, keepdims=True) + NORM_EPS)
+    normed = (values * scale * gain_ref[...].astype(F32)).astype(BF16)
+    normed_ref[...] = normed
+    columns, cap, width = rows_ref.shape
+    rank = rank_ref[...]
+    slot = lax.broadcasted_iota(jnp.int32, (columns, cap, rank.shape[1]), 1).astype(F32)
+    send = jnp.where(rank[:, None, :] == slot, 1.0, 0.0).reshape(columns * cap, rank.shape[1])
+    rows = dot(send.astype(BF16), normed, ((1,), (0,))).astype(BF16)
+    rows_ref[...] = rows.reshape(columns, cap, width)
 
 
 def blend(rank, weight, cap):
@@ -274,8 +313,9 @@
 ):
     core_tp = ("sp_2", "tp")
     own = (w_gate[0], w_up[0], w_down[0])
+    middle = w_up.shape[1] // 2
     other = []
-    for w in own:
+    for w in (own[0], own[1][:middle], own[1][middle:], own[2]):
         other.append(lax.ppermute(w, core_tp, WEIGHT_PAIRS))
     experts, cores = lax.axis_size(SP), lax.axis_size("sp_2")
     columns = experts // cores
@@ -297,30 +337,39 @@
     theirs_plan = lax.ppermute(away, "sp_2", swap_cores)
     plans = (here, theirs_plan)
 
-    by_token = mixer(queries, key_rows, value_rows, out_gate, decay_logit, head_gain)
-    by_token = by_token.transpose(1, 0, 2).reshape(quarter, -1)
-    projected = jnp.dot(by_token, w_out, preferred_element_type=F32)
-    residual = (residual_in.astype(F32) + projected).astype(BF16)
-    values = residual.astype(F32)
-    scale = lax.rsqrt(jnp.mean(values * values, axis=-1, keepdims=True) + NORM_EPS)
-    normed = (values * scale * ffn_gain.astype(F32)).astype(BF16)
+    pieces = mixer(queries, key_rows, value_rows, out_gate, decay_logit, head_gain)
+    residual, normed, rows = call(
+        prepare_kernel,
+        [
+            shaped((quarter, width), BF16),
+            shaped((quarter, width), BF16),
+            shaped((columns, cap, width), BF16),
+        ],
+        residual_in, ffn_gain[None], here[0].T, kept=(pieces,), loads=(w_out,),
+        scratch=[
+            pltpu.VMEM((pieces.shape[0], pieces.shape[2], width), BF16),
+            pltpu.SemaphoreType.DMA((pieces.shape[0],)),
+        ],
+    )
     normed_other = lax.ppermute(normed, "sp_2", swap_cores)
 
     columns_axes = ("sp_0", "sp_1")
     arrived, swapped = [], []
-    for c, source in enumerate((normed, normed_other)):
-        send = (plans[c][0].T[:, None, :] == slots[None, :, None]).astype(BF16)
-        rows = jnp.dot(send.reshape(columns * cap, quarter), source, preferred_element_type=F32).astype(BF16)
-        rows = lax.all_to_all(rows.reshape(columns, cap, width), columns_axes, 0, 0, tiled=True)
+    for c in range(2):
+        if c:
+            send = (theirs_plan[0].T[:, None, :] == slots[None, :, None]).astype(BF16)
+            rows = jnp.dot(send.reshape(columns * cap, quarter), normed_other, preferred_element_type=F32)
+            rows = rows.astype(BF16).reshape(columns, cap, width)
+        rows = lax.all_to_all(rows, columns_axes, 0, 0, tiled=True)
         rows = rows.reshape(columns * cap, width)
         arrived.append(rows)
         swapped.append(lax.ppermute(rows, core_tp, ROW_PAIRS))
     sums = []
     for c in range(2):
-        mine = ffn(arrived[c], own, other, F32)
-        theirs = ffn(swapped[c], own, other, BF16)
+        theirs = ffn(swapped[c], own, other, shaped)
+        mine = ffn(arrived[c], own, other, resident)
         back = lax.ppermute(theirs, core_tp, ROW_PAIRS)
-        out = (mine + back.astype(F32)).astype(BF16)
+        out = (mine.astype(F32) + back.astype(F32)).astype(BF16)
         home = lax.all_to_all(out.reshape(columns, cap, width), columns_axes, 0, 0, tiled=True)
         home = home.reshape(columns * cap, width)
         lead, rest = blend(plans[c][0], plans[c][1], cap)

time: 247 us -> 244 us (0.988)
  matrix products: 8.84 us -> 4.18 us
  other arithmetic: 7.13 us -> 3.86 us
  starting transfers between devices: 55.6 us -> 58.5 us
    pallas_call x4 -> x0, Pallas kernels: 34.6 us -> none  [ffn(): pl.pallas_call(ffn_kernel, out_shape=shaped((rows, width), dtype), in_spe...]
    pallas_call x4 -> x9, Pallas kernels: 8.81 us -> 42.9 us  [call(): pl.pallas_call(kernel, out_shape=outs, in_specs=specs, out_specs=[pl.Bloc...]
    dot_general x3 -> x1, matrix products: 6.14 us -> 1.47 us  [on_device(): jnp.dot(send.reshape(columns * cap, quarter), normed_other, preferred_ele...]
    reshape x2, other arithmetic: 5.86 us -> 2.79 us  [on_device(): out.reshape(columns, cap, width)]
    ppermute x2, waiting for transfers between devices: 10.2 us -> 13 us  [on_device(): back = lax.ppermute(theirs, core_tp, ROW_PAIRS)]
    ppermute x3 -> x4, starting transfers between devices: 4.49 us -> 6.56 us  [on_device(): other.append(lax.ppermute(w, core_tp, WEIGHT_PAIRS))]
    ppermute x3 -> x4, waiting for transfers between devices: 48.6 us -> 48.7 us  [on_device(): other.append(lax.ppermute(w, core_tp, WEIGHT_PAIRS))]
  transfers between devices with their start and end apart: 17 -> 18, of which waited for: 10 -> 11; matrix products, arithmetic and copies ran while one was open for 6% -> 3% of each run, Pallas kernels for 15% -> 16%
where the time goes in v2:
time: 244 us; the launch traced here: 243 us
  waiting for transfers between devices  128 us (52%)
  starting transfers between devices  58.5 us (24%)
  Pallas kernels  42.9 us (18%)
  local copies, waits for them, and re-layouts  5.31 us (2%)
  matrix products  4.18 us (2%)
  other arithmetic  3.86 us (2%)
    ppermute x4, waiting for transfers between devices, on_device(): other.append(lax.ppermute(w, core_tp, WEIGHT_PAIRS))  48.7 us
    pallas_call x9, Pallas kernels, call(): pl.pallas_call(kernel, out_shape=outs, in_specs=specs, out_specs=[pl.Bloc...  42.9 us
    all_to_all x2, waiting for transfers between devices, on_device(): lax.all_to_all(out.reshape(columns, cap, width), columns_axes, 0, 0, tile...  24.8 us
    all_to_all x2, waiting for transfers between devices, on_device(): rows = lax.all_to_all(rows, columns_axes, 0, 0, tiled=True)  20.8 us
    all_to_all x2, starting transfers between devices, on_device(): lax.all_to_all(out.reshape(columns, cap, width), columns_axes, 0, 0, tile...  19.6 us
    ppermute x2, waiting for transfers between devices, on_device(): back = lax.ppermute(theirs, core_tp, ROW_PAIRS)  13 us
    all_to_all x2, starting transfers between devices, on_device(): rows = lax.all_to_all(rows, columns_axes, 0, 0, tiled=True)  11.3 us
    all_to_all x1, waiting for transfers between devices, mixer(): along = lax.all_to_all(total, 'sp_0', 0, 0, tiled=True)  9.32 us
  transfers between devices with their start and end apart: 18, of which 11 were waited for; matrix products, arithmetic and copies ran while one was open for 3% of the time, Pallas kernels for 16%

profile of v2, /device:TPU:2, one launch (start us, length us, event | category | flops | bytes accessed | tf_op | source)
XLA Modules:
  0.0 243.4 jit_solution(9408439175860868294)
XLA Ops:
  0.0 2.3 shard_map.136
  2.4 5.6 %all-to-all-start = ((bf16[8,136,128]{2,1,0:T(8,128)(2,1)}), bf16[8,136,128]{2,1,0:T(8,128)(2,1)S(1)}, u32[]{:S(2)}, u32[]{:S(2)}) async-start(bf16[8,136,128]{2,1,0:T(8,128)(2,1)} %get-tuple-element.15), calls=%async_computation | async-start | bytes 557056 | tf_op jit(solution)/shard_map/all_to_all | solution.py:213
  9.3 4.9 %all-to-all-done.all_ref = bf16[8,136,128]{2,1,0:T(8,128)(2,1)S(1)} async-done(((bf16[8,136,128]{2,1,0:T(8,128)(2,1)}), bf16[8,136,128]{2,1,0:T(8,128)(2,1)S(1)}, u32[]{:S(2)}, u32[]{:S(2)}) %all-to-all-start) | async-done | bytes 278560 | tf_op jit(solution)/shard_map/all_to_all | solution.py:213
  15.0 7.7 %all-to-all-start.1 = ((bf16[8,136,128]{2,1,0:T(8,128)(2,1)}), bf16[8,136,128]{2,1,0:T(8,128)(2,1)S(1)}, u32[]{:S(2)}, u32[]{:S(2)}) async-start(bf16[8,136,128]{2,1,0:T(8,128)(2,1)} %get-tuple-element.21), calls=%async_computation.1 | async-start | bytes 557056 | tf_op jit(solution)/shard_map/all_to_all | solution.py:219
  23.4 1.8 shard_map.138
  25.2 9.3 %all-to-all-done.1.all_ref = bf16[8,136,128]{2,1,0:T(8,128)(2,1)S(1)} async-done(((bf16[8,136,128]{2,1,0:T(8,128)(2,1)}), bf16[8,136,128]{2,1,0:T(8,128)(2,1)S(1)}, u32[]{:S(2)}, u32[]{:S(2)}) %all-to-all-start.1) | async-done | bytes 278560 | tf_op jit(solution)/shard_map/all_to_all | solution.py:219
  35.6 4.5 %all-to-all-start.2 = ((bf16[4,64,256]{2,1,0:T(8,128)(2,1)}), bf16[4,64,256]{2,1,0:T(8,128)(2,1)S(1)}, u32[]{:S(2)}, u32[]{:S(2)}) async-start(bf16[4,64,256]{2,1,0:T(8,128)(2,1)} %shard_map.139), calls=%async_computation.2 | async-start | bytes 262144 | tf_op jit(solution)/shard_map/all_to_all | solution.py:226
  40.6 5.4 %all-to-all-done.2.piece_ref = bf16[4,64,256]{2,1,0:T(8,128)(2,1)S(1)} async-done(((bf16[4,64,256]{2,1,0:T(8,128)(2,1)}), bf16[4,64,256]{2,1,0:T(8,128)(2,1)S(1)}, u32[]{:S(2)}, u32[]{:S(2)}) %all-to-all-start.2) | async-done | bytes 131104 | tf_op jit(solution)/shard_map/all_to_all | solution.py:226
  46.0 5.0 %shard_map.140 = (bf16[64,2048]{1,0:T(8,128)(2,1)}, bf16[64,2048]{1,0:T(8,128)(2,1)}, bf16[32,8,2048]{2,1,0:T(8,128)(2,1)}) custom-call(bf16[64,2048]{1,0:T(8,128)(2,1)} %res_ref.1, bf16[1,2048]{1,0:T(2,128)(2,1)} %broadcast_in_dim.68.gain_ref, f32[32,64]{1,0:T(8,128)} %get-tuple-element.28.rank_ref, bf16[4,64,256]{2,1,0:T(8,128)(2,1)S(1)} %all-to-all-done.2.piece_ref, ...), custom_call_target="tpu_custom_call" | custom-call | flops 1048576 | bytes 524288 | tf_op jit(solution)/shard_map/pallas_call | solution.py:180
  51.3 1.6 collective-permute-done.7
  52.9 1.5 fusion
  54.4 5.7 %all-to-all-start.5 = ((bf16[32,8,2048]{2,1,0:T(8,128)(2,1)}), bf16[32,8,2048]{2,1,0:T(8,128)(2,1)}, u32[]{:S(2)}, u32[]{:S(2)}) async-start(bf16[32,8,2048]{2,1,0:T(8,128)(2,1)} %fusion), calls=%async_computation.5 | async-start | bytes 2097152 | tf_op jit(solution)/shard_map/all_to_all | solution.py:363
  61.3 2.1 collective-permute-start.3
  63.4 1.5 slice_bitcast_fusion
  66.0 2.1 collective-permute-start.2
  68.1 20.8 %all-to-all-done.5 = bf16[32,8,2048]{2,1,0:T(8,128)(2,1)} async-done(((bf16[32,8,2048]{2,1,0:T(8,128)(2,1)}), bf16[32,8,2048]{2,1,0:T(8,128)(2,1)}, u32[]{:S(2)}, u32[]{:S(2)}) %all-to-all-start.5) | async-done | bytes 1048608 | tf_op jit(solution)/shard_map/all_to_all | solution.py:363
  88.9 5.6 %all-to-all-start.3 = ((bf16[32,8,2048]{2,1,0:T(8,128)(2,1)}), bf16[32,8,2048]{2,1,0:T(8,128)(2,1)}, u32[]{:S(2)}, u32[]{:S(2)}) async-start(bf16[32,8,2048]{2,1,0:T(8,128)(2,1)} %get-tuple-element.23), calls=%async_computation.3 | async-start | bytes 2097152 | tf_op jit(solution)/shard_map/all_to_all | solution.py:363
  95.2 37.4 %collective-permute-done.1.refs_4_ = bf16[1024,512]{1,0:T(8,128)(2,1)S(1)} collective-permute-done((bf16[1024,512]{1,0:T(8,128)(2,1)}, bf16[1024,512]{1,0:T(8,128)(2,1)S(1)}, u32[]{:S(2)}, u32[]{:S(2)}) %collective-permute-start.1) | collective-permute-done | bytes 1048608 | tf_op jit(solution)/shard_map/ppermute | solution.py:319
  132.6 11.2 %collective-permute-done.2.refs_5_ = bf16[1024,512]{1,0:T(8,128)(2,1)S(1)} collective-permute-done((bf16[1024,512]{1,0:T(8,128)(2,1)}, bf16[1024,512]{1,0:T(8,128)(2,1)S(1)}, u32[]{:S(2)}, u32[]{:S(2)}) %collective-permute-start.2) | collective-permute-done | bytes 1048608 | tf_op jit(solution)/shard_map/ppermute | solution.py:319
  145.1 8.5 %shard_map.144 = bf16[256,2048]{1,0:T(8,128)(2,1)} custom-call(bf16[256,2048]{1,0:T(8,128)(2,1)} %copy-done.6, bf16[2048,512]{1,0:T(8,128)(2,1)} %bitcast.73, bf16[2048,512]{1,0:T(8,128)(2,1)} %bitcast.68, bf16[512,2048]{1,0:T(8,128)(2,1)} %bitcast.78, bf16[2048,512]{1,0:T(8,128)(2,1)} %collective-permute-done.refs_3_, bf16[1024,512]{1,0:T(8,128)(2,1)} %copy-done.4, ...), custom_call_target="tpu_custom_call" | custom-call | flops 3221225472 | bytes 524288 | tf_op jit(solution)/shard_map/pallas_call | solution.py:180
  153.9 2.0 collective-permute-start.4
  155.9 7.5 %shard_map.143 = bf16[256,2048]{1,0:T(8,128)(2,1)S(1)} custom-call(bf16[256,2048]{1,0:T(8,128)(2,1)} %bitcast.26.x_ref, bf16[2048,512]{1,0:T(8,128)(2,1)} %bitcast.74, bf16[2048,512]{1,0:T(8,128)(2,1)} %bitcast.69, bf16[512,2048]{1,0:T(8,128)(2,1)} %bitcast.79, bf16[2048,512]{1,0:T(8,128)(2,1)} %collective-permute-done.refs_3_, bf16[1024,512]{1,0:T(8,128)(2,1)} %copy-done.4, ...), custom_call_target="tpu_custom_call" | custom-call | flops 3221225472 | bytes 524288 | tf_op jit(solution)/shard_map/pallas_call | solution.py:180
  163.4 5.5 %collective-permute-done.9 = bf16[256,2048]{1,0:T(8,128)(2,1)S(1)} collective-permute-done((bf16[256,2048]{1,0:T(8,128)(2,1)}, bf16[256,2048]{1,0:T(8,128)(2,1)S(1)}, u32[]{:S(2)}, u32[]{:S(2)}) %collective-permute-start.9) | collective-permute-done | bytes 1048608 | tf_op jit(solution)/shard_map/ppermute | solution.py:371
  168.9 1.4 fusion.11
  170.3 9.9 %all-to-all-start.6 = ((bf16[32,8,2048]{2,1,0:T(8,128)(2,1)}), bf16[32,8,2048]{2,1,0:T(8,128)(2,1)S(1)}, u32[]{:S(2)}, u32[]{:S(2)}) async-start(bf16[32,8,2048]{2,1,0:T(8,128)(2,1)} %fusion.11), calls=%async_computation.6 | async-start | bytes 2097152 | tf_op jit(solution)/shard_map/all_to_all | solution.py:373
  181.2 8.6 %shard_map.142 = bf16[256,2048]{1,0:T(8,128)(2,1)} custom-call(bf16[256,2048]{1,0:T(8,128)(2,1)} %copy-done.7, bf16[2048,512]{1,0:T(8,128)(2,1)} %bitcast.75, bf16[2048,512]{1,0:T(8,128)(2,1)} %bitcast.70, bf16[512,2048]{1,0:T(8,128)(2,1)} %bitcast.80, bf16[2048,512]{1,0:T(8,128)(2,1)} %collective-permute-done.refs_3_, bf16[1024,512]{1,0:T(8,128)(2,1)} %copy-done.4, ...), custom_call_target="tpu_custom_call" | custom-call | flops 3221225472 | bytes 524288 | tf_op jit(solution)/shard_map/pallas_call | solution.py:180
  189.9 7.5 %shard_map.141 = bf16[256,2048]{1,0:T(8,128)(2,1)S(1)} custom-call(bf16[256,2048]{1,0:T(8,128)(2,1)} %bitcast.10.x_ref, bf16[2048,512]{1,0:T(8,128)(2,1)} %bitcast.76, bf16[2048,512]{1,0:T(8,128)(2,1)} %bitcast.71, bf16[512,2048]{1,0:T(8,128)(2,1)} %bitcast.81, bf16[2048,512]{1,0:T(8,128)(2,1)} %collective-permute-done.refs_3_, bf16[1024,512]{1,0:T(8,128)(2,1)} %copy-done.4, ...), custom_call_target="tpu_custom_call" | custom-call | flops 3221225472 | bytes 524288 | tf_op jit(solution)/shard_map/pallas_call | solution.py:180
  197.4 7.5 %collective-permute-done.5 = bf16[256,2048]{1,0:T(8,128)(2,1)S(1)} collective-permute-done((bf16[256,2048]{1,0:T(8,128)(2,1)}, bf16[256,2048]{1,0:T(8,128)(2,1)S(1)}, u32[]{:S(2)}, u32[]{:S(2)}) %collective-permute-start.5) | collective-permute-done | bytes 1048608 | tf_op jit(solution)/shard_map/ppermute | solution.py:371
  204.9 1.4 fusion.10
  206.3 9.7 %all-to-all-start.4 = ((bf16[32,8,2048]{2,1,0:T(8,128)(2,1)}), bf16[32,8,2048]{2,1,0:T(8,128)(2,1)S(1)}, u32[]{:S(2)}, u32[]{:S(2)}) async-start(bf16[32,8,2048]{2,1,0:T(8,128)(2,1)} %fusion.10), calls=%async_computation.4 | async-start | bytes 2097152 | tf_op jit(solution)/shard_map/all_to_all | solution.py:373
  216.2 1.3 fusion.6
  217.5 24.7 %all-to-all-done.4 = bf16[32,8,2048]{2,1,0:T(8,128)(2,1)S(1)} async-done(((bf16[32,8,2048]{2,1,0:T(8,128)(2,1)}), bf16[32,8,2048]{2,1,0:T(8,128)(2,1)S(1)}, u32[]{:S(2)}, u32[]{:S(2)}) %all-to-all-start.4) | async-done | bytes 1048608 | tf_op jit(solution)/shard_map/all_to_all | solution.py:373
  (56 shorter events, 11.8 us)
Async XLA Ops:
  0.0 7.9 %copy-start = (s32[256,4]{0,1:T(4,128)S(1)}, s32[256,4]{0,1:T(4,128)}, u32[]{:S(2)}) copy-start(s32[256,4]{0,1:T(4,128)} %param.23) | copy-start | bytes 12292
  0.0 22.8 %copy-start.8 = (bf16[2048]{0:T(1024)(128)(2,1)S(1)}, bf16[2048]{0:T(1024)(128)(2,1)}, u32[]{:S(2)}) copy-start(bf16[2048]{0:T(1024)(128)(2,1)} %param.22) | copy-start | bytes 12292
  0.0 34.5 %copy-start.2 = (bf16[128]{0:T(256)(128)(2,1)S(1)}, bf16[128]{0:T(256)(128)(2,1)}, u32[]{:S(2)}) copy-start(bf16[128]{0:T(256)(128)(2,1)} %param.20) | copy-start | bytes 772
  0.0 34.5 %copy-start.1 = (bf16[256,256]{1,0:T(8,128)(2,1)S(1)}, bf16[256,256]{1,0:T(8,128)(2,1)}, u32[]{:S(2)}) copy-start(bf16[256,256]{1,0:T(8,128)(2,1)} %gate_ref.1) | copy-start | bytes 393220
  2.4 11.8 %all-to-all-start = ((bf16[8,136,128]{2,1,0:T(8,128)(2,1)}), bf16[8,136,128]{2,1,0:T(8,128)(2,1)S(1)}, u32[]{:S(2)}, u32[]{:S(2)}) async-start(bf16[8,136,128]{2,1,0:T(8,128)(2,1)} %get-tuple-element.15), calls=%async_computation | async-start | bytes 557056 | tf_op jit(solution)/shard_map/all_to_all | solution.py:213
  15.0 19.5 %all-to-all-start.1 = ((bf16[8,136,128]{2,1,0:T(8,128)(2,1)}), bf16[8,136,128]{2,1,0:T(8,128)(2,1)S(1)}, u32[]{:S(2)}, u32[]{:S(2)}) async-start(bf16[8,136,128]{2,1,0:T(8,128)(2,1)} %get-tuple-element.21), calls=%async_computation.1 | async-start | bytes 557056 | tf_op jit(solution)/shard_map/all_to_all | solution.py:219
  22.7 28.5 %collective-permute-start.6 = (f32[2,64,32]{1,2,0:T(8,128)S(1)}, f32[2,64,32]{1,2,0:T(8,128)S(1)}, u32[]{:S(2)}, u32[]{:S(2)}) collective-permute-start(f32[2,64,32]{1,2,0:T(8,128)S(1)} %dynamic-slice_bitcast_fusion), channel_id=1, source_target_pairs={{0,4},{4,0},{1,5},{5,1},{2,6},{6,2},{3,7},{7,3},{8,12},{12,8},{9,1... | collective-permute-start | bytes 49160 | tf_op jit(solution)/shard_map/ppermute | solution.py:337
  35.6 10.4 %all-to-all-start.2 = ((bf16[4,64,256]{2,1,0:T(8,128)(2,1)}), bf16[4,64,256]{2,1,0:T(8,128)(2,1)S(1)}, u32[]{:S(2)}, u32[]{:S(2)}) async-start(bf16[4,64,256]{2,1,0:T(8,128)(2,1)} %shard_map.139), calls=%async_computation.2 | async-start | bytes 262144 | tf_op jit(solution)/shard_map/all_to_all | solution.py:226
  51.0 12.4 %copy-start.3 = (bf16[1,2048,512]{2,1,0:T(8,128)(2,1)S(1)}, bf16[1,2048,512]{2,1,0:T(8,128)(2,1)}, u32[]{:S(2)}) copy-start(bf16[1,2048,512]{2,1,0:T(8,128)(2,1)} %param.26) | copy-start | bytes 6291460
  51.1 1.8 collective-permute-start.7
  54.4 34.5 %all-to-all-start.5 = ((bf16[32,8,2048]{2,1,0:T(8,128)(2,1)}), bf16[32,8,2048]{2,1,0:T(8,128)(2,1)}, u32[]{:S(2)}, u32[]{:S(2)}) async-start(bf16[32,8,2048]{2,1,0:T(8,128)(2,1)} %fusion), calls=%async_computation.5 | async-start | bytes 2097152 | tf_op jit(solution)/shard_map/all_to_all | solution.py:363
  60.1 83.7 %collective-permute-start = (bf16[2048,512]{1,0:T(8,128)(2,1)}, bf16[2048,512]{1,0:T(8,128)(2,1)}, u32[]{:S(2)}, u32[]{:S(2)}) collective-permute-start(bf16[2048,512]{1,0:T(8,128)(2,1)} %bitcast.72), channel_id=1, source_target_pairs={{0,3},{1,2},{2,1},{3,0},{4,5},{5,4},{6,7},{7,6},{8,11},{9,10},{10,... | collective-permute-start | bytes 6291464 | tf_op jit(solution)/shard_map/ppermute | solution.py:319
  61.3 82.5 %collective-permute-start.3 = (bf16[512,2048]{1,0:T(8,128)(2,1)}, bf16[512,2048]{1,0:T(8,128)(2,1)}, u32[]{:S(2)}, u32[]{:S(2)}) collective-permute-start(bf16[512,2048]{1,0:T(8,128)(2,1)} %bitcast.77), channel_id=1, source_target_pairs={{0,3},{1,2},{2,1},{3,0},{4,5},{5,4},{6,7},{7,6},{8,11},{9,10},{10,... | collective-permute-start | bytes 6291464 | tf_op jit(solution)/shard_map/ppermute | solution.py:319
  64.9 67.7 %collective-permute-start.1 = (bf16[1024,512]{1,0:T(8,128)(2,1)}, bf16[1024,512]{1,0:T(8,128)(2,1)S(1)}, u32[]{:S(2)}, u32[]{:S(2)}) collective-permute-start(bf16[1024,512]{1,0:T(8,128)(2,1)} %get-tuple-element.26), channel_id=1, source_target_pairs={{0,3},{1,2},{2,1},{3,0},{4,5},{5,4},{6,7},{7,6},{8,11},{9,10},{10,... | collective-permute-start | bytes 3145736 | tf_op jit(solution)/shard_map/ppermute | solution.py:319
  66.0 77.8 %collective-permute-start.2 = (bf16[1024,512]{1,0:T(8,128)(2,1)}, bf16[1024,512]{1,0:T(8,128)(2,1)S(1)}, u32[]{:S(2)}, u32[]{:S(2)}) collective-permute-start(bf16[1024,512]{1,0:T(8,128)(2,1)} %get-tuple-element.25), channel_id=1, source_target_pairs={{0,3},{1,2},{2,1},{3,0},{4,5},{5,4},{6,7},{7,6},{8,11},{9,10},{10,... | collective-permute-start | bytes 3145736 | tf_op jit(solution)/shard_map/ppermute | solution.py:319
  88.9 65.0 %all-to-all-start.3 = ((bf16[32,8,2048]{2,1,0:T(8,128)(2,1)}), bf16[32,8,2048]{2,1,0:T(8,128)(2,1)}, u32[]{:S(2)}, u32[]{:S(2)}) async-start(bf16[32,8,2048]{2,1,0:T(8,128)(2,1)} %get-tuple-element.23), calls=%async_computation.3 | async-start | bytes 2097152 | tf_op jit(solution)/shard_map/all_to_all | solution.py:363
  94.5 49.3 %collective-permute-start.8 = (bf16[256,2048]{1,0:T(8,128)(2,1)}, bf16[256,2048]{1,0:T(8,128)(2,1)S(1)}, u32[]{:S(2)}, u32[]{:S(2)}) collective-permute-start(bf16[256,2048]{1,0:T(8,128)(2,1)} %bitcast.26.x_ref), channel_id=1, source_target_pairs={{0,1},{1,0},{2,3},{3,2},{4,7},{5,6},{6,5},{7,4},{8,9},{9,8},{10,11... | collective-permute-start | bytes 3145736 | tf_op jit(solution)/shard_map/ppermute | solution.py:366
  132.6 11.3 %copy-start.4 = (bf16[1024,512]{1,0:T(8,128)(2,1)}, bf16[1024,512]{1,0:T(8,128)(2,1)S(1)}, u32[]{:S(2)}) copy-start(bf16[1024,512]{1,0:T(8,128)(2,1)S(1)} %collective-permute-done.1.refs_4_) | copy-start | bytes 3145732
  143.8 1.0 copy-start.5
  143.8 1.3 copy-start.6
  153.6 15.3 %collective-permute-start.9 = (bf16[256,2048]{1,0:T(8,128)(2,1)}, bf16[256,2048]{1,0:T(8,128)(2,1)S(1)}, u32[]{:S(2)}, u32[]{:S(2)}) collective-permute-start(bf16[256,2048]{1,0:T(8,128)(2,1)} %shard_map.144), channel_id=1, source_target_pairs={{0,1},{1,0},{2,3},{3,2},{4,7},{5,6},{6,5},{7,4},{8,9},{9,8},{10,11... | collective-permute-start | bytes 3145736 | tf_op jit(solution)/shard_map/ppermute | solution.py:371
  153.9 26.3 %collective-permute-start.4 = (bf16[256,2048]{1,0:T(8,128)(2,1)}, bf16[256,2048]{1,0:T(8,128)(2,1)S(1)}, u32[]{:S(2)}, u32[]{:S(2)}) collective-permute-start(bf16[256,2048]{1,0:T(8,128)(2,1)} %bitcast.10.x_ref), channel_id=1, source_target_pairs={{0,1},{1,0},{2,3},{3,2},{4,7},{5,6},{6,5},{7,4},{8,9},{9,8},{10,11... | collective-permute-start | bytes 3145736 | tf_op jit(solution)/shard_map/ppermute | solution.py:366
  170.3 36.0 %all-to-all-start.6 = ((bf16[32,8,2048]{2,1,0:T(8,128)(2,1)}), bf16[32,8,2048]{2,1,0:T(8,128)(2,1)S(1)}, u32[]{:S(2)}, u32[]{:S(2)}) async-start(bf16[32,8,2048]{2,1,0:T(8,128)(2,1)} %fusion.11), calls=%async_computation.6 | async-start | bytes 2097152 | tf_op jit(solution)/shard_map/all_to_all | solution.py:373
  180.2 1.0 copy-start.7
  189.8 15.1 %collective-permute-start.5 = (bf16[256,2048]{1,0:T(8,128)(2,1)}, bf16[256,2048]{1,0:T(8,128)(2,1)S(1)}, u32[]{:S(2)}, u32[]{:S(2)}) collective-permute-start(bf16[256,2048]{1,0:T(8,128)(2,1)} %shard_map.142), channel_id=1, source_target_pairs={{0,1},{1,0},{2,3},{3,2},{4,7},{5,6},{6,5},{7,4},{8,9},{9,8},{10,11... | collective-permute-start | bytes 3145736 | tf_op jit(solution)/shard_map/ppermute | solution.py:371
  206.3 35.9 %all-to-all-start.4 = ((bf16[32,8,2048]{2,1,0:T(8,128)(2,1)}), bf16[32,8,2048]{2,1,0:T(8,128)(2,1)S(1)}, u32[]{:S(2)}, u32[]{:S(2)}) async-start(bf16[32,8,2048]{2,1,0:T(8,128)(2,1)} %fusion.10), calls=%async_computation.4 | async-start | bytes 2097152 | tf_op jit(solution)/shard_map/all_to_all | solution.py:373
  216.0 26.2 %copy-start.9 = (bf16[64,2048]{1,0:T(8,128)(2,1)S(1)}, bf16[64,2048]{1,0:T(8,128)(2,1)}, u32[]{:S(2)}) copy-start(bf16[64,2048]{1,0:T(8,128)(2,1)} %get-tuple-element.22) | copy-start | bytes 786436
  217.5 24.7 %collective-permute-start.10 = (f32[64,2048]{1,0:T(8,128)}, f32[64,2048]{1,0:T(8,128)S(1)}, u32[]{:S(2)}, u32[]{:S(2)}) collective-permute-start(f32[64,2048]{1,0:T(8,128)} %fusion.6), channel_id=1, source_target_pairs={{0,4},{4,0},{1,5},{5,1},{2,6},{6,2},{3,7},{7,3},{8,12},{12,8},{9,1... | collective-permute-start | bytes 1572872 | tf_op jit(solution)/shard_map/ppermute | solution.py:377

commit v3 on v2

--- a/solution.py
+++ b/solution.py
@@ -185,7 +185,7 @@
         scratch_shapes=scratch,
         cost_estimate=pl.CostEstimate(flops=flops, bytes_accessed=2**19, transcendentals=2**16),
         compiler_params=pltpu.CompilerParams(vmem_limit_bytes=limit),
-    )(*args, *(held(a) for a in kept), *loads)
+    )(*args, *(held(a) for a in kept), *(pltpu.with_memory_space_constraint(a, pltpu.HBM) for a in loads))
 
 
 def shaped(shape, dtype):
@@ -232,45 +232,40 @@
     return (up_cut + 1.0) * (gate_cut / (1.0 + jnp.exp(-SIGMOID_SLOPE * gate_cut)))
 
 
-def ffn_kernel(x_ref, *refs):
-    sources, out_ref, bufs, sem = refs[:-8], refs[-8], refs[-7:-1], refs[-1]
-    copies, k = [], 0
-    for buf in bufs:
-        at, parts = 0, []
-        while at < buf.shape[0]:
-            rows = sources[k].shape[0]
-            parts.append(pltpu.make_async_copy(sources[k], buf.at[pl.ds(at, rows)], sem.at[k]))
-            at, k = at + rows, k + 1
-        copies.append(parts)
-    for parts in copies:
-        for copy in parts:
-            copy.start()
-
-    def product(x, which):
-        for copy in copies[which]:
-            copy.wait()
-        return dot(x, bufs[which][...], ((1,), (0,)))
-
+def load_kernel(*refs):
+    count = len(refs) // 2
+    sources, targets, sem = refs[:count], refs[count:-1], refs[-1]
+    copies = [pltpu.make_async_copy(a, b, sem.at[k]) for k, (a, b) in enumerate(zip(sources, targets))]
+    for copy in copies:
+        copy.start()
+    for copy in copies:
+        copy.wait()
+
+
+def load(arrays):
+    return call(
+        load_kernel, [resident(a.shape, a.dtype) for a in arrays], loads=arrays,
+        scratch=[pltpu.SemaphoreType.DMA((len(arrays),))], limit=SMALL,
+    )
+
+
+def expert_part(x, gate_cols, up_cols, down_rows):
+    gate_pre = dot(x, gate_cols[...], ((1,), (0,)))
+    up_pre = dot(x, up_cols[...], ((1,), (0,)))
+    hidden = clamped_unit(gate_pre, up_pre).astype(BF16)
+    return dot(hidden, down_rows[...], ((1,), (0,)))
+
+
+def ffn_kernel(x_ref, g0, u0, d0, g1, u1, d1, out_ref):
     x = x_ref[...]
-    total = None
-    for half in (0, 3):
-        gate_pre = product(x, half)
-        up_pre = product(x, half + 1)
-        part = product(clamped_unit(gate_pre, up_pre).astype(BF16), half + 2)
-        total = part if total is None else total + part
-    out_ref[...] = total.astype(out_ref.dtype)
-
-
-def ffn(x, own, other, kind):
+    out_ref[...] = (expert_part(x, g0, u0, d0) + expert_part(x, g1, u1, d1)).astype(out_ref.dtype)
+
+
+def ffn(x, weights, kind):
     rows, width = x.shape
-    sources = (*own, *other)
     (out,) = call(
-        ffn_kernel, [kind((rows, width), BF16)], x, loads=sources,
-        scratch=[
-            *(pltpu.VMEM(w.shape, w.dtype) for w in (*own, *own)),
-            pltpu.SemaphoreType.DMA((len(sources),)),
-        ],
-        flops=12 * rows * width * own[0].shape[1],
+        ffn_kernel, [kind((rows, width), BF16)], kept=(x, *weights), limit=SMALL,
+        flops=12 * rows * width * weights[0].shape[1],
     )
     return out
 
@@ -313,9 +308,8 @@
 ):
     core_tp = ("sp_2", "tp")
     own = (w_gate[0], w_up[0], w_down[0])
-    middle = w_up.shape[1] // 2
     other = []
-    for w in (own[0], own[1][:middle], own[1][middle:], own[2]):
+    for w in own:
         other.append(lax.ppermute(w, core_tp, WEIGHT_PAIRS))
     experts, cores = lax.axis_size(SP), lax.axis_size("sp_2")
     columns = experts // cores
@@ -366,8 +360,9 @@
         swapped.append(lax.ppermute(rows, core_tp, ROW_PAIRS))
     sums = []
     for c in range(2):
-        theirs = ffn(swapped[c], own, other, shaped)
-        mine = ffn(arrived[c], own, other, resident)
+        weights = load((*own, *other))
+        theirs = ffn(swapped[c], weights, shaped)
+        mine = ffn(arrived[c], weights, resident)
         back = lax.ppermute(theirs, core_tp, ROW_PAIRS)
         out = (mine.astype(F32) + back.astype(F32)).astype(BF16)
         home = lax.all_to_all(out.reshape(columns, cap, width), columns_axes, 0, 0, tiled=True)

time: 244 us -> 249 us (1.020)
  local copies, waits for them, and re-layouts: 5.31 us -> 17.5 us
  Pallas kernels: 42.9 us -> 35.6 us
  starting transfers between devices: 58.5 us -> 55.6 us
    unnamed x21 -> x43, local copies, waits for them, and re-layouts: 2.31 us -> 16 us
    pallas_call x9 -> x10, Pallas kernels: 42.9 us -> 35.6 us  [call(): pl.pallas_call(kernel, out_shape=outs, in_specs=specs, out_specs=[pl.Bloc...]
    all_to_all x2, waiting for transfers between devices: 20.8 us -> 24.2 us  [on_device(): rows = lax.all_to_all(rows, columns_axes, 0, 0, tiled=True)]
    ppermute x4 -> x3, starting transfers between devices: 6.56 us -> 4.49 us  [on_device(): other.append(lax.ppermute(w, core_tp, WEIGHT_PAIRS))]
    ppermute x4 -> x3, waiting for transfers between devices: 48.7 us -> 48.7 us  [on_device(): other.append(lax.ppermute(w, core_tp, WEIGHT_PAIRS))]
  transfers between devices with their start and end apart: 18 -> 17, of which waited for: 11 -> 10; matrix products, arithmetic and copies ran while one was open for 3% -> 3% of each run, Pallas kernels for 16% -> 13%
where the time goes in v3:
time: 249 us; the launch traced here: 247 us
  waiting for transfers between devices  130 us (52%)
  starting transfers between devices  55.6 us (22%)
  Pallas kernels  35.6 us (14%)
  local copies, waits for them, and re-layouts  17.5 us (7%)
  other arithmetic  5 us (2%)
  matrix products  3.35 us (1%)
    ppermute x3, waiting for transfers between devices, on_device(): other.append(lax.ppermute(w, core_tp, WEIGHT_PAIRS))  48.7 us
    pallas_call x10, Pallas kernels, call(): pl.pallas_call(kernel, out_shape=outs, in_specs=specs, out_specs=[pl.Bloc...  35.6 us
    all_to_all x2, waiting for transfers between devices, on_device(): lax.all_to_all(out.reshape(columns, cap, width), columns_axes, 0, 0, tile...  24.5 us
    all_to_all x2, waiting for transfers between devices, on_device(): rows = lax.all_to_all(rows, columns_axes, 0, 0, tiled=True)  24.2 us
    all_to_all x2, starting transfers between devices, on_device(): lax.all_to_all(out.reshape(columns, cap, width), columns_axes, 0, 0, tile...  19.7 us
    unnamed x43, local copies, waits for them, and re-layouts  16 us
    ppermute x2, waiting for transfers between devices, on_device(): back = lax.ppermute(theirs, core_tp, ROW_PAIRS)  11.5 us
    all_to_all x2, starting transfers between devices, on_device(): rows = lax.all_to_all(rows, columns_axes, 0, 0, tiled=True)  10.7 us
  transfers between devices with their start and end apart: 17, of which 10 were waited for; matrix products, arithmetic and copies ran while one was open for 3% of the time, Pallas kernels for 13%

profile of v3, /device:TPU:2, one launch (start us, length us, event | category | flops | bytes accessed | tf_op | source)
XLA Modules:
  0.0 247.5 jit_solution(5929695652842795788)
XLA Ops:
  0.0 2.4 shard_map.136
  2.4 5.6 %all-to-all-start = ((bf16[8,136,128]{2,1,0:T(8,128)(2,1)}), bf16[8,136,128]{2,1,0:T(8,128)(2,1)S(1)}, u32[]{:S(2)}, u32[]{:S(2)}) async-start(bf16[8,136,128]{2,1,0:T(8,128)(2,1)} %get-tuple-element.21), calls=%async_computation | async-start | bytes 557056 | tf_op jit(solution)/shard_map/all_to_all | solution.py:213
  9.3 4.9 %all-to-all-done.all_ref = bf16[8,136,128]{2,1,0:T(8,128)(2,1)S(1)} async-done(((bf16[8,136,128]{2,1,0:T(8,128)(2,1)}), bf16[8,136,128]{2,1,0:T(8,128)(2,1)S(1)}, u32[]{:S(2)}, u32[]{:S(2)}) %all-to-all-start) | async-done | bytes 278560 | tf_op jit(solution)/shard_map/all_to_all | solution.py:213
  15.0 7.7 %all-to-all-start.1 = ((bf16[8,136,128]{2,1,0:T(8,128)(2,1)}), bf16[8,136,128]{2,1,0:T(8,128)(2,1)S(1)}, u32[]{:S(2)}, u32[]{:S(2)}) async-start(bf16[8,136,128]{2,1,0:T(8,128)(2,1)} %get-tuple-element.27), calls=%async_computation.1 | async-start | bytes 557056 | tf_op jit(solution)/shard_map/all_to_all | solution.py:219
  23.5 1.8 shard_map.138
  25.2 9.3 %all-to-all-done.1.all_ref = bf16[8,136,128]{2,1,0:T(8,128)(2,1)S(1)} async-done(((bf16[8,136,128]{2,1,0:T(8,128)(2,1)}), bf16[8,136,128]{2,1,0:T(8,128)(2,1)S(1)}, u32[]{:S(2)}, u32[]{:S(2)}) %all-to-all-start.1) | async-done | bytes 278560 | tf_op jit(solution)/shard_map/all_to_all | solution.py:219
  35.6 4.5 %all-to-all-start.2 = ((bf16[4,64,256]{2,1,0:T(8,128)(2,1)}), bf16[4,64,256]{2,1,0:T(8,128)(2,1)S(1)}, u32[]{:S(2)}, u32[]{:S(2)}) async-start(bf16[4,64,256]{2,1,0:T(8,128)(2,1)} %shard_map.139), calls=%async_computation.2 | async-start | bytes 262144 | tf_op jit(solution)/shard_map/all_to_all | solution.py:226
  40.6 5.4 %all-to-all-done.2.piece_ref = bf16[4,64,256]{2,1,0:T(8,128)(2,1)S(1)} async-done(((bf16[4,64,256]{2,1,0:T(8,128)(2,1)}), bf16[4,64,256]{2,1,0:T(8,128)(2,1)S(1)}, u32[]{:S(2)}, u32[]{:S(2)}) %all-to-all-start.2) | async-done | bytes 131104 | tf_op jit(solution)/shard_map/all_to_all | solution.py:226
  46.0 5.0 %shard_map.140 = (bf16[64,2048]{1,0:T(8,128)(2,1)}, bf16[64,2048]{1,0:T(8,128)(2,1)}, bf16[32,8,2048]{2,1,0:T(8,128)(2,1)}) custom-call(bf16[64,2048]{1,0:T(8,128)(2,1)} %res_ref.1, bf16[1,2048]{1,0:T(2,128)(2,1)} %broadcast_in_dim.68.gain_ref, f32[32,64]{1,0:T(8,128)} %get-tuple-element.38.rank_ref, bf16[4,64,256]{2,1,0:T(8,128)(2,1)S(1)} %all-to-all-done.2.piece_ref, ...), custom_call_target="tpu_custom_call" | custom-call | flops 1048576 | bytes 524288 | tf_op jit(solution)/shard_map/pallas_call | solution.py:180
  51.3 1.6 collective-permute-done.6
  54.3 5.0 %all-to-all-start.5 = ((bf16[32,8,2048]{2,1,0:T(8,128)(2,1)}), bf16[32,8,2048]{2,1,0:T(8,128)(2,1)S(1)}, u32[]{:S(2)}, u32[]{:S(2)}) async-start(bf16[32,8,2048]{2,1,0:T(8,128)(2,1)} %fusion), calls=%async_computation.5 | async-start | bytes 2097152 | tf_op jit(solution)/shard_map/all_to_all | solution.py:357
  60.7 2.1 collective-permute-start.1
  63.9 24.2 %all-to-all-done.5 = bf16[32,8,2048]{2,1,0:T(8,128)(2,1)S(1)} async-done(((bf16[32,8,2048]{2,1,0:T(8,128)(2,1)}), bf16[32,8,2048]{2,1,0:T(8,128)(2,1)S(1)}, u32[]{:S(2)}, u32[]{:S(2)}) %all-to-all-start.5) | async-done | bytes 1048608 | tf_op jit(solution)/shard_map/all_to_all | solution.py:357
  88.7 5.6 %all-to-all-start.3 = ((bf16[32,8,2048]{2,1,0:T(8,128)(2,1)}), bf16[32,8,2048]{2,1,0:T(8,128)(2,1)}, u32[]{:S(2)}, u32[]{:S(2)}) async-start(bf16[32,8,2048]{2,1,0:T(8,128)(2,1)} %get-tuple-element.29), calls=%async_computation.3 | async-start | bytes 2097152 | tf_op jit(solution)/shard_map/all_to_all | solution.py:357
  94.3 26.2 %collective-permute-done.1.refs_4_ = bf16[2048,512]{1,0:T(8,128)(2,1)} collective-permute-done((bf16[2048,512]{1,0:T(8,128)(2,1)}, bf16[2048,512]{1,0:T(8,128)(2,1)}, u32[]{:S(2)}, u32[]{:S(2)}) %collective-permute-start.1) | collective-permute-done | bytes 2097184 | tf_op jit(solution)/shard_map/ppermute | solution.py:313
  120.5 22.5 %collective-permute-done.2.refs_5_ = bf16[512,2048]{1,0:T(8,128)(2,1)} collective-permute-done((bf16[512,2048]{1,0:T(8,128)(2,1)}, bf16[512,2048]{1,0:T(8,128)(2,1)}, u32[]{:S(2)}, u32[]{:S(2)}) %collective-permute-start.2) | collective-permute-done | bytes 2097184 | tf_op jit(solution)/shard_map/ppermute | solution.py:313
  143.0 4.7 %shard_map.141 = (bf16[2048,512]{1,0:T(8,128)(2,1)S(1)}, bf16[2048,512]{1,0:T(8,128)(2,1)S(1)}, bf16[512,2048]{1,0:T(8,128)(2,1)S(1)}, bf16[2048,512]{1,0:T(8,12...) custom-call(bf16[2048,512]{1,0:T(8,128)(2,1)} %bitcast.66, bf16[2048,512]{1,0:T(8,128)(2,1)} %bitcast.69, ...), custom_call_target="tpu_custom_call" | custom-call | flops 1048576 | bytes 524288 | tf_op jit(solution)/shard_map/pallas_call | solution.py:180
  147.8 6.7 %shard_map.145 = bf16[256,2048]{1,0:T(8,128)(2,1)} custom-call(bf16[256,2048]{1,0:T(8,128)(2,1)} %collective-permute-done.7.x_ref, bf16[2048,512]{1,0:T(8,128)(2,1)S(1)} %get-tuple-element.30.g0, bf16[2048,512]{1,0:T(8,128)(2,1)S(1)} %get-tuple-element.31.u0, bf16[512,2048]{1,0:T(8,128)(2,1)S(1)} %get-tuple-element.32.d0, ...), custom_call_target="tpu_custom_call" | custom-call | flops 3221225472 | bytes 524288 | tf_op jit(solution)/shard_map/pallas_call | solution.py:180
  154.6 2.0 collective-permute-start.3
  156.6 1.6 copy-done.2
  158.2 1.6 copy-done.5
  159.8 1.6 copy-done.8
  161.4 1.6 copy-done.11
  163.0 1.6 copy-done.14
  164.6 3.6 %shard_map.144 = bf16[256,2048]{1,0:T(8,128)(2,1)S(1)} custom-call(bf16[256,2048]{1,0:T(8,128)(2,1)S(1)} %bitcast.64, bf16[2048,512]{1,0:T(8,128)(2,1)S(1)} %get-tuple-element.30.g0, bf16[2048,512]{1,0:T(8,128)(2,1)S(1)} %copy-done.2, bf16[512,2048]{1,0:T(8,128)(2,1)S(1)} %copy-done.5, bf16[2048,512]{1,0:T(8,128)(2,1)S(1)} %copy-done.8, ...), custom_call_target="tpu_custom_call" | custom-call | flops 3221225472 | bytes 524288 | tf_op jit(solution)/shard_map/pallas_call | solution.py:180
  169.7 2.5 %fusion.11 = bf16[32,8,2048]{2,1,0:T(8,128)(2,1)} fusion(bf16[256,2048]{1,0:T(8,128)(2,1)} %collective-permute-done.8, bf16[256,2048]{1,0:T(8,128)(2,1)S(1)} %shard_map.144), kind=kLoop, calls=%fused_computation.16 | loop fusion | flops 2097152 | bytes 3145728 | tf_op jit(solution)/shard_map/reshape | solution.py:368
  172.2 9.9 %all-to-all-start.6 = ((bf16[32,8,2048]{2,1,0:T(8,128)(2,1)}), bf16[32,8,2048]{2,1,0:T(8,128)(2,1)S(1)}, u32[]{:S(2)}, u32[]{:S(2)}) async-start(bf16[32,8,2048]{2,1,0:T(8,128)(2,1)} %fusion.11), calls=%async_computation.6 | async-start | bytes 2097152 | tf_op jit(solution)/shard_map/all_to_all | solution.py:368
  190.1 4.8 %shard_map.143 = bf16[256,2048]{1,0:T(8,128)(2,1)S(1)} custom-call(bf16[256,2048]{1,0:T(8,128)(2,1)} %collective-permute-done.3.x_ref, bf16[2048,512]{1,0:T(8,128)(2,1)S(1)} %get-tuple-element.30.g0, bf16[2048,512]{1,0:T(8,128)(2,1)S(1)} %copy-done.3, bf16[512,2048]{1,0:T(8,128)(2,1)S(1)} %copy-done.6, bf16[2048,512]{1,0:T(8,128)(2,1)S(1)} %copy-done.9, ...), custom_call_target="tpu_custom_call" | custom-call | flops 3221225472 | bytes 524288 | tf_op jit(solution)/shard_map/pallas_call | solution.py:180
  195.0 4.8 %shard_map.142 = bf16[256,2048]{1,0:T(8,128)(2,1)S(1)} custom-call(bf16[256,2048]{1,0:T(8,128)(2,1)} %bitcast.10.x_ref, bf16[2048,512]{1,0:T(8,128)(2,1)S(1)} %get-tuple-element.30.g0, bf16[2048,512]{1,0:T(8,128)(2,1)S(1)} %copy-done.3, bf16[512,2048]{1,0:T(8,128)(2,1)S(1)} %copy-done.6, bf16[2048,512]{1,0:T(8,128)(2,1)S(1)} %copy-done.9, ...), custom_call_target="tpu_custom_call" | custom-call | flops 3221225472 | bytes 524288 | tf_op jit(solution)/shard_map/pallas_call | solution.py:180
  199.9 9.9 %collective-permute-done.4 = bf16[256,2048]{1,0:T(8,128)(2,1)S(1)} collective-permute-done((bf16[256,2048]{1,0:T(8,128)(2,1)S(1)}, bf16[256,2048]{1,0:T(8,128)(2,1)S(1)}, u32[]{:S(2)}, u32[]{:S(2)}) %collective-permute-start.4) | collective-permute-done | bytes 1048608 | tf_op jit(solution)/shard_map/ppermute | solution.py:366
  211.2 9.8 %all-to-all-start.4 = ((bf16[32,8,2048]{2,1,0:T(8,128)(2,1)}), bf16[32,8,2048]{2,1,0:T(8,128)(2,1)S(1)}, u32[]{:S(2)}, u32[]{:S(2)}) async-start(bf16[32,8,2048]{2,1,0:T(8,128)(2,1)} %fusion.10), calls=%async_computation.4 | async-start | bytes 2097152 | tf_op jit(solution)/shard_map/all_to_all | solution.py:368
  221.8 24.5 %all-to-all-done.4 = bf16[32,8,2048]{2,1,0:T(8,128)(2,1)S(1)} async-done(((bf16[32,8,2048]{2,1,0:T(8,128)(2,1)}), bf16[32,8,2048]{2,1,0:T(8,128)(2,1)S(1)}, u32[]{:S(2)}, u32[]{:S(2)}) %all-to-all-start.4) | async-done | bytes 1048608 | tf_op jit(solution)/shard_map/all_to_all | solution.py:368
  (76 shorter events, 22.2 us)
Async XLA Ops:
  0.0 7.9 %copy-start = (s32[256,4]{0,1:T(4,128)S(1)}, s32[256,4]{0,1:T(4,128)}, u32[]{:S(2)}) copy-start(s32[256,4]{0,1:T(4,128)} %param.23) | copy-start | bytes 12292
  0.0 22.8 %copy-start.19 = (bf16[2048]{0:T(1024)(128)(2,1)S(1)}, bf16[2048]{0:T(1024)(128)(2,1)}, u32[]{:S(2)}) copy-start(bf16[2048]{0:T(1024)(128)(2,1)} %param.22) | copy-start | bytes 12292
  0.0 34.5 %copy-start.17 = (bf16[128]{0:T(256)(128)(2,1)S(1)}, bf16[128]{0:T(256)(128)(2,1)}, u32[]{:S(2)}) copy-start(bf16[128]{0:T(256)(128)(2,1)} %param.20) | copy-start | bytes 772
  0.0 34.5 %copy-start.16 = (bf16[256,256]{1,0:T(8,128)(2,1)S(1)}, bf16[256,256]{1,0:T(8,128)(2,1)}, u32[]{:S(2)}) copy-start(bf16[256,256]{1,0:T(8,128)(2,1)} %gate_ref.1) | copy-start | bytes 393220
  2.4 11.8 %all-to-all-start = ((bf16[8,136,128]{2,1,0:T(8,128)(2,1)}), bf16[8,136,128]{2,1,0:T(8,128)(2,1)S(1)}, u32[]{:S(2)}, u32[]{:S(2)}) async-start(bf16[8,136,128]{2,1,0:T(8,128)(2,1)} %get-tuple-element.21), calls=%async_computation | async-start | bytes 557056 | tf_op jit(solution)/shard_map/all_to_all | solution.py:213
  15.0 19.5 %all-to-all-start.1 = ((bf16[8,136,128]{2,1,0:T(8,128)(2,1)}), bf16[8,136,128]{2,1,0:T(8,128)(2,1)S(1)}, u32[]{:S(2)}, u32[]{:S(2)}) async-start(bf16[8,136,128]{2,1,0:T(8,128)(2,1)} %get-tuple-element.27), calls=%async_computation.1 | async-start | bytes 557056 | tf_op jit(solution)/shard_map/all_to_all | solution.py:219
  22.7 28.6 %collective-permute-start.5 = (f32[2,64,32]{1,2,0:T(8,128)S(1)}, f32[2,64,32]{1,2,0:T(8,128)S(1)}, u32[]{:S(2)}, u32[]{:S(2)}) collective-permute-start(f32[2,64,32]{1,2,0:T(8,128)S(1)} %dynamic-slice_bitcast_fusion), channel_id=1, source_target_pairs={{0,4},{4,0},{1,5},{5,1},{2,6},{6,2},{3,7},{7,3},{8,12},{12,8},{9,1... | collective-permute-start | bytes 49160 | tf_op jit(solution)/shard_map/ppermute | solution.py:331
  35.6 10.4 %all-to-all-start.2 = ((bf16[4,64,256]{2,1,0:T(8,128)(2,1)}), bf16[4,64,256]{2,1,0:T(8,128)(2,1)S(1)}, u32[]{:S(2)}, u32[]{:S(2)}) async-start(bf16[4,64,256]{2,1,0:T(8,128)(2,1)} %shard_map.139), calls=%async_computation.2 | async-start | bytes 262144 | tf_op jit(solution)/shard_map/all_to_all | solution.py:226
  51.1 8.3 %copy-start.18 = (bf16[1,2048,512]{2,1,0:T(8,128)(2,1)S(1)}, bf16[1,2048,512]{2,1,0:T(8,128)(2,1)}, u32[]{:S(2)}) copy-start(bf16[1,2048,512]{2,1,0:T(8,128)(2,1)} %param.25) | copy-start | bytes 6291460
  51.1 1.8 collective-permute-start.6
  54.3 33.8 %all-to-all-start.5 = ((bf16[32,8,2048]{2,1,0:T(8,128)(2,1)}), bf16[32,8,2048]{2,1,0:T(8,128)(2,1)S(1)}, u32[]{:S(2)}, u32[]{:S(2)}) async-start(bf16[32,8,2048]{2,1,0:T(8,128)(2,1)} %fusion), calls=%async_computation.5 | async-start | bytes 2097152 | tf_op jit(solution)/shard_map/all_to_all | solution.py:357
  59.4 34.9 %collective-permute-start = (bf16[2048,512]{1,0:T(8,128)(2,1)S(1)}, bf16[2048,512]{1,0:T(8,128)(2,1)}, u32[]{:S(2)}, u32[]{:S(2)}) collective-permute-start(bf16[2048,512]{1,0:T(8,128)(2,1)S(1)} %bitcast.67), channel_id=1, source_target_pairs={{0,3},{1,2},{2,1},{3,0},{4,5},{5,4},{6,7},{7,6},{8,11},{9,10},{10,... | collective-permute-start | bytes 6291464 | tf_op jit(solution)/shard_map/ppermute | solution.py:313
  60.7 59.9 %collective-permute-start.1 = (bf16[2048,512]{1,0:T(8,128)(2,1)}, bf16[2048,512]{1,0:T(8,128)(2,1)}, u32[]{:S(2)}, u32[]{:S(2)}) collective-permute-start(bf16[2048,512]{1,0:T(8,128)(2,1)} %bitcast.68), channel_id=1, source_target_pairs={{0,3},{1,2},{2,1},{3,0},{4,5},{5,4},{6,7},{7,6},{8,11},{9,10},{10,... | collective-permute-start | bytes 6291464 | tf_op jit(solution)/shard_map/ppermute | solution.py:313
  62.7 80.3 %collective-permute-start.2 = (bf16[512,2048]{1,0:T(8,128)(2,1)}, bf16[512,2048]{1,0:T(8,128)(2,1)}, u32[]{:S(2)}, u32[]{:S(2)}) collective-permute-start(bf16[512,2048]{1,0:T(8,128)(2,1)} %bitcast.70), channel_id=1, source_target_pairs={{0,3},{1,2},{2,1},{3,0},{4,5},{5,4},{6,7},{7,6},{8,11},{9,10},{10,... | collective-permute-start | bytes 6291464 | tf_op jit(solution)/shard_map/ppermute | solution.py:313
  88.1 59.7 %collective-permute-start.7 = (bf16[256,2048]{1,0:T(8,128)(2,1)S(1)}, bf16[256,2048]{1,0:T(8,128)(2,1)}, u32[]{:S(2)}, u32[]{:S(2)}) collective-permute-start(bf16[256,2048]{1,0:T(8,128)(2,1)S(1)} %bitcast.63), channel_id=1, source_target_pairs={{0,1},{1,0},{2,3},{3,2},{4,7},{5,6},{6,5},{7,4},{8,9},{9,8},{10,11... | collective-permute-start | bytes 3145736 | tf_op jit(solution)/shard_map/ppermute | solution.py:360
  88.7 65.9 %all-to-all-start.3 = ((bf16[32,8,2048]{2,1,0:T(8,128)(2,1)}), bf16[32,8,2048]{2,1,0:T(8,128)(2,1)}, u32[]{:S(2)}, u32[]{:S(2)}) async-start(bf16[32,8,2048]{2,1,0:T(8,128)(2,1)} %get-tuple-element.29), calls=%async_computation.3 | async-start | bytes 2097152 | tf_op jit(solution)/shard_map/all_to_all | solution.py:357
  147.7 6.7 %copy-start.1 = (bf16[2048,512]{1,0:T(8,128)(2,1)}, bf16[2048,512]{1,0:T(8,128)(2,1)S(1)}, u32[]{:S(2)}) copy-start(bf16[2048,512]{1,0:T(8,128)(2,1)S(1)} %get-tuple-element.31.u0) | copy-start | bytes 6291460
  147.7 6.7 %copy-start.4 = (bf16[512,2048]{1,0:T(8,128)(2,1)}, bf16[512,2048]{1,0:T(8,128)(2,1)S(1)}, u32[]{:S(2)}) copy-start(bf16[512,2048]{1,0:T(8,128)(2,1)S(1)} %get-tuple-element.32.d0) | copy-start | bytes 6291460
  147.8 6.7 %copy-start.7 = (bf16[2048,512]{1,0:T(8,128)(2,1)}, bf16[2048,512]{1,0:T(8,128)(2,1)S(1)}, u32[]{:S(2)}) copy-start(bf16[2048,512]{1,0:T(8,128)(2,1)S(1)} %get-tuple-element.33.g1) | copy-start | bytes 6291460
  147.8 6.7 %copy-start.10 = (bf16[2048,512]{1,0:T(8,128)(2,1)}, bf16[2048,512]{1,0:T(8,128)(2,1)S(1)}, u32[]{:S(2)}) copy-start(bf16[2048,512]{1,0:T(8,128)(2,1)S(1)} %get-tuple-element.34.u1) | copy-start | bytes 6291460
  147.8 6.7 %copy-start.13 = (bf16[512,2048]{1,0:T(8,128)(2,1)}, bf16[512,2048]{1,0:T(8,128)(2,1)S(1)}, u32[]{:S(2)}) copy-start(bf16[512,2048]{1,0:T(8,128)(2,1)S(1)} %get-tuple-element.35.d1) | copy-start | bytes 6291460
  154.5 15.2 %collective-permute-start.8 = (bf16[256,2048]{1,0:T(8,128)(2,1)}, bf16[256,2048]{1,0:T(8,128)(2,1)}, u32[]{:S(2)}, u32[]{:S(2)}) collective-permute-start(bf16[256,2048]{1,0:T(8,128)(2,1)} %shard_map.145), channel_id=1, source_target_pairs={{0,1},{1,0},{2,3},{3,2},{4,7},{5,6},{6,5},{7,4},{8,9},{9,8},{10,11... | collective-permute-start | bytes 3145736 | tf_op jit(solution)/shard_map/ppermute | solution.py:366
  154.6 27.5 %collective-permute-start.3 = (bf16[256,2048]{1,0:T(8,128)(2,1)}, bf16[256,2048]{1,0:T(8,128)(2,1)}, u32[]{:S(2)}, u32[]{:S(2)}) collective-permute-start(bf16[256,2048]{1,0:T(8,128)(2,1)} %bitcast.10.x_ref), channel_id=1, source_target_pairs={{0,1},{1,0},{2,3},{3,2},{4,7},{5,6},{6,5},{7,4},{8,9},{9,8},{10,11... | collective-permute-start | bytes 3145736 | tf_op jit(solution)/shard_map/ppermute | solution.py:360
  156.6 1.6 copy-start.2
  158.2 1.6 copy-start.5
  159.8 1.6 copy-start.8
  172.2 39.0 %all-to-all-start.6 = ((bf16[32,8,2048]{2,1,0:T(8,128)(2,1)}), bf16[32,8,2048]{2,1,0:T(8,128)(2,1)S(1)}, u32[]{:S(2)}, u32[]{:S(2)}) async-start(bf16[32,8,2048]{2,1,0:T(8,128)(2,1)} %fusion.11), calls=%async_computation.6 | async-start | bytes 2097152 | tf_op jit(solution)/shard_map/all_to_all | solution.py:368
  182.1 1.6 copy-start.3
  194.9 14.9 %collective-permute-start.4 = (bf16[256,2048]{1,0:T(8,128)(2,1)S(1)}, bf16[256,2048]{1,0:T(8,128)(2,1)S(1)}, u32[]{:S(2)}, u32[]{:S(2)}) collective-permute-start(bf16[256,2048]{1,0:T(8,128)(2,1)S(1)} %shard_map.143), channel_id=1, source_target_pairs={{0,1},{1,0},{2,3},{3,2},{4,7},{5,6},{6,5},{7,4},{8,9},{9,8},{10,11... | collective-permute-start | bytes 3145736 | tf_op jit(solution)/shard_map/ppermute | solution.py:366
  211.2 35.0 %all-to-all-start.4 = ((bf16[32,8,2048]{2,1,0:T(8,128)(2,1)}), bf16[32,8,2048]{2,1,0:T(8,128)(2,1)S(1)}, u32[]{:S(2)}, u32[]{:S(2)}) async-start(bf16[32,8,2048]{2,1,0:T(8,128)(2,1)} %fusion.10), calls=%async_computation.4 | async-start | bytes 2097152 | tf_op jit(solution)/shard_map/all_to_all | solution.py:368
  221.0 25.2 %copy-start.20 = (bf16[64,2048]{1,0:T(8,128)(2,1)S(1)}, bf16[64,2048]{1,0:T(8,128)(2,1)}, u32[]{:S(2)}) copy-start(bf16[64,2048]{1,0:T(8,128)(2,1)} %get-tuple-element.28) | copy-start | bytes 786436
  221.7 24.6 %collective-permute-start.9 = (f32[64,2048]{1,0:T(8,128)S(1)}, f32[64,2048]{1,0:T(8,128)S(1)}, u32[]{:S(2)}, u32[]{:S(2)}) collective-permute-start(f32[64,2048]{1,0:T(8,128)S(1)} %fusion.6), channel_id=1, source_target_pairs={{0,4},{4,0},{1,5},{5,1},{2,6},{6,2},{3,7},{7,3},{8,12},{12,8},{9,1... | collective-permute-start | bytes 1572872 | tf_op jit(solution)/shard_map/ppermute | solution.py:372
  (6 other events, 9.5 us)

commit v4 on v3

--- a/solution.py
+++ b/solution.py
@@ -21,6 +21,7 @@
 BF16 = jnp.bfloat16
 
 ROW_PAIRS = [(c * 4 + y, c * 4 + ((y ^ 1) if c == 0 else 3 - y)) for c in range(2) for y in range(4)]
+CROSS_PAIRS = [(a, b ^ 4) for a, b in ROW_PAIRS]
 WEIGHT_PAIRS = [(c * 4 + y, c * 4 + ((3 - y) if c == 0 else (y ^ 1))) for c in range(2) for y in range(4)]
 
 
@@ -328,8 +329,7 @@
     core = lax.axis_index("sp_2")
     here = lax.dynamic_index_in_dim(both, core, 3, keepdims=False)
     away = lax.dynamic_index_in_dim(both, 1 - core, 3, keepdims=False)
-    theirs_plan = lax.ppermute(away, "sp_2", swap_cores)
-    plans = (here, theirs_plan)
+    crossing = lax.ppermute(away[0], "sp_2", swap_cores)
 
     pieces = mixer(queries, key_rows, value_rows, out_gate, decay_logit, head_gain)
     residual, normed, rows = call(
@@ -351,26 +351,29 @@
     arrived, swapped = [], []
     for c in range(2):
         if c:
-            send = (theirs_plan[0].T[:, None, :] == slots[None, :, None]).astype(BF16)
+            send = (crossing.T[:, None, :] == slots[None, :, None]).astype(BF16)
             rows = jnp.dot(send.reshape(columns * cap, quarter), normed_other, preferred_element_type=F32)
             rows = rows.astype(BF16).reshape(columns, cap, width)
         rows = lax.all_to_all(rows, columns_axes, 0, 0, tiled=True)
         rows = rows.reshape(columns * cap, width)
         arrived.append(rows)
         swapped.append(lax.ppermute(rows, core_tp, ROW_PAIRS))
-    sums = []
-    for c in range(2):
+    routed = residual.astype(F32)
+    for c, plan in enumerate((here, away)):
         weights = load((*own, *other))
         theirs = ffn(swapped[c], weights, shaped)
         mine = ffn(arrived[c], weights, resident)
-        back = lax.ppermute(theirs, core_tp, ROW_PAIRS)
+        back = lax.ppermute(theirs, core_tp, CROSS_PAIRS if c else ROW_PAIRS)
+        if c:
+            mine = lax.ppermute(mine, "sp_2", swap_cores)
         out = (mine.astype(F32) + back.astype(F32)).astype(BF16)
         home = lax.all_to_all(out.reshape(columns, cap, width), columns_axes, 0, 0, tiled=True)
         home = home.reshape(columns * cap, width)
-        lead, rest = blend(plans[c][0], plans[c][1], cap)
-        sums.append(jnp.dot(jnp.concatenate([lead, rest], axis=1), jnp.concatenate([home, home]), preferred_element_type=F32))
-    from_other = lax.ppermute(sums[1], "sp_2", swap_cores)
-    return (residual.astype(F32) + (sums[0] + from_other)).astype(BF16)
+        parts = blend(plan[0], plan[1], cap)
+        routed = routed + jnp.dot(
+            jnp.concatenate(parts, axis=1), jnp.concatenate([home, home]), preferred_element_type=F32
+        )
+    return routed.astype(BF16)
 
 
 def solution(mesh):

time: 249 us -> 254 us (1.020)
  waiting for transfers between devices: 130 us -> 134 us
    ppermute x4, waiting for transfers between devices: 11.5 us -> 18 us  [the longest x2 16.9 us: on_device(): back = lax.ppermute(theirs, core_tp, CROSS_PAIRS if c else ROW_PAIRS)]
    all_to_all x2, waiting for transfers between devices: 24.2 us -> 18.7 us  [on_device(): rows = lax.all_to_all(rows, columns_axes, 0, 0, tiled=True)]
    all_to_all x2, waiting for transfers between devices: 24.5 us -> 27.1 us  [on_device(): lax.all_to_all(out.reshape(columns, cap, width), columns_axes, 0, 0, tile...]
    unnamed x43 -> x41, local copies, waits for them, and re-layouts: 16 us -> 15.9 us
  transfers between devices with their start and end apart: 17 -> 17, of which waited for: 10 -> 10; matrix products, arithmetic and copies ran while one was open for 3% -> 4% of each run, Pallas kernels for 13% -> 10%
where the time goes in v4:
time: 254 us; the launch traced here: 252 us
  waiting for transfers between devices  134 us (53%)
  starting transfers between devices  56.1 us (22%)
  Pallas kernels  35.5 us (14%)
  local copies, waits for them, and re-layouts  18.2 us (7%)
  other arithmetic  4.97 us (2%)
  matrix products  3.37 us (1%)
    ppermute x3, waiting for transfers between devices, on_device(): other.append(lax.ppermute(w, core_tp, WEIGHT_PAIRS))  51 us
    pallas_call x10, Pallas kernels, call(): pl.pallas_call(kernel, out_shape=outs, in_specs=specs, out_specs=[pl.Bloc...  35.5 us
    all_to_all x2, waiting for transfers between devices, on_device(): lax.all_to_all(out.reshape(columns, cap, width), columns_axes, 0, 0, tile...  27.1 us
    all_to_all x2, starting transfers between devices, on_device(): lax.all_to_all(out.reshape(columns, cap, width), columns_axes, 0, 0, tile...  19.7 us
    all_to_all x2, waiting for transfers between devices, on_device(): rows = lax.all_to_all(rows, columns_axes, 0, 0, tiled=True)  18.7 us
    ppermute x2, waiting for transfers between devices, on_device(): back = lax.ppermute(theirs, core_tp, CROSS_PAIRS if c else ROW_PAIRS)  16.9 us
    unnamed x41, local copies, waits for them, and re-layouts  15.9 us
    all_to_all x2, starting transfers between devices, on_device(): rows = lax.all_to_all(rows, columns_axes, 0, 0, tiled=True)  10.8 us
  transfers between devices with their start and end apart: 17, of which 10 were waited for; matrix products, arithmetic and copies ran while one was open for 4% of the time, Pallas kernels for 10%

profile of v4, /device:TPU:2, one launch (start us, length us, event | category | flops | bytes accessed | tf_op | source)
XLA Modules:
  0.0 252.4 jit_solution(7239902913413102022)
XLA Ops:
  0.0 2.3 shard_map.136
  2.4 5.6 %all-to-all-start = ((bf16[8,136,128]{2,1,0:T(8,128)(2,1)}), bf16[8,136,128]{2,1,0:T(8,128)(2,1)S(1)}, u32[]{:S(2)}, u32[]{:S(2)}) async-start(bf16[8,136,128]{2,1,0:T(8,128)(2,1)} %get-tuple-element.21), calls=%async_computation | async-start | bytes 557056 | tf_op jit(solution)/shard_map/all_to_all | solution.py:214
  8.3 5.9 %all-to-all-done.all_ref = bf16[8,136,128]{2,1,0:T(8,128)(2,1)S(1)} async-done(((bf16[8,136,128]{2,1,0:T(8,128)(2,1)}), bf16[8,136,128]{2,1,0:T(8,128)(2,1)S(1)}, u32[]{:S(2)}, u32[]{:S(2)}) %all-to-all-start) | async-done | bytes 278560 | tf_op jit(solution)/shard_map/all_to_all | solution.py:214
  15.0 7.7 %all-to-all-start.1 = ((bf16[8,136,128]{2,1,0:T(8,128)(2,1)}), bf16[8,136,128]{2,1,0:T(8,128)(2,1)S(1)}, u32[]{:S(2)}, u32[]{:S(2)}) async-start(bf16[8,136,128]{2,1,0:T(8,128)(2,1)} %get-tuple-element.27), calls=%async_computation.1 | async-start | bytes 557056 | tf_op jit(solution)/shard_map/all_to_all | solution.py:220
  25.0 1.8 shard_map.138
  26.8 7.8 %all-to-all-done.1.all_ref = bf16[8,136,128]{2,1,0:T(8,128)(2,1)S(1)} async-done(((bf16[8,136,128]{2,1,0:T(8,128)(2,1)}), bf16[8,136,128]{2,1,0:T(8,128)(2,1)S(1)}, u32[]{:S(2)}, u32[]{:S(2)}) %all-to-all-start.1) | async-done | bytes 278560 | tf_op jit(solution)/shard_map/all_to_all | solution.py:220
  35.6 4.5 %all-to-all-start.2 = ((bf16[4,64,256]{2,1,0:T(8,128)(2,1)}), bf16[4,64,256]{2,1,0:T(8,128)(2,1)S(1)}, u32[]{:S(2)}, u32[]{:S(2)}) async-start(bf16[4,64,256]{2,1,0:T(8,128)(2,1)} %shard_map.139), calls=%async_computation.2 | async-start | bytes 262144 | tf_op jit(solution)/shard_map/all_to_all | solution.py:227
  40.6 5.4 %all-to-all-done.2.piece_ref = bf16[4,64,256]{2,1,0:T(8,128)(2,1)S(1)} async-done(((bf16[4,64,256]{2,1,0:T(8,128)(2,1)}), bf16[4,64,256]{2,1,0:T(8,128)(2,1)S(1)}, u32[]{:S(2)}, u32[]{:S(2)}) %all-to-all-start.2) | async-done | bytes 131104 | tf_op jit(solution)/shard_map/all_to_all | solution.py:227
  46.0 5.0 %shard_map.140 = (bf16[64,2048]{1,0:T(8,128)(2,1)}, bf16[64,2048]{1,0:T(8,128)(2,1)}, bf16[32,8,2048]{2,1,0:T(8,128)(2,1)}) custom-call(bf16[64,2048]{1,0:T(8,128)(2,1)} %res_ref.1, bf16[1,2048]{1,0:T(2,128)(2,1)} %broadcast_in_dim.68.gain_ref, f32[32,64]{1,0:T(8,128)} %get-tuple-element.38.rank_ref, bf16[4,64,256]{2,1,0:T(8,128)(2,1)S(1)} %all-to-all-done.2.piece_ref, ...), custom_call_target="tpu_custom_call" | custom-call | flops 1048576 | bytes 524288 | tf_op jit(solution)/shard_map/pallas_call | solution.py:181
  51.0 5.2 %all-to-all-start.3 = ((bf16[32,8,2048]{2,1,0:T(8,128)(2,1)}), bf16[32,8,2048]{2,1,0:T(8,128)(2,1)S(1)}, u32[]{:S(2)}, u32[]{:S(2)}) async-start(bf16[32,8,2048]{2,1,0:T(8,128)(2,1)} %get-tuple-element.29), calls=%async_computation.3 | async-start | bytes 2097152 | tf_op jit(solution)/shard_map/all_to_all | solution.py:357
  57.5 2.1 collective-permute-start.1
  62.5 18.7 %all-to-all-done.3 = bf16[32,8,2048]{2,1,0:T(8,128)(2,1)S(1)} async-done(((bf16[32,8,2048]{2,1,0:T(8,128)(2,1)}), bf16[32,8,2048]{2,1,0:T(8,128)(2,1)S(1)}, u32[]{:S(2)}, u32[]{:S(2)}) %all-to-all-start.3) | async-done | bytes 1048608 | tf_op jit(solution)/shard_map/all_to_all | solution.py:357
  83.2 5.6 %all-to-all-start.5 = ((bf16[32,8,2048]{2,1,0:T(8,128)(2,1)}), bf16[32,8,2048]{2,1,0:T(8,128)(2,1)}, u32[]{:S(2)}, u32[]{:S(2)}) async-start(bf16[32,8,2048]{2,1,0:T(8,128)(2,1)} %fusion), calls=%async_computation.5 | async-start | bytes 2097152 | tf_op jit(solution)/shard_map/all_to_all | solution.py:357
  88.9 28.5 %collective-permute-done.1.refs_4_ = bf16[2048,512]{1,0:T(8,128)(2,1)} collective-permute-done((bf16[2048,512]{1,0:T(8,128)(2,1)}, bf16[2048,512]{1,0:T(8,128)(2,1)}, u32[]{:S(2)}, u32[]{:S(2)}) %collective-permute-start.1) | collective-permute-done | bytes 2097184 | tf_op jit(solution)/shard_map/ppermute | solution.py:314
  117.4 22.5 %collective-permute-done.2.refs_5_ = bf16[512,2048]{1,0:T(8,128)(2,1)} collective-permute-done((bf16[512,2048]{1,0:T(8,128)(2,1)}, bf16[512,2048]{1,0:T(8,128)(2,1)}, u32[]{:S(2)}, u32[]{:S(2)}) %collective-permute-start.2) | collective-permute-done | bytes 2097184 | tf_op jit(solution)/shard_map/ppermute | solution.py:314
  139.8 4.7 %shard_map.141 = (bf16[2048,512]{1,0:T(8,128)(2,1)S(1)}, bf16[2048,512]{1,0:T(8,128)(2,1)S(1)}, bf16[512,2048]{1,0:T(8,128)(2,1)S(1)}, bf16[2048,512]{1,0:T(8,12...) custom-call(bf16[2048,512]{1,0:T(8,128)(2,1)} %bitcast.62, bf16[2048,512]{1,0:T(8,128)(2,1)} %bitcast.65, ...), custom_call_target="tpu_custom_call" | custom-call | flops 1048576 | bytes 524288 | tf_op jit(solution)/shard_map/pallas_call | solution.py:181
  144.6 6.7 %shard_map.143 = bf16[256,2048]{1,0:T(8,128)(2,1)} custom-call(bf16[256,2048]{1,0:T(8,128)(2,1)} %collective-permute-done.3.x_ref, bf16[2048,512]{1,0:T(8,128)(2,1)S(1)} %get-tuple-element.30.g0, bf16[2048,512]{1,0:T(8,128)(2,1)S(1)} %get-tuple-element.31.u0, bf16[512,2048]{1,0:T(8,128)(2,1)S(1)} %get-tuple-element.32.d0, ...), custom_call_target="tpu_custom_call" | custom-call | flops 3221225472 | bytes 524288 | tf_op jit(solution)/shard_map/pallas_call | solution.py:181
  151.4 2.0 collective-permute-start.8
  153.4 1.6 copy-done.2
  155.0 1.6 copy-done.5
  156.6 1.6 copy-done.8
  158.2 1.6 copy-done.11
  159.8 1.6 copy-done.14
  161.4 3.6 %shard_map.142 = bf16[256,2048]{1,0:T(8,128)(2,1)S(1)} custom-call(bf16[256,2048]{1,0:T(8,128)(2,1)S(1)} %bitcast.60, bf16[2048,512]{1,0:T(8,128)(2,1)S(1)} %get-tuple-element.30.g0, bf16[2048,512]{1,0:T(8,128)(2,1)S(1)} %copy-done.2, bf16[512,2048]{1,0:T(8,128)(2,1)S(1)} %copy-done.5, bf16[2048,512]{1,0:T(8,128)(2,1)S(1)} %copy-done.8, ...), custom_call_target="tpu_custom_call" | custom-call | flops 3221225472 | bytes 524288 | tf_op jit(solution)/shard_map/pallas_call | solution.py:181
  166.5 2.5 %fusion.8 = bf16[32,8,2048]{2,1,0:T(8,128)(2,1)} fusion(bf16[256,2048]{1,0:T(8,128)(2,1)} %collective-permute-done.4, bf16[256,2048]{1,0:T(8,128)(2,1)S(1)} %shard_map.142), kind=kLoop, calls=%fused_computation.14 | loop fusion | flops 2097152 | bytes 3145728 | tf_op jit(solution)/shard_map/reshape | solution.py:370
  169.0 9.9 %all-to-all-start.4 = ((bf16[32,8,2048]{2,1,0:T(8,128)(2,1)}), bf16[32,8,2048]{2,1,0:T(8,128)(2,1)S(1)}, u32[]{:S(2)}, u32[]{:S(2)}) async-start(bf16[32,8,2048]{2,1,0:T(8,128)(2,1)} %fusion.8), calls=%async_computation.4 | async-start | bytes 2097152 | tf_op jit(solution)/shard_map/all_to_all | solution.py:370
  185.3 1.6 copy-done.15
  186.9 4.8 %shard_map.144 = bf16[256,2048]{1,0:T(8,128)(2,1)S(1)} custom-call(bf16[256,2048]{1,0:T(8,128)(2,1)} %bitcast.23.x_ref, bf16[2048,512]{1,0:T(8,128)(2,1)S(1)} %get-tuple-element.30.g0, bf16[2048,512]{1,0:T(8,128)(2,1)S(1)} %copy-done.3, bf16[512,2048]{1,0:T(8,128)(2,1)S(1)} %copy-done.6, bf16[2048,512]{1,0:T(8,128)(2,1)S(1)} %copy-done.9, ...), custom_call_target="tpu_custom_call" | custom-call | flops 3221225472 | bytes 524288 | tf_op jit(solution)/shard_map/pallas_call | solution.py:181
  191.8 4.8 %shard_map.145 = bf16[256,2048]{1,0:T(8,128)(2,1)S(1)} custom-call(bf16[256,2048]{1,0:T(8,128)(2,1)} %collective-permute-done.8.x_ref, bf16[2048,512]{1,0:T(8,128)(2,1)S(1)} %get-tuple-element.30.g0, bf16[2048,512]{1,0:T(8,128)(2,1)S(1)} %copy-done.3, bf16[512,2048]{1,0:T(8,128)(2,1)S(1)} %copy-done.6, bf16[2048,512]{1,0:T(8,128)(2,1)S(1)} %copy-done.9, ...), custom_call_target="tpu_custom_call" | custom-call | flops 3221225472 | bytes 524288 | tf_op jit(solution)/shard_map/pallas_call | solution.py:181
  196.9 15.3 %collective-permute-done.9 = bf16[256,2048]{1,0:T(8,128)(2,1)S(1)} collective-permute-done((bf16[256,2048]{1,0:T(8,128)(2,1)S(1)}, bf16[256,2048]{1,0:T(8,128)(2,1)S(1)}, u32[]{:S(2)}, u32[]{:S(2)}) %collective-permute-start.9) | collective-permute-done | bytes 1048608 | tf_op jit(solution)/shard_map/ppermute | solution.py:366
  213.6 9.8 %all-to-all-start.6 = ((bf16[32,8,2048]{2,1,0:T(8,128)(2,1)}), bf16[32,8,2048]{2,1,0:T(8,128)(2,1)S(1)}, u32[]{:S(2)}, u32[]{:S(2)}) async-start(bf16[32,8,2048]{2,1,0:T(8,128)(2,1)} %fusion.9), calls=%async_computation.6 | async-start | bytes 2097152 | tf_op jit(solution)/shard_map/all_to_all | solution.py:370
  224.0 27.1 %all-to-all-done.6 = bf16[32,8,2048]{2,1,0:T(8,128)(2,1)S(1)} async-done(((bf16[32,8,2048]{2,1,0:T(8,128)(2,1)}), bf16[32,8,2048]{2,1,0:T(8,128)(2,1)S(1)}, u32[]{:S(2)}, u32[]{:S(2)}) %all-to-all-start.6) | async-done | bytes 1048608 | tf_op jit(solution)/shard_map/all_to_all | solution.py:370
  (72 shorter events, 22.9 us)
Async XLA Ops:
  0.0 7.9 %copy-start = (s32[256,4]{0,1:T(4,128)S(1)}, s32[256,4]{0,1:T(4,128)}, u32[]{:S(2)}) copy-start(s32[256,4]{0,1:T(4,128)} %param.23) | copy-start | bytes 12292
  0.0 34.5 %copy-start.17 = (bf16[128]{0:T(256)(128)(2,1)S(1)}, bf16[128]{0:T(256)(128)(2,1)}, u32[]{:S(2)}) copy-start(bf16[128]{0:T(256)(128)(2,1)} %param.20) | copy-start | bytes 772
  0.0 34.5 %copy-start.16 = (bf16[256,256]{1,0:T(8,128)(2,1)S(1)}, bf16[256,256]{1,0:T(8,128)(2,1)}, u32[]{:S(2)}) copy-start(bf16[256,256]{1,0:T(8,128)(2,1)} %gate_ref.1) | copy-start | bytes 393220
  2.4 11.8 %all-to-all-start = ((bf16[8,136,128]{2,1,0:T(8,128)(2,1)}), bf16[8,136,128]{2,1,0:T(8,128)(2,1)S(1)}, u32[]{:S(2)}, u32[]{:S(2)}) async-start(bf16[8,136,128]{2,1,0:T(8,128)(2,1)} %get-tuple-element.21), calls=%async_computation | async-start | bytes 557056 | tf_op jit(solution)/shard_map/all_to_all | solution.py:214
  15.0 19.5 %all-to-all-start.1 = ((bf16[8,136,128]{2,1,0:T(8,128)(2,1)}), bf16[8,136,128]{2,1,0:T(8,128)(2,1)S(1)}, u32[]{:S(2)}, u32[]{:S(2)}) async-start(bf16[8,136,128]{2,1,0:T(8,128)(2,1)} %get-tuple-element.27), calls=%async_computation.1 | async-start | bytes 557056 | tf_op jit(solution)/shard_map/all_to_all | solution.py:220
  35.6 10.4 %all-to-all-start.2 = ((bf16[4,64,256]{2,1,0:T(8,128)(2,1)}), bf16[4,64,256]{2,1,0:T(8,128)(2,1)S(1)}, u32[]{:S(2)}, u32[]{:S(2)}) async-start(bf16[4,64,256]{2,1,0:T(8,128)(2,1)} %shard_map.139), calls=%async_computation.2 | async-start | bytes 262144 | tf_op jit(solution)/shard_map/all_to_all | solution.py:227
  51.0 5.2 %copy-start.18 = (bf16[1,2048,512]{2,1,0:T(8,128)(2,1)S(1)}, bf16[1,2048,512]{2,1,0:T(8,128)(2,1)}, u32[]{:S(2)}) copy-start(bf16[1,2048,512]{2,1,0:T(8,128)(2,1)} %param.25) | copy-start | bytes 6291460
  51.0 30.2 %all-to-all-start.3 = ((bf16[32,8,2048]{2,1,0:T(8,128)(2,1)}), bf16[32,8,2048]{2,1,0:T(8,128)(2,1)S(1)}, u32[]{:S(2)}, u32[]{:S(2)}) async-start(bf16[32,8,2048]{2,1,0:T(8,128)(2,1)} %get-tuple-element.29), calls=%async_computation.3 | async-start | bytes 2097152 | tf_op jit(solution)/shard_map/all_to_all | solution.py:357
  56.2 32.6 %collective-permute-start = (bf16[2048,512]{1,0:T(8,128)(2,1)S(1)}, bf16[2048,512]{1,0:T(8,128)(2,1)}, u32[]{:S(2)}, u32[]{:S(2)}) collective-permute-start(bf16[2048,512]{1,0:T(8,128)(2,1)S(1)} %bitcast.63), channel_id=1, source_target_pairs={{0,3},{1,2},{2,1},{3,0},{4,5},{5,4},{6,7},{7,6},{8,11},{9,10},{10,... | collective-permute-start | bytes 6291464 | tf_op jit(solution)/shard_map/ppermute | solution.py:314
  57.5 59.9 %collective-permute-start.1 = (bf16[2048,512]{1,0:T(8,128)(2,1)}, bf16[2048,512]{1,0:T(8,128)(2,1)}, u32[]{:S(2)}, u32[]{:S(2)}) collective-permute-start(bf16[2048,512]{1,0:T(8,128)(2,1)} %bitcast.64), channel_id=1, source_target_pairs={{0,3},{1,2},{2,1},{3,0},{4,5},{5,4},{6,7},{7,6},{8,11},{9,10},{10,... | collective-permute-start | bytes 6291464 | tf_op jit(solution)/shard_map/ppermute | solution.py:314
  59.6 80.3 %collective-permute-start.2 = (bf16[512,2048]{1,0:T(8,128)(2,1)}, bf16[512,2048]{1,0:T(8,128)(2,1)}, u32[]{:S(2)}, u32[]{:S(2)}) collective-permute-start(bf16[512,2048]{1,0:T(8,128)(2,1)} %bitcast.66), channel_id=1, source_target_pairs={{0,3},{1,2},{2,1},{3,0},{4,5},{5,4},{6,7},{7,6},{8,11},{9,10},{10,... | collective-permute-start | bytes 6291464 | tf_op jit(solution)/shard_map/ppermute | solution.py:314
  60.7 21.0 %collective-permute-start.6 = (bf16[64,2048]{1,0:T(8,128)(2,1)}, bf16[64,2048]{1,0:T(8,128)(2,1)S(1)}, u32[]{:S(2)}, u32[]{:S(2)}) collective-permute-start(bf16[64,2048]{1,0:T(8,128)(2,1)} %get-tuple-element.36), channel_id=1, source_target_pairs={{0,4},{4,0},{1,5},{5,1},{2,6},{6,2},{3,7},{7,3},{8,12},{12,8},{9,1... | collective-permute-start | bytes 786440 | tf_op jit(solution)/shard_map/ppermute | solution.py:348
  60.7 1.8 collective-permute-start.5
  81.2 63.4 %collective-permute-start.3 = (bf16[256,2048]{1,0:T(8,128)(2,1)S(1)}, bf16[256,2048]{1,0:T(8,128)(2,1)}, u32[]{:S(2)}, u32[]{:S(2)}) collective-permute-start(bf16[256,2048]{1,0:T(8,128)(2,1)S(1)} %bitcast.59), channel_id=1, source_target_pairs={{0,1},{1,0},{2,3},{3,2},{4,7},{5,6},{6,5},{7,4},{8,9},{9,8},{10,11... | collective-permute-start | bytes 3145736 | tf_op jit(solution)/shard_map/ppermute | solution.py:360
  83.2 68.2 %all-to-all-start.5 = ((bf16[32,8,2048]{2,1,0:T(8,128)(2,1)}), bf16[32,8,2048]{2,1,0:T(8,128)(2,1)}, u32[]{:S(2)}, u32[]{:S(2)}) async-start(bf16[32,8,2048]{2,1,0:T(8,128)(2,1)} %fusion), calls=%async_computation.5 | async-start | bytes 2097152 | tf_op jit(solution)/shard_map/all_to_all | solution.py:357
  144.6 6.7 %copy-start.1 = (bf16[2048,512]{1,0:T(8,128)(2,1)}, bf16[2048,512]{1,0:T(8,128)(2,1)S(1)}, u32[]{:S(2)}) copy-start(bf16[2048,512]{1,0:T(8,128)(2,1)S(1)} %get-tuple-element.31.u0) | copy-start | bytes 6291460
  144.6 6.7 %copy-start.4 = (bf16[512,2048]{1,0:T(8,128)(2,1)}, bf16[512,2048]{1,0:T(8,128)(2,1)S(1)}, u32[]{:S(2)}) copy-start(bf16[512,2048]{1,0:T(8,128)(2,1)S(1)} %get-tuple-element.32.d0) | copy-start | bytes 6291460
  144.6 6.7 %copy-start.7 = (bf16[2048,512]{1,0:T(8,128)(2,1)}, bf16[2048,512]{1,0:T(8,128)(2,1)S(1)}, u32[]{:S(2)}) copy-start(bf16[2048,512]{1,0:T(8,128)(2,1)S(1)} %get-tuple-element.33.g1) | copy-start | bytes 6291460
  144.6 6.7 %copy-start.10 = (bf16[2048,512]{1,0:T(8,128)(2,1)}, bf16[2048,512]{1,0:T(8,128)(2,1)S(1)}, u32[]{:S(2)}) copy-start(bf16[2048,512]{1,0:T(8,128)(2,1)S(1)} %get-tuple-element.34.u1) | copy-start | bytes 6291460
  144.6 6.7 %copy-start.13 = (bf16[512,2048]{1,0:T(8,128)(2,1)}, bf16[512,2048]{1,0:T(8,128)(2,1)S(1)}, u32[]{:S(2)}) copy-start(bf16[512,2048]{1,0:T(8,128)(2,1)S(1)} %get-tuple-element.35.d1) | copy-start | bytes 6291460
  151.3 15.2 %collective-permute-start.4 = (bf16[256,2048]{1,0:T(8,128)(2,1)}, bf16[256,2048]{1,0:T(8,128)(2,1)}, u32[]{:S(2)}, u32[]{:S(2)}) collective-permute-start(bf16[256,2048]{1,0:T(8,128)(2,1)} %shard_map.143), channel_id=1, source_target_pairs={{0,1},{1,0},{2,3},{3,2},{4,7},{5,6},{6,5},{7,4},{8,9},{9,8},{10,11... | collective-permute-start | bytes 3145736 | tf_op jit(solution)/shard_map/ppermute | solution.py:366
  151.4 40.4 %collective-permute-start.8 = (bf16[256,2048]{1,0:T(8,128)(2,1)}, bf16[256,2048]{1,0:T(8,128)(2,1)}, u32[]{:S(2)}, u32[]{:S(2)}) collective-permute-start(bf16[256,2048]{1,0:T(8,128)(2,1)} %bitcast.23.x_ref), channel_id=1, source_target_pairs={{0,1},{1,0},{2,3},{3,2},{4,7},{5,6},{6,5},{7,4},{8,9},{9,8},{10,11... | collective-permute-start | bytes 3145736 | tf_op jit(solution)/shard_map/ppermute | solution.py:360
  156.6 1.6 copy-start.8
  158.2 1.6 copy-start.11
  159.8 1.6 copy-start.14
  169.0 44.5 %all-to-all-start.4 = ((bf16[32,8,2048]{2,1,0:T(8,128)(2,1)}), bf16[32,8,2048]{2,1,0:T(8,128)(2,1)S(1)}, u32[]{:S(2)}, u32[]{:S(2)}) async-start(bf16[32,8,2048]{2,1,0:T(8,128)(2,1)} %fusion.8), calls=%async_computation.4 | async-start | bytes 2097152 | tf_op jit(solution)/shard_map/all_to_all | solution.py:370
  178.9 1.6 copy-start.3
  180.5 1.6 copy-start.6
  191.7 5.1 %collective-permute-start.7 = (bf16[256,2048]{1,0:T(8,128)(2,1)S(1)}, bf16[256,2048]{1,0:T(8,128)(2,1)S(1)}, u32[]{:S(2)}, u32[]{:S(2)}) collective-permute-start(bf16[256,2048]{1,0:T(8,128)(2,1)S(1)} %shard_map.144), channel_id=1, source_target_pairs={{0,4},{4,0},{1,5},{5,1},{2,6},{6,2},{3,7},{7,3},{8,12},{12,8},{9,1... | collective-permute-start | bytes 3145736 | tf_op jit(solution)/shard_map/ppermute | solution.py:368
  196.7 26.8 %copy-start.19 = (bf16[64,2048]{1,0:T(8,128)(2,1)S(1)}, bf16[64,2048]{1,0:T(8,128)(2,1)}, u32[]{:S(2)}) copy-start(bf16[64,2048]{1,0:T(8,128)(2,1)} %get-tuple-element.28) | copy-start | bytes 786436
  196.7 15.5 %collective-permute-start.9 = (bf16[256,2048]{1,0:T(8,128)(2,1)S(1)}, bf16[256,2048]{1,0:T(8,128)(2,1)S(1)}, u32[]{:S(2)}, u32[]{:S(2)}) collective-permute-start(bf16[256,2048]{1,0:T(8,128)(2,1)S(1)} %shard_map.145), channel_id=1, source_target_pairs={{0,5},{1,4},{2,7},{3,6},{4,3},{5,2},{6,1},{7,0},{8,13},{9,12},{10,... | collective-permute-start | bytes 3145736 | tf_op jit(solution)/shard_map/ppermute | solution.py:366
  213.6 37.6 %all-to-all-start.6 = ((bf16[32,8,2048]{2,1,0:T(8,128)(2,1)}), bf16[32,8,2048]{2,1,0:T(8,128)(2,1)S(1)}, u32[]{:S(2)}, u32[]{:S(2)}) async-start(bf16[32,8,2048]{2,1,0:T(8,128)(2,1)} %fusion.9), calls=%async_computation.6 | async-start | bytes 2097152 | tf_op jit(solution)/shard_map/all_to_all | solution.py:370
  (5 other events, 8.0 us)

commit v5 on v4

--- a/solution.py
+++ b/solution.py
@@ -69,7 +69,14 @@
     return item[:DV], item[DV : DV + 1] + item[DV + 1 : DV + 2] + item[DV + 2 : DV + 3]
 
 
-def local_kernel(k_ref, v_ref, d_ref, state_ref, cum_ref):
+def row_block(first, source, target, buf, sem):
+    inward = pltpu.make_async_copy(source.at[pl.ds(first, buf.shape[0])], buf, sem.at[0])
+    return inward, pltpu.make_async_copy(buf, target, sem.at[1])
+
+
+def local_kernel(k_ref, v_ref, d_ref, w_ref, state_ref, cum_ref, part_ref, buf, sem):
+    inward, outward = row_block(0, w_ref, part_ref, buf, sem)
+    inward.start()
     logit = d_ref[...]
     logdecay = (jnp.minimum(logit, 0.0) - jnp.log1p(jnp.exp(-jnp.abs(logit)))) / DECAY_TEMP
     rows = logdecay.shape[0]
@@ -79,13 +86,18 @@
     ).astype(F32).astype(BF16)
     cum = sum(dot(low, part, ((1,), (0,))) for part in split3(logdecay))
     cum_ref[...] = cum
+    inward.wait()
+    outward.start()
     end = cum[rows - 1 : rows]
     kdec = (k_ref[...].astype(F32) * jnp.exp(end - cum)).astype(BF16)
     state_t = pick_heads(dot(v_ref[...], kdec, ((0,), (0,))))
     store_state(state_ref, state_t, end)
-
-
-def inner_kernel(cum_ref, q_ref, k_ref, v_ref, inner_ref, qdec_ref):
+    outward.wait()
+
+
+def inner_kernel(cum_ref, q_ref, k_ref, v_ref, w_ref, inner_ref, qdec_ref, part_ref, buf, sem):
+    inward, outward = row_block(buf.shape[0], w_ref, part_ref, buf, sem)
+    inward.start()
     rows = q_ref.shape[0]
     half = BLOCK // 2
     cum_all = cum_ref[...]
@@ -98,6 +110,9 @@
     far = (t >= half) & (s < half)
     state = jnp.zeros((DV, 2 * DK), F32)
     for b in range(rows // BLOCK):
+        if b == 2:
+            inward.wait()
+            outward.start()
         at = slice(b * BLOCK, (b + 1) * BLOCK)
         cum = cum_all[at]
         if b:
@@ -126,6 +141,7 @@
             kdec = (k * jnp.exp(end - cum)).astype(BF16)
             added = pick_heads(dot(v, kdec, ((0,), (0,))))
             state = added if b == 0 else state * jnp.exp(end) + added
+    outward.wait()
 
 
 def plane_kernel(at_ref, all_ref, total_ref, before_ref, logb_ref):
@@ -172,7 +188,7 @@
     return pltpu.with_memory_space_constraint(x, pltpu.VMEM)
 
 
-def call(kernel, outs, *args, kept=(), loads=(), scratch=(), flops=2**20, limit=None):
+def call(kernel, outs, *args, kept=(), loads=(), scratch=(), flops=2**20, limit=None, parts=0):
     specs = [
         pl.BlockSpec(memory_space=pltpu.SMEM if a.dtype == jnp.int32 else pltpu.VMEM) for a in args
     ]
@@ -182,7 +198,8 @@
         kernel,
         out_shape=outs,
         in_specs=specs,
-        out_specs=[pl.BlockSpec(memory_space=pltpu.VMEM)] * len(outs),
+        out_specs=[pl.BlockSpec(memory_space=pltpu.VMEM)] * (len(outs) - parts)
+        + [pl.BlockSpec(memory_space=pl.ANY)] * parts,
         scratch_shapes=scratch,
         cost_estimate=pl.CostEstimate(flops=flops, bytes_accessed=2**19, transcendentals=2**16),
         compiler_params=pltpu.CompilerParams(vmem_limit_bytes=limit),
@@ -197,19 +214,21 @@
     return pltpu.VMEM(shape, dtype)
 
 
-def mixer(queries, key_rows, value_rows, out_gate, decay_logit, head_gain):
+def mixer(queries, key_rows, value_rows, out_gate, decay_logit, head_gain, w_up):
     rows = queries.shape[0]
+    half = shaped((w_up.shape[0] // 2, w_up.shape[1]), BF16)
+    through = [pltpu.VMEM(half.shape, BF16), pltpu.SemaphoreType.DMA((2,))]
     planes, members, tps = lax.axis_size("sp_0"), lax.axis_size(PLANE), lax.axis_size("tp")
     packed = DV + 8
-    state, cum = call(
+    state, cum, upper = call(
         local_kernel,
-        [shaped((members, packed, 2 * DK), BF16), shaped((rows, 2 * DK), F32)],
-        key_rows, value_rows, decay_logit,
-    )
-    inner, qdec = call(
+        [shaped((members, packed, 2 * DK), BF16), shaped((rows, 2 * DK), F32), half],
+        key_rows, value_rows, decay_logit, loads=(w_up,), scratch=through, parts=1,
+    )
+    inner, qdec, lower = call(
         inner_kernel,
-        [resident((rows, 2 * DV), F32), resident((rows, 2 * DK), BF16)],
-        cum, queries, key_rows, value_rows,
+        [resident((rows, 2 * DV), F32), resident((rows, 2 * DK), BF16), half],
+        cum, queries, key_rows, value_rows, loads=(w_up,), scratch=through, parts=1,
     )
     in_plane = lax.all_to_all(state, PLANE, 0, 0, tiled=True)
     total, before, logb = call(
@@ -224,7 +243,7 @@
         lax.axis_index("sp_0")[None].astype(jnp.int32), before, logb, inner, qdec, out_gate,
         head_gain[None], kept=(along,), limit=SMALL,
     )
-    return lax.all_to_all(mixed, "tp", 0, 0, tiled=True)
+    return lax.all_to_all(mixed, "tp", 0, 0, tiled=True), upper, lower
 
 
 def clamped_unit(gate_pre, up_pre):
@@ -234,19 +253,25 @@
 
 
 def load_kernel(*refs):
-    count = len(refs) // 2
-    sources, targets, sem = refs[:count], refs[count:-1], refs[-1]
-    copies = [pltpu.make_async_copy(a, b, sem.at[k]) for k, (a, b) in enumerate(zip(sources, targets))]
+    sources, targets, sem = list(refs[:7]), refs[7:13], refs[13]
+    copies = []
+    for target in targets:
+        at = 0
+        while at < target.shape[0]:
+            source = sources.pop(0)
+            place = target.at[pl.ds(at, source.shape[0])]
+            copies.append(pltpu.make_async_copy(source, place, sem.at[len(copies)]))
+            at += source.shape[0]
     for copy in copies:
         copy.start()
     for copy in copies:
         copy.wait()
 
 
-def load(arrays):
+def load(own, other):
     return call(
-        load_kernel, [resident(a.shape, a.dtype) for a in arrays], loads=arrays,
-        scratch=[pltpu.SemaphoreType.DMA((len(arrays),))], limit=SMALL,
+        load_kernel, [resident(a.shape, a.dtype) for a in (*own, *own)], loads=(*own, *other),
+        scratch=[pltpu.SemaphoreType.DMA((7,))], limit=SMALL,
     )
 
 
@@ -309,9 +334,6 @@
 ):
     core_tp = ("sp_2", "tp")
     own = (w_gate[0], w_up[0], w_down[0])
-    other = []
-    for w in own:
-        other.append(lax.ppermute(w, core_tp, WEIGHT_PAIRS))
     experts, cores = lax.axis_size(SP), lax.axis_size("sp_2")
     columns = experts // cores
     quarter, width = residual_in.shape
@@ -331,7 +353,12 @@
     away = lax.dynamic_index_in_dim(both, 1 - core, 3, keepdims=False)
     crossing = lax.ppermute(away[0], "sp_2", swap_cores)
 
-    pieces = mixer(queries, key_rows, value_rows, out_gate, decay_logit, head_gain)
+    pieces, upper, lower = mixer(
+        queries, key_rows, value_rows, out_gate, decay_logit, head_gain, own[1]
+    )
+    other = []
+    for w in (own[0], upper, lower, own[2]):
+        other.append(lax.ppermute(w, core_tp, WEIGHT_PAIRS))
     residual, normed, rows = call(
         prepare_kernel,
         [
@@ -360,7 +387,7 @@
         swapped.append(lax.ppermute(rows, core_tp, ROW_PAIRS))
     routed = residual.astype(F32)
     for c, plan in enumerate((here, away)):
-        weights = load((*own, *other))
+        weights = load(own, other)
         theirs = ffn(swapped[c], weights, shaped)
         mine = ffn(arrived[c], weights, resident)
         back = lax.ppermute(theirs, core_tp, CROSS_PAIRS if c else ROW_PAIRS)

time: 254 us -> 256 us (level)
  Pallas kernels: 35.5 us -> 38.6 us
    pallas_call x10, Pallas kernels: 35.5 us -> 38.6 us  [call(): pl.pallas_call(kernel, out_shape=outs, in_specs=specs, out_specs=[pl.Bloc...]
    ppermute x3 -> x4, starting transfers between devices: 4.49 us -> 6.65 us  [on_device(): other.append(lax.ppermute(w, core_tp, WEIGHT_PAIRS))]
    ppermute x3 -> x4, waiting for transfers between devices: 51 us -> 50.9 us  [on_device(): other.append(lax.ppermute(w, core_tp, WEIGHT_PAIRS))]
    unnamed x41 -> x45, local copies, waits for them, and re-layouts: 15.9 us -> 16 us
  transfers between devices with their start and end apart: 17 -> 18, of which waited for: 10 -> 9; matrix products, arithmetic and copies ran while one was open for 4% -> 3% of each run, Pallas kernels for 10% -> 11%
where the time goes in v5:
time: 256 us; the launch traced here: 254 us
  waiting for transfers between devices  132 us (52%)
  starting transfers between devices  58.4 us (23%)
  Pallas kernels  38.6 us (15%)
  local copies, waits for them, and re-layouts  17.5 us (7%)
  other arithmetic  4.31 us (2%)
  matrix products  3.42 us (1%)
    ppermute x4, waiting for transfers between devices, on_device(): other.append(lax.ppermute(w, core_tp, WEIGHT_PAIRS))  50.9 us
    pallas_call x10, Pallas kernels, call(): pl.pallas_call(kernel, out_shape=outs, in_specs=specs, out_specs=[pl.Bloc...  38.6 us
    all_to_all x2, waiting for transfers between devices, on_device(): lax.all_to_all(out.reshape(columns, cap, width), columns_axes, 0, 0, tile...  27.1 us
    all_to_all x2, starting transfers between devices, on_device(): lax.all_to_all(out.reshape(columns, cap, width), columns_axes, 0, 0, tile...  19.7 us
    all_to_all x2, waiting for transfers between devices, on_device(): rows = lax.all_to_all(rows, columns_axes, 0, 0, tiled=True)  17.7 us
    ppermute x2, waiting for transfers between devices, on_device(): back = lax.ppermute(theirs, core_tp, CROSS_PAIRS if c else ROW_PAIRS)  16.9 us
    unnamed x45, local copies, waits for them, and re-layouts  16 us
    all_to_all x2, starting transfers between devices, on_device(): rows = lax.all_to_all(rows, columns_axes, 0, 0, tiled=True)  10.8 us
  transfers between devices with their start and end apart: 18, of which 9 were waited for; matrix products, arithmetic and copies ran while one was open for 3% of the time, Pallas kernels for 11%

profile of v5, /device:TPU:2, one launch (start us, length us, event | category | flops | bytes accessed | tf_op | source)
XLA Modules:
  0.0 254.2 jit_solution(9444712364642999256)
XLA Ops:
  0.0 4.0 %shard_map.136 = (bf16[8,136,128]{2,1,0:T(8,128)(2,1)}, f32[256,128]{1,0:T(8,128)}, bf16[1024,512]{1,0:T(8,128)(2,1)}) custom-call(bf16[256,128]{1,0:T(8,128)(2,1)} %k_ref.3, bf16[256,256]{1,0:T(8,128)(2,1)} %v_ref.3, f32[256,128]{1,0:T(8,128)} %d_ref.1, bf16[2048,512]{1,0:T(8,128)(2,1)} %bitcast.62), custom_call_target="tpu_custom_call" | custom-call | flops 1048576 | bytes 524288 | tf_op jit(solution)/shard_map/pallas_call | solution.py:197
  4.1 5.7 %all-to-all-start = ((bf16[8,136,128]{2,1,0:T(8,128)(2,1)}), bf16[8,136,128]{2,1,0:T(8,128)(2,1)S(1)}, u32[]{:S(2)}, u32[]{:S(2)}) async-start(bf16[8,136,128]{2,1,0:T(8,128)(2,1)} %get-tuple-element.23), calls=%async_computation | async-start | bytes 557056 | tf_op jit(solution)/shard_map/all_to_all | solution.py:233
  10.2 5.9 %all-to-all-done.all_ref = bf16[8,136,128]{2,1,0:T(8,128)(2,1)S(1)} async-done(((bf16[8,136,128]{2,1,0:T(8,128)(2,1)}), bf16[8,136,128]{2,1,0:T(8,128)(2,1)S(1)}, u32[]{:S(2)}, u32[]{:S(2)}) %all-to-all-start) | async-done | bytes 278560 | tf_op jit(solution)/shard_map/all_to_all | solution.py:233
  16.8 7.7 %all-to-all-start.1 = ((bf16[8,136,128]{2,1,0:T(8,128)(2,1)}), bf16[8,136,128]{2,1,0:T(8,128)(2,1)S(1)}, u32[]{:S(2)}, u32[]{:S(2)}) async-start(bf16[8,136,128]{2,1,0:T(8,128)(2,1)} %get-tuple-element.29), calls=%async_computation.1 | async-start | bytes 557056 | tf_op jit(solution)/shard_map/all_to_all | solution.py:239
  25.4 3.2 %shard_map.138 = (f32[256,256]{1,0:T(8,128)S(1)}, bf16[256,128]{1,0:T(8,128)(2,1)S(1)}, bf16[1024,512]{1,0:T(8,128)(2,1)}) custom-call(f32[256,128]{1,0:T(8,128)} %get-tuple-element.26.cum_ref, bf16[256,128]{1,0:T(8,128)(2,1)} %q_ref.1, bf16[256,128]{1,0:T(8,128)(2,1)} %k_ref.3, bf16[256,256]{1,0:T(8,128)(2,1)} %v_ref.3, bf16[2048,512]{1,0:T(8,128)(2,1)} %bitcast.63), custom_call_target="tpu_custom_call" | custom-call | flops 1048576 | bytes 524288 | tf_op jit(solution)/shard_map/pallas_call | solution.py:197
  28.7 7.6 %all-to-all-done.1.all_ref = bf16[8,136,128]{2,1,0:T(8,128)(2,1)S(1)} async-done(((bf16[8,136,128]{2,1,0:T(8,128)(2,1)}), bf16[8,136,128]{2,1,0:T(8,128)(2,1)S(1)}, u32[]{:S(2)}, u32[]{:S(2)}) %all-to-all-start.1) | async-done | bytes 278560 | tf_op jit(solution)/shard_map/all_to_all | solution.py:239
  37.4 4.5 %all-to-all-start.2 = ((bf16[4,64,256]{2,1,0:T(8,128)(2,1)}), bf16[4,64,256]{2,1,0:T(8,128)(2,1)S(1)}, u32[]{:S(2)}, u32[]{:S(2)}) async-start(bf16[4,64,256]{2,1,0:T(8,128)(2,1)} %shard_map.139), calls=%async_computation.2 | async-start | bytes 262144 | tf_op jit(solution)/shard_map/all_to_all | solution.py:246
  42.5 5.4 %all-to-all-done.2.piece_ref = bf16[4,64,256]{2,1,0:T(8,128)(2,1)S(1)} async-done(((bf16[4,64,256]{2,1,0:T(8,128)(2,1)}), bf16[4,64,256]{2,1,0:T(8,128)(2,1)S(1)}, u32[]{:S(2)}, u32[]{:S(2)}) %all-to-all-start.2) | async-done | bytes 131104 | tf_op jit(solution)/shard_map/all_to_all | solution.py:246
  47.8 5.0 %shard_map.140 = (bf16[64,2048]{1,0:T(8,128)(2,1)}, bf16[64,2048]{1,0:T(8,128)(2,1)}, bf16[32,8,2048]{2,1,0:T(8,128)(2,1)}) custom-call(bf16[64,2048]{1,0:T(8,128)(2,1)} %res_ref.1, bf16[1,2048]{1,0:T(2,128)(2,1)} %broadcast_in_dim.68.gain_ref, f32[32,64]{1,0:T(8,128)} %get-tuple-element.42.rank_ref, bf16[4,64,256]{2,1,0:T(8,128)(2,1)S(1)} %all-to-all-done.2.piece_ref, ...), custom_call_target="tpu_custom_call" | custom-call | flops 1048576 | bytes 524288 | tf_op jit(solution)/shard_map/pallas_call | solution.py:197
  52.9 5.2 %all-to-all-start.3 = ((bf16[32,8,2048]{2,1,0:T(8,128)(2,1)}), bf16[32,8,2048]{2,1,0:T(8,128)(2,1)S(1)}, u32[]{:S(2)}, u32[]{:S(2)}) async-start(bf16[32,8,2048]{2,1,0:T(8,128)(2,1)} %get-tuple-element.31), calls=%async_computation.3 | async-start | bytes 2097152 | tf_op jit(solution)/shard_map/all_to_all | solution.py:384
  59.3 2.1 collective-permute-start.3
  63.2 2.2 collective-permute-start.1
  65.3 17.7 %all-to-all-done.3 = bf16[32,8,2048]{2,1,0:T(8,128)(2,1)S(1)} async-done(((bf16[32,8,2048]{2,1,0:T(8,128)(2,1)}), bf16[32,8,2048]{2,1,0:T(8,128)(2,1)S(1)}, u32[]{:S(2)}, u32[]{:S(2)}) %all-to-all-start.3) | async-done | bytes 1048608 | tf_op jit(solution)/shard_map/all_to_all | solution.py:384
  85.1 5.6 %all-to-all-start.5 = ((bf16[32,8,2048]{2,1,0:T(8,128)(2,1)}), bf16[32,8,2048]{2,1,0:T(8,128)(2,1)}, u32[]{:S(2)}, u32[]{:S(2)}) async-start(bf16[32,8,2048]{2,1,0:T(8,128)(2,1)} %fusion), calls=%async_computation.5 | async-start | bytes 2097152 | tf_op jit(solution)/shard_map/all_to_all | solution.py:384
  90.7 39.7 %collective-permute-done.2.refs_5_ = bf16[1024,512]{1,0:T(8,128)(2,1)} collective-permute-done((bf16[1024,512]{1,0:T(8,128)(2,1)}, bf16[1024,512]{1,0:T(8,128)(2,1)}, u32[]{:S(2)}, u32[]{:S(2)}) %collective-permute-start.2) | collective-permute-done | bytes 1048608 | tf_op jit(solution)/shard_map/ppermute | solution.py:361
  130.4 11.2 %collective-permute-done.1.refs_4_ = bf16[1024,512]{1,0:T(8,128)(2,1)} collective-permute-done((bf16[1024,512]{1,0:T(8,128)(2,1)}, bf16[1024,512]{1,0:T(8,128)(2,1)}, u32[]{:S(2)}, u32[]{:S(2)}) %collective-permute-start.1) | collective-permute-done | bytes 1048608 | tf_op jit(solution)/shard_map/ppermute | solution.py:361
  141.7 4.7 %shard_map.141 = (bf16[2048,512]{1,0:T(8,128)(2,1)S(1)}, bf16[2048,512]{1,0:T(8,128)(2,1)S(1)}, bf16[512,2048]{1,0:T(8,128)(2,1)S(1)}, bf16[2048,512]{1,0:T(8,12...) custom-call(bf16[2048,512]{1,0:T(8,128)(2,1)} %bitcast.65, bf16[2048,512]{1,0:T(8,128)(2,1)} %bitcast.64, ...), custom_call_target="tpu_custom_call" | custom-call | flops 1048576 | bytes 524288 | tf_op jit(solution)/shard_map/pallas_call | solution.py:197
  146.5 6.6 %shard_map.143 = bf16[256,2048]{1,0:T(8,128)(2,1)} custom-call(bf16[256,2048]{1,0:T(8,128)(2,1)} %collective-permute-done.4.x_ref, bf16[2048,512]{1,0:T(8,128)(2,1)S(1)} %get-tuple-element.34.g0, bf16[2048,512]{1,0:T(8,128)(2,1)S(1)} %get-tuple-element.35.u0, bf16[512,2048]{1,0:T(8,128)(2,1)S(1)} %get-tuple-element.36.d0, ...), custom_call_target="tpu_custom_call" | custom-call | flops 3221225472 | bytes 524288 | tf_op jit(solution)/shard_map/pallas_call | solution.py:197
  153.2 2.0 collective-permute-start.9
  155.3 1.6 copy-done.2
  156.8 1.6 copy-done.5
  158.4 1.6 copy-done.8
  163.2 3.6 %shard_map.142 = bf16[256,2048]{1,0:T(8,128)(2,1)S(1)} custom-call(bf16[256,2048]{1,0:T(8,128)(2,1)S(1)} %bitcast.60, bf16[2048,512]{1,0:T(8,128)(2,1)S(1)} %get-tuple-element.34.g0, bf16[2048,512]{1,0:T(8,128)(2,1)S(1)} %copy-done.2, bf16[512,2048]{1,0:T(8,128)(2,1)S(1)} %copy-done.5, bf16[2048,512]{1,0:T(8,128)(2,1)S(1)} %copy-done.8, ...), custom_call_target="tpu_custom_call" | custom-call | flops 3221225472 | bytes 524288 | tf_op jit(solution)/shard_map/pallas_call | solution.py:197
  168.3 2.5 %fusion.8 = bf16[32,8,2048]{2,1,0:T(8,128)(2,1)} fusion(bf16[256,2048]{1,0:T(8,128)(2,1)} %collective-permute-done.5, bf16[256,2048]{1,0:T(8,128)(2,1)S(1)} %shard_map.142), kind=kLoop, calls=%fused_computation.14 | loop fusion | flops 2097152 | bytes 3145728 | tf_op jit(solution)/shard_map/reshape | solution.py:397
  170.9 9.9 %all-to-all-start.4 = ((bf16[32,8,2048]{2,1,0:T(8,128)(2,1)}), bf16[32,8,2048]{2,1,0:T(8,128)(2,1)S(1)}, u32[]{:S(2)}, u32[]{:S(2)}) async-start(bf16[32,8,2048]{2,1,0:T(8,128)(2,1)} %fusion.8), calls=%async_computation.4 | async-start | bytes 2097152 | tf_op jit(solution)/shard_map/all_to_all | solution.py:397
  182.4 1.6 copy-done.6
  184.0 1.6 copy-done.9
  188.7 4.8 %shard_map.144 = bf16[256,2048]{1,0:T(8,128)(2,1)S(1)} custom-call(bf16[256,2048]{1,0:T(8,128)(2,1)} %bitcast.23.x_ref, bf16[2048,512]{1,0:T(8,128)(2,1)S(1)} %get-tuple-element.34.g0, bf16[2048,512]{1,0:T(8,128)(2,1)S(1)} %copy-done.3, bf16[512,2048]{1,0:T(8,128)(2,1)S(1)} %copy-done.6, bf16[2048,512]{1,0:T(8,128)(2,1)S(1)} %copy-done.9, ...), custom_call_target="tpu_custom_call" | custom-call | flops 3221225472 | bytes 524288 | tf_op jit(solution)/shard_map/pallas_call | solution.py:197
  193.6 4.8 %shard_map.145 = bf16[256,2048]{1,0:T(8,128)(2,1)S(1)} custom-call(bf16[256,2048]{1,0:T(8,128)(2,1)} %collective-permute-done.9.x_ref, bf16[2048,512]{1,0:T(8,128)(2,1)S(1)} %get-tuple-element.34.g0, bf16[2048,512]{1,0:T(8,128)(2,1)S(1)} %copy-done.3, bf16[512,2048]{1,0:T(8,128)(2,1)S(1)} %copy-done.6, bf16[2048,512]{1,0:T(8,128)(2,1)S(1)} %copy-done.9, ...), custom_call_target="tpu_custom_call" | custom-call | flops 3221225472 | bytes 524288 | tf_op jit(solution)/shard_map/pallas_call | solution.py:197
  198.6 15.3 %collective-permute-done.10 = bf16[256,2048]{1,0:T(8,128)(2,1)S(1)} collective-permute-done((bf16[256,2048]{1,0:T(8,128)(2,1)S(1)}, bf16[256,2048]{1,0:T(8,128)(2,1)S(1)}, u32[]{:S(2)}, u32[]{:S(2)}) %collective-permute-start.10) | collective-permute-done | bytes 1048608 | tf_op jit(solution)/shard_map/ppermute | solution.py:393
  215.4 9.8 %all-to-all-start.6 = ((bf16[32,8,2048]{2,1,0:T(8,128)(2,1)}), bf16[32,8,2048]{2,1,0:T(8,128)(2,1)S(1)}, u32[]{:S(2)}, u32[]{:S(2)}) async-start(bf16[32,8,2048]{2,1,0:T(8,128)(2,1)} %fusion.9), calls=%async_computation.6 | async-start | bytes 2097152 | tf_op jit(solution)/shard_map/all_to_all | solution.py:397
  225.8 27.1 %all-to-all-done.6 = bf16[32,8,2048]{2,1,0:T(8,128)(2,1)S(1)} async-done(((bf16[32,8,2048]{2,1,0:T(8,128)(2,1)}), bf16[32,8,2048]{2,1,0:T(8,128)(2,1)S(1)}, u32[]{:S(2)}, u32[]{:S(2)}) %all-to-all-start.6) | async-done | bytes 1048608 | tf_op jit(solution)/shard_map/all_to_all | solution.py:397
  (78 shorter events, 22.0 us)
Async XLA Ops:
  0.0 9.8 %copy-start = (s32[256,4]{0,1:T(4,128)S(1)}, s32[256,4]{0,1:T(4,128)}, u32[]{:S(2)}) copy-start(s32[256,4]{0,1:T(4,128)} %param.23) | copy-start | bytes 12292
  0.0 24.5 %copy-start.20 = (f32[64,4]{0,1:T(4,128)S(1)}, f32[64,4]{0,1:T(4,128)}, u32[]{:S(2)}) copy-start(f32[64,4]{0,1:T(4,128)} %param.24) | copy-start | bytes 3076
  0.0 24.8 %copy-start.19 = (bf16[2048]{0:T(1024)(128)(2,1)S(1)}, bf16[2048]{0:T(1024)(128)(2,1)}, u32[]{:S(2)}) copy-start(bf16[2048]{0:T(1024)(128)(2,1)} %param.22) | copy-start | bytes 12292
  4.0 32.3 %copy-start.16 = (bf16[256,256]{1,0:T(8,128)(2,1)S(1)}, bf16[256,256]{1,0:T(8,128)(2,1)}, u32[]{:S(2)}) copy-start(bf16[256,256]{1,0:T(8,128)(2,1)} %gate_ref.1) | copy-start | bytes 393220
  4.1 32.3 %copy-start.17 = (bf16[128]{0:T(256)(128)(2,1)S(1)}, bf16[128]{0:T(256)(128)(2,1)}, u32[]{:S(2)}) copy-start(bf16[128]{0:T(256)(128)(2,1)} %param.20) | copy-start | bytes 772
  4.1 12.0 %all-to-all-start = ((bf16[8,136,128]{2,1,0:T(8,128)(2,1)}), bf16[8,136,128]{2,1,0:T(8,128)(2,1)S(1)}, u32[]{:S(2)}, u32[]{:S(2)}) async-start(bf16[8,136,128]{2,1,0:T(8,128)(2,1)} %get-tuple-element.23), calls=%async_computation | async-start | bytes 557056 | tf_op jit(solution)/shard_map/all_to_all | solution.py:233
  16.8 19.5 %all-to-all-start.1 = ((bf16[8,136,128]{2,1,0:T(8,128)(2,1)}), bf16[8,136,128]{2,1,0:T(8,128)(2,1)S(1)}, u32[]{:S(2)}, u32[]{:S(2)}) async-start(bf16[8,136,128]{2,1,0:T(8,128)(2,1)} %get-tuple-element.29), calls=%async_computation.1 | async-start | bytes 557056 | tf_op jit(solution)/shard_map/all_to_all | solution.py:239
  37.4 10.4 %all-to-all-start.2 = ((bf16[4,64,256]{2,1,0:T(8,128)(2,1)}), bf16[4,64,256]{2,1,0:T(8,128)(2,1)S(1)}, u32[]{:S(2)}, u32[]{:S(2)}) async-start(bf16[4,64,256]{2,1,0:T(8,128)(2,1)} %shard_map.139), calls=%async_computation.2 | async-start | bytes 262144 | tf_op jit(solution)/shard_map/all_to_all | solution.py:246
  52.8 5.2 %copy-start.18 = (bf16[1,2048,512]{2,1,0:T(8,128)(2,1)S(1)}, bf16[1,2048,512]{2,1,0:T(8,128)(2,1)}, u32[]{:S(2)}) copy-start(bf16[1,2048,512]{2,1,0:T(8,128)(2,1)} %param.25) | copy-start | bytes 6291460
  52.9 30.2 %all-to-all-start.3 = ((bf16[32,8,2048]{2,1,0:T(8,128)(2,1)}), bf16[32,8,2048]{2,1,0:T(8,128)(2,1)S(1)}, u32[]{:S(2)}, u32[]{:S(2)}) async-start(bf16[32,8,2048]{2,1,0:T(8,128)(2,1)} %get-tuple-element.31), calls=%async_computation.3 | async-start | bytes 2097152 | tf_op jit(solution)/shard_map/all_to_all | solution.py:384
  58.1 83.6 %collective-permute-start = (bf16[2048,512]{1,0:T(8,128)(2,1)S(1)}, bf16[2048,512]{1,0:T(8,128)(2,1)}, u32[]{:S(2)}, u32[]{:S(2)}) collective-permute-start(bf16[2048,512]{1,0:T(8,128)(2,1)S(1)} %bitcast.66), channel_id=1, source_target_pairs={{0,3},{1,2},{2,1},{3,0},{4,5},{5,4},{6,7},{7,6},{8,11},{9,10},{10,... | collective-permute-start | bytes 6291464 | tf_op jit(solution)/shard_map/ppermute | solution.py:361
  59.3 82.4 %collective-permute-start.3 = (bf16[512,2048]{1,0:T(8,128)(2,1)}, bf16[512,2048]{1,0:T(8,128)(2,1)}, u32[]{:S(2)}, u32[]{:S(2)}) collective-permute-start(bf16[512,2048]{1,0:T(8,128)(2,1)} %bitcast.67), channel_id=1, source_target_pairs={{0,3},{1,2},{2,1},{3,0},{4,5},{5,4},{6,7},{7,6},{8,11},{9,10},{10,... | collective-permute-start | bytes 6291464 | tf_op jit(solution)/shard_map/ppermute | solution.py:361
  61.4 3.9 %collective-permute-start.7 = (bf16[64,2048]{1,0:T(8,128)(2,1)}, bf16[64,2048]{1,0:T(8,128)(2,1)S(1)}, u32[]{:S(2)}, u32[]{:S(2)}) collective-permute-start(bf16[64,2048]{1,0:T(8,128)(2,1)} %get-tuple-element.40), channel_id=1, source_target_pairs={{0,4},{4,0},{1,5},{5,1},{2,6},{6,2},{3,7},{7,3},{8,12},{12,8},{9,1... | collective-permute-start | bytes 786440 | tf_op jit(solution)/shard_map/ppermute | solution.py:375
  61.4 1.8 collective-permute-start.6
  61.9 68.5 %collective-permute-start.2 = (bf16[1024,512]{1,0:T(8,128)(2,1)}, bf16[1024,512]{1,0:T(8,128)(2,1)}, u32[]{:S(2)}, u32[]{:S(2)}) collective-permute-start(bf16[1024,512]{1,0:T(8,128)(2,1)} %get-tuple-element.33), channel_id=1, source_target_pairs={{0,3},{1,2},{2,1},{3,0},{4,5},{5,4},{6,7},{7,6},{8,11},{9,10},{10,... | collective-permute-start | bytes 3145736 | tf_op jit(solution)/shard_map/ppermute | solution.py:361
  63.2 78.5 %collective-permute-start.1 = (bf16[1024,512]{1,0:T(8,128)(2,1)}, bf16[1024,512]{1,0:T(8,128)(2,1)}, u32[]{:S(2)}, u32[]{:S(2)}) collective-permute-start(bf16[1024,512]{1,0:T(8,128)(2,1)} %get-tuple-element.32), channel_id=1, source_target_pairs={{0,3},{1,2},{2,1},{3,0},{4,5},{5,4},{6,7},{7,6},{8,11},{9,10},{10,... | collective-permute-start | bytes 3145736 | tf_op jit(solution)/shard_map/ppermute | solution.py:361
  83.0 63.4 %collective-permute-start.4 = (bf16[256,2048]{1,0:T(8,128)(2,1)S(1)}, bf16[256,2048]{1,0:T(8,128)(2,1)}, u32[]{:S(2)}, u32[]{:S(2)}) collective-permute-start(bf16[256,2048]{1,0:T(8,128)(2,1)S(1)} %bitcast.59), channel_id=1, source_target_pairs={{0,1},{1,0},{2,3},{3,2},{4,7},{5,6},{6,5},{7,4},{8,9},{9,8},{10,11... | collective-permute-start | bytes 3145736 | tf_op jit(solution)/shard_map/ppermute | solution.py:387
  85.1 68.2 %all-to-all-start.5 = ((bf16[32,8,2048]{2,1,0:T(8,128)(2,1)}), bf16[32,8,2048]{2,1,0:T(8,128)(2,1)}, u32[]{:S(2)}, u32[]{:S(2)}) async-start(bf16[32,8,2048]{2,1,0:T(8,128)(2,1)} %fusion), calls=%async_computation.5 | async-start | bytes 2097152 | tf_op jit(solution)/shard_map/all_to_all | solution.py:384
  146.4 6.7 %copy-start.1 = (bf16[2048,512]{1,0:T(8,128)(2,1)}, bf16[2048,512]{1,0:T(8,128)(2,1)S(1)}, u32[]{:S(2)}) copy-start(bf16[2048,512]{1,0:T(8,128)(2,1)S(1)} %get-tuple-element.35.u0) | copy-start | bytes 6291460
  146.4 6.7 %copy-start.4 = (bf16[512,2048]{1,0:T(8,128)(2,1)}, bf16[512,2048]{1,0:T(8,128)(2,1)S(1)}, u32[]{:S(2)}) copy-start(bf16[512,2048]{1,0:T(8,128)(2,1)S(1)} %get-tuple-element.36.d0) | copy-start | bytes 6291460
  146.4 6.7 %copy-start.7 = (bf16[2048,512]{1,0:T(8,128)(2,1)}, bf16[2048,512]{1,0:T(8,128)(2,1)S(1)}, u32[]{:S(2)}) copy-start(bf16[2048,512]{1,0:T(8,128)(2,1)S(1)} %get-tuple-element.37.g1) | copy-start | bytes 6291460
  146.4 6.7 %copy-start.10 = (bf16[2048,512]{1,0:T(8,128)(2,1)}, bf16[2048,512]{1,0:T(8,128)(2,1)S(1)}, u32[]{:S(2)}) copy-start(bf16[2048,512]{1,0:T(8,128)(2,1)S(1)} %get-tuple-element.38.u1) | copy-start | bytes 6291460
  146.4 6.7 %copy-start.13 = (bf16[512,2048]{1,0:T(8,128)(2,1)}, bf16[512,2048]{1,0:T(8,128)(2,1)S(1)}, u32[]{:S(2)}) copy-start(bf16[512,2048]{1,0:T(8,128)(2,1)S(1)} %get-tuple-element.39.d1) | copy-start | bytes 6291460
  153.1 15.2 %collective-permute-start.5 = (bf16[256,2048]{1,0:T(8,128)(2,1)}, bf16[256,2048]{1,0:T(8,128)(2,1)}, u32[]{:S(2)}, u32[]{:S(2)}) collective-permute-start(bf16[256,2048]{1,0:T(8,128)(2,1)} %shard_map.143), channel_id=1, source_target_pairs={{0,1},{1,0},{2,3},{3,2},{4,7},{5,6},{6,5},{7,4},{8,9},{9,8},{10,11... | collective-permute-start | bytes 3145736 | tf_op jit(solution)/shard_map/ppermute | solution.py:393
  153.2 40.4 %collective-permute-start.9 = (bf16[256,2048]{1,0:T(8,128)(2,1)}, bf16[256,2048]{1,0:T(8,128)(2,1)}, u32[]{:S(2)}, u32[]{:S(2)}) collective-permute-start(bf16[256,2048]{1,0:T(8,128)(2,1)} %bitcast.23.x_ref), channel_id=1, source_target_pairs={{0,1},{1,0},{2,3},{3,2},{4,7},{5,6},{6,5},{7,4},{8,9},{9,8},{10,11... | collective-permute-start | bytes 3145736 | tf_op jit(solution)/shard_map/ppermute | solution.py:387
  158.4 1.6 copy-start.8
  170.9 44.5 %all-to-all-start.4 = ((bf16[32,8,2048]{2,1,0:T(8,128)(2,1)}), bf16[32,8,2048]{2,1,0:T(8,128)(2,1)S(1)}, u32[]{:S(2)}, u32[]{:S(2)}) async-start(bf16[32,8,2048]{2,1,0:T(8,128)(2,1)} %fusion.8), calls=%async_computation.4 | async-start | bytes 2097152 | tf_op jit(solution)/shard_map/all_to_all | solution.py:397
  180.8 1.6 copy-start.3
  193.5 5.1 %collective-permute-start.8 = (bf16[256,2048]{1,0:T(8,128)(2,1)S(1)}, bf16[256,2048]{1,0:T(8,128)(2,1)S(1)}, u32[]{:S(2)}, u32[]{:S(2)}) collective-permute-start(bf16[256,2048]{1,0:T(8,128)(2,1)S(1)} %shard_map.144), channel_id=1, source_target_pairs={{0,4},{4,0},{1,5},{5,1},{2,6},{6,2},{3,7},{7,3},{8,12},{12,8},{9,1... | collective-permute-start | bytes 3145736 | tf_op jit(solution)/shard_map/ppermute | solution.py:395
  198.5 26.9 %copy-start.21 = (bf16[64,2048]{1,0:T(8,128)(2,1)S(1)}, bf16[64,2048]{1,0:T(8,128)(2,1)}, u32[]{:S(2)}) copy-start(bf16[64,2048]{1,0:T(8,128)(2,1)} %get-tuple-element.30) | copy-start | bytes 786436
  198.5 15.5 %collective-permute-start.10 = (bf16[256,2048]{1,0:T(8,128)(2,1)S(1)}, bf16[256,2048]{1,0:T(8,128)(2,1)S(1)}, u32[]{:S(2)}, u32[]{:S(2)}) collective-permute-start(bf16[256,2048]{1,0:T(8,128)(2,1)S(1)} %shard_map.145), channel_id=1, source_target_pairs={{0,5},{1,4},{2,7},{3,6},{4,3},{5,2},{6,1},{7,0},{8,13},{9,12},{10,... | collective-permute-start | bytes 3145736 | tf_op jit(solution)/shard_map/ppermute | solution.py:393
  215.4 37.6 %all-to-all-start.6 = ((bf16[32,8,2048]{2,1,0:T(8,128)(2,1)}), bf16[32,8,2048]{2,1,0:T(8,128)(2,1)S(1)}, u32[]{:S(2)}, u32[]{:S(2)}) async-start(bf16[32,8,2048]{2,1,0:T(8,128)(2,1)} %fusion.9), calls=%async_computation.6 | async-start | bytes 2097152 | tf_op jit(solution)/shard_map/all_to_all | solution.py:397
  (8 other events, 12.7 us)
